TPU v7x, 512 devices: a whole 4x8x8 slice. The times are simulated.
512 devices in a mesh: sp: 32 (over z, x), tp: 16 (over y, core).
Axes of the slice: x: 4, y: 8, z: 8, core: 2. Of those that a mesh axis runs over, the one named last changes fastest.
Arguments:
- ffn_input: bfloat16 [4096, 2048], P('sp', 'tp'), may hold values from -6 to 6
- out_grad: bfloat16 [4096, 2048], P('sp', 'tp'), may hold values from -6 to 6
- routes: int32 [4096, 2], P('sp'), may hold values from 0 to 31, all different within a row; in each aligned block of 128 rows (0 to 127, 128 to 255, ...) at most 10 rows name the same one
- route_weight: float32 [4096, 2], P('sp'), may hold values from 0.05 to 1
- gate_w: bfloat16 [32, 2048, 2048], P('sp', None, 'tp'), may hold values from -0.125 to 0.125
- up_w: bfloat16 [32, 2048, 2048], P('sp', None, 'tp'), may hold values from -0.125 to 0.125
- down_w: bfloat16 [32, 2048, 2048], P('sp', 'tp'), may hold values from -0.125 to 0.125
- out_proj: bfloat16 [2048, 2048], P('tp'), may hold values from -0.125 to 0.125
- rec_value: bfloat16 [4096, 2048], P('sp', 'tp'), may hold values from -6 to 6
- rate_pre: bfloat16 [4096, 2048], P('sp', 'tp'), may hold values from -6 to 6
- input_pre: bfloat16 [4096, 2048], P('sp', 'tp'), may hold values from -4 to 4
- prev_state: bfloat16 [4096, 2048], P('sp', 'tp'), may hold values from -6 to 6
- decay_param: float32 [2048], P('tp'), may hold values from 4 to 12
Outputs:
- gate_w_grad: bfloat16 [32, 2048, 2048], P('sp', None, 'tp')
- up_w_grad: bfloat16 [32, 2048, 2048], P('sp', None, 'tp')
- down_w_grad: bfloat16 [32, 2048, 2048], P('sp', 'tp')
- out_proj_grad: float32 [2048, 2048], P('sp', 'tp')
- rec_value_grad: bfloat16 [4096, 2048], P('sp', 'tp')
- rate_pre_grad: bfloat16 [4096, 2048], P('sp', 'tp')
- input_pre_grad: bfloat16 [4096, 2048], P('sp', 'tp')
Inputs may be any that keep to these rules, and one draw needn't show every extreme that they name: `routes`: each token names 2 different experts. Within each aligned block of 128 tokens no expert is named more than 10 times, a bound that some block reaches.
All inputs are finite; a program needn't handle non-finite values.
Results may differ from a plain program's by a relative error of at most 0.02.
Values may be sent and summed in bfloat16 or wider, within the bound.
No kernel may reach another device: no remote copies, remote signals or barrier semaphores. Data moves between devices by JAX's collectives and lax.ppermute only.
A program may use at most 64 MiB of HBM per device.

v0:
```python
import functools

import jax
import jax.numpy as jnp
from jax import lax
from jax.experimental import pallas as pl
from jax.experimental.pallas import tpu as pltpu
from jax.sharding import Mesh
from jax.sharding import PartitionSpec as P

SP = ("z", "x")
TP = ("y", "c")
F32 = jnp.float32
BF16 = jnp.bfloat16
decay_scale = 8.0

SMEM = pl.BlockSpec(memory_space=pltpu.SMEM)
VMEM = pl.BlockSpec(memory_space=pltpu.VMEM)


def whole(shape, dtype):
    return jax.ShapeDtypeStruct(shape, dtype)


def dot(a, b, dims):
    return lax.dot_general(a, b, (dims, ((), ())), preferred_element_type=F32)


def iota(shape, dim):
    return lax.broadcasted_iota(jnp.int32, shape, dim)


def route_body(core, routes, weights, pick, choose, scale, *, experts, half):
    me = core[0]
    count, tokens = routes.shape
    slots = experts * half
    here = [iota((experts, tokens), 0) == routes[k : k + 1, :] for k in range(count)]
    named = functools.reduce(jnp.logical_or, here)
    earlier = iota((tokens, tokens), 0) < iota((tokens, tokens), 1)
    before = dot(
        jnp.where(named, 1.0, 0.0).astype(BF16), jnp.where(earlier, 1.0, 0.0).astype(BF16), ((1,), (0,))
    )
    back, mine = [], []
    for k in range(count):
        rank = jnp.sum(jnp.where(here[k], before, 0.0), axis=0, keepdims=True).astype(jnp.int32)
        name = routes[k : k + 1, :]
        back.append(name * 16 + rank + jnp.where(rank >= half, 8 - half, 0))
        at = rank - me * half
        mine.append(jnp.where((at >= 0) & (at < half), name * half + at, -1))
    hit = functools.reduce(jnp.logical_or, [iota(pick.shape, 0) == b for b in back])
    pick[...] = jnp.where(hit, 1.0, 0.0).astype(BF16)
    row = iota((slots, tokens), 0)
    hits = [row == m for m in mine]
    scale[...] = sum(
        jnp.sum(jnp.where(h, weights[k : k + 1, :], 0.0), axis=1, keepdims=True)
        for k, h in enumerate(hits)
    )
    choose[...] = jnp.where(functools.reduce(jnp.logical_or, hits), 1.0, 0.0).astype(BF16)


def route_slots(core, routes, weights, experts, half):
    tokens, slots = routes.shape[1], experts * half
    return pl.pallas_call(
        functools.partial(route_body, experts=experts, half=half),
        out_shape=(
            whole((experts * 16, tokens), BF16),
            whole((slots, tokens), BF16),
            whole((slots, 1), F32),
        ),
        in_specs=[SMEM] + [VMEM] * 2,
        name="route_slots",
    )(core, routes, weights)


def fill_body(core, choose, scale, mine, peer, send, rows):
    me = core[0]
    slots = choose.shape[0]
    for a in range(2):
        for n in range(2):
            for c in range(2):
                x = jnp.where(me == c, mine[n, a], peer[n, a])
                r = dot(choose[...], x, ((1,), (0,)))
                rows[pl.ds(4 * a + 2 * n + c, slots, stride=8), :] = scale[...] * r if a else r
    send[...] = rows[...].astype(BF16)


def fill_slots(core, choose, scale, mine, peer):
    fw = mine.shape[-1]
    total = choose.shape[0] * 8
    return pl.pallas_call(
        fill_body,
        out_shape=whole((total, fw), BF16),
        in_specs=[SMEM] + [VMEM] * 4,
        scratch_shapes=[pltpu.VMEM((total, fw), F32)],
        name="fill_slots",
    )(core, choose, scale, mine, peer)


def sort_body(recv, both, near, rows):
    slots = recv.shape[0] // 8
    rows[...] = recv[...].astype(F32)
    for a in range(2):
        for n in range(2):
            for c in range(2):
                v = rows[pl.ds(4 * a + 2 * n + c, slots, stride=8), :].astype(BF16)
                both[n, 2 * a + c] = v
                if n == 0:
                    near[2 * a + c] = v


def sort_pieces(recv):
    slots, fw = recv.shape[0] // 8, recv.shape[1]
    return pl.pallas_call(
        sort_body,
        out_shape=(whole((2, 4, slots, fw), BF16), whole((4, slots, fw), BF16)),
        scratch_shapes=[pltpu.VMEM(recv.shape, F32)],
        name="sort_pieces",
    )(recv)


def shards(chip, both, f1, b1, f2, b2, n_y):
    found = []
    for off, ref in ((0, both), (n_y - 1, f1), (1, b1)):
        for n in range(2):
            found.append((off + 4 * n, [ref[n, i] for i in range(4)]))
    for off, ref in ((n_y - 2, f2), (2, b2)):
        found.append((off, [ref[i] for i in range(4)]))
    for off, p in found:
        y = lax.rem(chip + off, n_y)
        yield y, jnp.concatenate(p[:2], axis=1), jnp.concatenate(p[2:], axis=1)


def expert_body(chip, both, f1, b1, f2, b2, wgu_peer, wg, wu, wd, wd_peer, gu_grad, hidden, part):
    n_y = part.shape[0]
    fw = wd.shape[0]
    rows, hid = hidden.shape
    acc = jnp.zeros((rows, 2 * hid), F32)
    back = jnp.zeros((rows, hid), F32)

    def weights(y):
        at = pl.ds(pl.multiple_of(y * 2 * fw, 2 * fw), 2 * fw)
        return jnp.concatenate([wg[at, :], wgu_peer[0, at, :], wu[at, :], wgu_peer[1, at, :]], axis=1), at

    for y, x_in, x_cot in shards(chip[0], both, f1, b1, f2, b2, n_y):
        w, at = weights(y)
        acc = acc + dot(x_in, w, ((1,), (0,)))
        back = back + dot(x_cot, jnp.concatenate([wd[:, at], wd_peer[:, at]], axis=0), ((1,), (1,)))
    gate, up = acc[:, :hid], acc[:, hid:]
    squash = jax.nn.sigmoid(gate)
    silu = gate * squash
    hidden[...] = (silu * up).astype(BF16)
    g_grad = (back * up * squash * (1.0 + gate * (1.0 - squash))).astype(BF16)
    u_grad = (back * silu).astype(BF16)
    grads = jnp.concatenate([g_grad, u_grad], axis=1)
    gu_grad[...] = grads
    for y in range(n_y):
        w, _ = weights(y)
        r = dot(grads, w, ((1,), (1,))).astype(BF16)
        part[y, 0] = r[:, :fw]
        part[y, 1] = r[:, fw:]


def expert_rows_grad(chip, blocks, wgu_peer, wg, wu, wd, wd_peer, n_y):
    rows, fw = blocks[0].shape[2:]
    hid = 2 * wg.shape[1]

    return pl.pallas_call(
        expert_body,
        out_shape=(
            whole((rows, 2 * hid), BF16),
            whole((rows, hid), BF16),
            whole((n_y, 2, rows, fw), BF16),
        ),
        in_specs=[SMEM] + [VMEM] * 10,
        name="expert_rows_grad",
    )(chip, *blocks, wgu_peer, wg, wu, wd, wd_peer)


def weight_body(chip, both, f1, b1, f2, b2, gu_grad, hidden, dgu, dgu_send, dd, dd_send):
    fw = dd.shape[0]
    hid = hidden.shape[1]
    n_y = dd.shape[1] // (2 * fw)
    for y, x_in, x_cot in shards(chip[0], both, f1, b1, f2, b2, n_y):
        at = pl.ds(pl.multiple_of(y * 2 * fw, 2 * fw), 2 * fw)
        r = dot(x_in, gu_grad[...], ((0,), (0,))).astype(BF16)
        for i in range(2):
            dgu[i, at, :] = r[:, i * hid : i * hid + fw]
            dgu_send[i, at, :] = r[:, i * hid + fw : (i + 1) * hid]
        r = dot(hidden[...], x_cot, ((0,), (0,))).astype(BF16)
        dd[:, at] = r[:fw]
        dd_send[:, at] = r[fw:]


def expert_weight_grads(chip, blocks, gu_grad, hidden, d):
    fw = blocks[0].shape[3]
    return pl.pallas_call(
        weight_body,
        out_shape=(whole((2, d, fw), BF16), whole((2, d, fw), BF16), whole((fw, d), BF16), whole((fw, d), BF16)),
        in_specs=[SMEM] + [VMEM] * 7,
        name="expert_weight_grads",
    )(chip, *blocks, gu_grad, hidden)


def add_body(parts, out, *, half):
    n_y, n_h, rows, _ = parts.shape
    j, r = iota((out.shape[0], rows), 0), iota((out.shape[0], rows), 1)
    slot = j & 7
    source = (j >> 4) * half + slot
    total = 0.0
    for h in range(n_h):
        s = parts[0, h].astype(F32)
        for y in range(1, n_y):
            s = s + parts[y, h].astype(F32)
        hit = (source == r) & (slot < half) & (((j >> 3) & 1) == h)
        total = total + dot(jnp.where(hit, 1.0, 0.0).astype(BF16), s.astype(BF16), ((1,), (0,)))
    out[...] = total.astype(BF16)


def add_parts(parts, blocks, half):
    return pl.pallas_call(
        functools.partial(add_body, half=half),
        out_shape=whole((blocks * 16, parts.shape[3]), BF16),
        name="add_parts",
    )(parts)


def later(v, step, fill):
    return jnp.concatenate([v[step:], jnp.full((step, v.shape[1]), fill, v.dtype)], axis=0)


def in_three(v):
    hi = v.astype(BF16)
    mid = (v - hi.astype(F32)).astype(BF16)
    lo = (v - hi.astype(F32) - mid.astype(F32)).astype(BF16)
    return [p.astype(F32) for p in (hi, mid, lo)]


def chain_body(mix, out_proj, rec_state, decay, local, through, last):
    n_sp, width = last.shape[0], last.shape[2]
    keep = mix.shape[1] // n_sp
    proj = dot(mix[...], rec_state[...], ((0,), (0,))).astype(BF16)
    for k in range(n_sp):
        last[k, :keep, :] = proj[k * keep : (k + 1) * keep, :]
    grad = dot(mix[...], out_proj[...], ((1,), (1,)))
    mult = later(decay[...], 1, 1.0)
    step = 1
    while step < grad.shape[0]:
        grad = grad + mult * later(grad, step, 0.0)
        mult = mult * later(mult, step, 1.0)
        step *= 2
    local[...] = grad
    through[...] = mult
    first = decay[0:1, :]
    row = iota((last.shape[1] - keep, width), 0)
    chain = jnp.zeros(row.shape, F32)
    for i, piece in enumerate(in_three(first * mult[0:1, :]) + in_three(first * grad[0:1, :])):
        chain = jnp.where(row == i, piece, chain)
    chain = chain.astype(BF16)
    for k in range(n_sp):
        last[k, keep:, :] = chain


def chain_within(mix, out_proj, rec_state, decay, n_sp):
    tokens, width = decay.shape
    return pl.pallas_call(
        chain_body,
        out_shape=(
            whole((tokens, width), F32),
            whole((tokens, width), F32),
            whole((n_sp, mix.shape[1] // n_sp + 8, width), BF16),
        ),
        name="chain_within",
    )(mix, out_proj, rec_state, decay)


def finish_body(here, last, local, through, value_by, input_by, rate_by, proj, value, inp, rate):
    n_sp = last.shape[0]
    keep = proj.shape[0]
    incoming = jnp.zeros((1, last.shape[2]), F32)
    for k in reversed(range(n_sp)):
        c = last[k, keep:, :].astype(F32)
        mult = (c[2:3] + c[1:2]) + c[0:1]
        add = (c[5:6] + c[4:5]) + c[3:4]
        incoming = jnp.where(k > here[0], add + mult * incoming, incoming)
    carried = local[...] + through[...] * incoming
    value[...] = (carried * value_by[...]).astype(BF16)
    inp[...] = (carried * input_by[...]).astype(BF16)
    rate[...] = (carried * rate_by[...]).astype(BF16)
    total = last[0, :keep, :].astype(F32)
    for k in range(1, n_sp):
        total = total + last[k, :keep, :].astype(F32)
    proj[...] = total


def finish(here, last, local, through, value_by, input_by, rate_by):
    grid = whole(local.shape, BF16)
    return pl.pallas_call(
        finish_body,
        out_shape=(whole((last.shape[1] - 8, last.shape[2]), F32), grid, grid, grid),
        in_specs=[SMEM] + [VMEM] * 6,
        name="finish",
    )(here, last, local, through, value_by, input_by, rate_by)


def per_device(
    ffn_input,
    out_grad,
    routes,
    route_weight,
    gate_w,
    up_w,
    down_w,
    out_proj,
    rec_value,
    rate_pre,
    input_pre,
    prev_state,
    decay_param,
):
    n_sp, n_y = lax.axis_size(SP), lax.axis_size("y")
    tok, count = routes.shape
    half = 5 * count * tok // (8 * n_sp)
    fw = ffn_input.shape[1]
    d = gate_w.shape[1]
    chip = lax.axis_index("y").reshape(1).astype(jnp.int32)
    core = lax.axis_index("c").reshape(1).astype(jnp.int32)

    def over_y(v, step):
        return lax.ppermute(v, "y", [(i, (i + step) % n_y) for i in range(n_y)])

    def over_cores(v):
        return lax.ppermute(v, "c", [(0, 1), (1, 0)])

    own = jnp.stack([ffn_input, out_grad])
    far = over_y(own, n_y // 2)
    mine = jnp.stack([own, far])
    peer = over_cores(mine)
    pick, choose, scale = route_slots(core, routes.T, route_weight.T, n_sp, half)
    send = fill_slots(core, choose, scale, mine, peer)

    send, late_gate, late_up, late_down = lax.optimization_barrier((send, gate_w, up_w, down_w))
    wgu = jnp.concatenate([late_gate, late_up], axis=0)
    wgu_peer = over_cores(wgu)
    wd_peer = over_cores(late_down[0])
    recv = lax.all_to_all(send.reshape(n_sp, -1, fw), SP, 0, 0, tiled=True).reshape(send.shape)
    both, near = sort_pieces(recv)
    blocks = (both, over_y(both, 1), over_y(both, -1), over_y(near, 2), over_y(near, -2))

    gu_grad, hidden, part = expert_rows_grad(
        chip, blocks, wgu_peer, gate_w[0], up_w[0], down_w[0], wd_peer, n_y
    )
    arrived = lax.all_to_all(part.reshape(2 * n_y, *part.shape[2:]), TP, 0, 0, tiled=True)
    back = add_parts(arrived.reshape(part.shape), n_sp, half)
    returned = lax.all_to_all(back.reshape(n_sp, 16, fw), SP, 0, 0, tiled=True).reshape(back.shape)
    dgu, dgu_send, dd, dd_send = expert_weight_grads(chip, blocks, gu_grad, hidden, d)
    dgu_sum = (dgu.astype(F32) + over_cores(dgu_send).astype(F32)).astype(BF16)
    d_down = (dd.astype(F32) + over_cores(dd_send).astype(F32)).astype(BF16)
    own_grad = (dot(pick, returned, ((0,), (0,))) + out_grad.astype(F32)).astype(BF16)
    mix_grad = lax.all_gather(own_grad, TP, axis=1, tiled=True)

    rate_gate = jax.nn.sigmoid(rate_pre.astype(F32))
    input_gate = jax.nn.sigmoid(input_pre.astype(F32))
    decay_speed = jax.nn.softplus(-decay_param)[None, :]
    log_decay = -decay_scale * rate_gate * decay_speed
    decay = jnp.exp(log_decay)
    scale_in = jnp.sqrt(-jnp.expm1(2.0 * log_decay))
    signal = rec_value.astype(F32)
    before_state = prev_state.astype(F32)
    rec_state = (decay * before_state + scale_in * input_gate * signal).astype(BF16)
    value_by = scale_in * input_gate
    input_by = value_by * signal * (1.0 - input_gate)
    decay_part = decay * before_state - input_gate * signal * decay * decay / scale_in
    rate_by = decay_part * (-decay_scale * decay_speed) * rate_gate * (1.0 - rate_gate)

    local, through, last = chain_within(mix_grad, out_proj, rec_state, decay, n_sp)
    last = lax.all_to_all(last, SP, 0, 0, tiled=True)
    here = lax.axis_index(SP).reshape(1).astype(jnp.int32)
    out_proj_grad, rec_value_grad, input_pre_grad, rate_pre_grad = finish(
        here, last, local, through, value_by, input_by, rate_by
    )
    return (
        dgu_sum[0][None],
        dgu_sum[1][None],
        d_down[None],
        out_proj_grad,
        rec_value_grad,
        rate_pre_grad,
        input_pre_grad,
    )


def solution(mesh):
    finer = Mesh(mesh.devices.reshape(8, 4, 8, 2), ("z", "x", "y", "c"))
    grid = P(SP, TP)
    return jax.shard_map(
        per_device,
        mesh=finer,
        in_specs=(
            grid,
            grid,
            P(SP, None),
            P(SP, None),
            P(SP, None, TP),
            P(SP, None, TP),
            P(SP, TP, None),
            P(TP, None),
            grid,
            grid,
            grid,
            grid,
            P(TP),
        ),
        out_specs=(P(SP, None, TP), P(SP, None, TP), P(SP, TP, None), grid, grid, grid, grid),
        check_vma=False,
    )
```

profile of v0, /device:TPU:8, one launch (start us, length us, event | category | flops | bytes accessed | tf_op | source)
XLA Modules:
  0.0 175.2 jit_solution(12934678302205156756)
XLA Ops:
  0.7 0.9 fusion.9
  1.5 6.8 %collective-permute-start = (bf16[2,128,128]{2,1,0:T(8,128)(2,1)S(1)}, bf16[2,128,128]{2,1,0:T(8,128)(2,1)S(1)}, u32[]{:S(2)}, u32[]{:S(2)}) collective-permute-start(bf16[2,128,128]{2,1,0:T(8,128)(2,1)S(1)} %get-tuple-element.59), channel_id=1, source_target_pairs={{0,8},{2,10},{4,12},{6,14},{8,0},{10,2},{12,4},{14,6},{1,9},{3,11}... | collective-permute-start | bytes 196616 | tf_op jit(solution)/shard_map/ppermute | solution.py:329
  8.4 3.2 %collective-permute-done = bf16[2,128,128]{2,1,0:T(8,128)(2,1)S(1)} collective-permute-done((bf16[2,128,128]{2,1,0:T(8,128)(2,1)S(1)}, bf16[2,128,128]{2,1,0:T(8,128)(2,1)S(1)}, u32[]{:S(2)}, u32[]{:S(2)}) %collective-permute-start) | collective-permute-done | bytes 65568 | tf_op jit(solution)/shard_map/ppermute | solution.py:329
  11.6 1.9 %collective-permute-start.1 = (bf16[2,2,128,128]{3,2,1,0:T(8,128)(2,1)S(1)}, bf16[2,2,128,128]{3,2,1,0:T(8,128)(2,1)S(1)}, u32[]{:S(2)}, u32[]{:S(2)}) collective-permute-start(bf16[2,2,128,128]{3,2,1,0:T(8,128)(2,1)S(1)} %pad_maximum_fusion.1.mine), channel_id=1, source_target_pairs={{0,1},{1,0},{2,3},{3,2},{4,5},{5,4},{6,7},{7,6},{8,9},{9,8},{10,11... | collective-permute-start | bytes 393224 | tf_op jit(solution)/shard_map/ppermute | solution.py:332
  13.6 1.6 route_slots.1
  15.9 2.0 %fill_slots.1 = bf16[1280,128]{1,0:T(8,128)(2,1)} custom-call(s32[1]{0:T(128)} %bitcast.1.core, bf16[160,128]{1,0:T(8,128)(2,1)} %get-tuple-element.30.choose, f32[160,1]{1,0:T(8,128)} %get-tuple-element.31.scale, bf16[2,2,128,128]{3,2,1,0:T(8,128)(2,1)} %copy-done.14, bf16[2,2,128,128]{3,2,1,0:T(8,128)(2,1)} %copy-done.15), custom_call_target="tpu_custom_call" | custom-call | tf_op jit(solution)/shard_map/fill_slots/pallas_call | solution.py:90
  18.0 2.5 %collective-permute-start.6 = (bf16[2,2048,128]{2,1,0:T(8,128)(2,1)S(1)}, bf16[2,2048,128]{2,1,0:T(8,128)(2,1)S(1)}, u32[]{:S(2)}, u32[]{:S(2)}) collective-permute-start(bf16[2,2048,128]{2,1,0:T(8,128)(2,1)S(1)} %pad_maximum_fusion), channel_id=1, source_target_pairs={{0,1},{1,0},{2,3},{3,2},{4,5},{5,4},{6,7},{7,6},{8,9},{9,8},{10,11... | collective-permute-start | bytes 3145736 | tf_op jit(solution)/shard_map/ppermute | solution.py:332
  20.6 13.2 %all-to-all-start = ((bf16[32,40,128]{2,1,0:T(8,128)(2,1)}), bf16[32,40,128]{2,1,0:T(8,128)(2,1)S(1)}, u32[]{:S(2)}, u32[]{:S(2)}) async-start(bf16[32,40,128]{2,1,0:T(8,128)(2,1)} %bitcast.8), calls=%async_computation | async-start | bytes 655360 | tf_op jit(solution)/shard_map/all_to_all | solution.py:345
  33.7 1.9 %collective-permute-start.7 = (bf16[128,2048]{1,0:T(8,128)(2,1)S(1)}, bf16[128,2048]{1,0:T(8,128)(2,1)}, u32[]{:S(2)}, u32[]{:S(2)}) collective-permute-start(bf16[128,2048]{1,0:T(8,128)(2,1)S(1)} %bitcast.30), channel_id=1, source_target_pairs={{0,1},{1,0},{2,3},{3,2},{4,5},{5,4},{6,7},{7,6},{8,9},{9,8},{10,11... | collective-permute-start | bytes 1572872 | tf_op jit(solution)/shard_map/ppermute | solution.py:332
  35.7 12.4 %all-to-all-done = bf16[32,40,128]{2,1,0:T(8,128)(2,1)S(1)} async-done(((bf16[32,40,128]{2,1,0:T(8,128)(2,1)}), bf16[32,40,128]{2,1,0:T(8,128)(2,1)S(1)}, u32[]{:S(2)}, u32[]{:S(2)}) %all-to-all-start) | async-done | bytes 327712 | tf_op jit(solution)/shard_map/all_to_all | solution.py:345
  48.8 1.9 %sort_pieces.1 = (bf16[2,4,160,128]{3,2,1,0:T(8,128)(2,1)}, bf16[4,160,128]{2,1,0:T(8,128)(2,1)}) custom-call(bf16[1280,128]{1,0:T(8,128)(2,1)} %bitcast.27), custom_call_target="tpu_custom_call" | custom-call | tf_op jit(solution)/shard_map/sort_pieces/pallas_call | solution.py:113
  50.7 3.0 %collective-permute-start.3 = (bf16[2,4,160,128]{3,2,1,0:T(8,128)(2,1)}, bf16[2,4,160,128]{3,2,1,0:T(8,128)(2,1)S(1)}, u32[]{:S(2)}, u32[]{:S(2)}) collective-permute-start(bf16[2,4,160,128]{3,2,1,0:T(8,128)(2,1)} %get-tuple-element.33.both), channel_id=1, source_target_pairs={{0,14},{2,0},{4,2},{6,4},{8,6},{10,8},{12,10},{14,12},{1,15},{3,1}... | collective-permute-start | bytes 983048 | tf_op jit(solution)/shard_map/ppermute | solution.py:329
  53.7 3.5 %collective-permute-start.2 = (bf16[2,4,160,128]{3,2,1,0:T(8,128)(2,1)}, bf16[2,4,160,128]{3,2,1,0:T(8,128)(2,1)S(1)}, u32[]{:S(2)}, u32[]{:S(2)}) collective-permute-start(bf16[2,4,160,128]{3,2,1,0:T(8,128)(2,1)} %get-tuple-element.33.both), channel_id=1, source_target_pairs={{0,2},{2,4},{4,6},{6,8},{8,10},{10,12},{12,14},{14,0},{1,3},{3,5},... | collective-permute-start | bytes 983048 | tf_op jit(solution)/shard_map/ppermute | solution.py:329
  57.1 6.9 %collective-permute-start.5 = (bf16[4,160,128]{2,1,0:T(8,128)(2,1)}, bf16[4,160,128]{2,1,0:T(8,128)(2,1)S(1)}, u32[]{:S(2)}, u32[]{:S(2)}) collective-permute-start(bf16[4,160,128]{2,1,0:T(8,128)(2,1)} %get-tuple-element.34), channel_id=1, source_target_pairs={{0,12},{2,14},{4,0},{6,2},{8,4},{10,6},{12,8},{14,10},{1,13},{3,15... | collective-permute-start | bytes 491528 | tf_op jit(solution)/shard_map/ppermute | solution.py:329
  64.0 1.9 %collective-permute-start.4 = (bf16[4,160,128]{2,1,0:T(8,128)(2,1)}, bf16[4,160,128]{2,1,0:T(8,128)(2,1)S(1)}, u32[]{:S(2)}, u32[]{:S(2)}) collective-permute-start(bf16[4,160,128]{2,1,0:T(8,128)(2,1)} %get-tuple-element.34), channel_id=1, source_target_pairs={{0,4},{2,6},{4,8},{6,10},{8,12},{10,14},{12,0},{14,2},{1,5},{3,7},... | collective-permute-start | bytes 491528 | tf_op jit(solution)/shard_map/ppermute | solution.py:329
  65.9 2.9 %collective-permute-done.5.b2 = bf16[4,160,128]{2,1,0:T(8,128)(2,1)S(1)} collective-permute-done((bf16[4,160,128]{2,1,0:T(8,128)(2,1)}, bf16[4,160,128]{2,1,0:T(8,128)(2,1)S(1)}, u32[]{:S(2)}, u32[]{:S(2)}) %collective-permute-start.5) | collective-permute-done | bytes 163872 | tf_op jit(solution)/shard_map/ppermute | solution.py:329
  68.8 6.4 %collective-permute-done.4.f2 = bf16[4,160,128]{2,1,0:T(8,128)(2,1)S(1)} collective-permute-done((bf16[4,160,128]{2,1,0:T(8,128)(2,1)}, bf16[4,160,128]{2,1,0:T(8,128)(2,1)S(1)}, u32[]{:S(2)}, u32[]{:S(2)}) %collective-permute-start.4) | collective-permute-done | bytes 163872 | tf_op jit(solution)/shard_map/ppermute | solution.py:329
  76.5 5.1 %expert_rows_grad.1 = (bf16[160,512]{1,0:T(8,128)(2,1)}, bf16[160,256]{1,0:T(8,128)(2,1)}, bf16[8,2,160,128]{3,2,1,0:T(8,128)(2,1)}) custom-call(s32[1]{0:T(128)} %bitcast.chip, bf16[2,4,160,128]{3,2,1,0:T(8,128)(2,1)} %get-tuple-element.33.both, bf16[2,4,160,128]{3,2,1,0:T(8,128)(2,1)} %copy-done.5, bf16[2,4,160,128]{3,2,1,0:T(8,128)(2,1)} %copy-done.4, ...), custom_call_target="tpu_custom_call" | custom-call | tf_op jit(solution)/shard_map/expert_rows_grad/pallas_call | solution.py:167
  81.7 4.3 %all-to-all-start.1 = ((bf16[16,160,128]{2,1,0:T(8,128)(2,1)}), bf16[16,160,128]{2,1,0:T(8,128)(2,1)S(1)}, u32[]{:S(2)}, u32[]{:S(2)}) async-start(bf16[16,160,128]{2,1,0:T(8,128)(2,1)} %bitcast.28), calls=%async_computation.1 | async-start | bytes 1310720 | tf_op jit(solution)/shard_map/all_to_all | solution.py:352
  86.0 16.5 %all-to-all-done.1 = bf16[16,160,128]{2,1,0:T(8,128)(2,1)S(1)} async-done(((bf16[16,160,128]{2,1,0:T(8,128)(2,1)}), bf16[16,160,128]{2,1,0:T(8,128)(2,1)S(1)}, u32[]{:S(2)}, u32[]{:S(2)}) %all-to-all-start.1) | async-done | bytes 655392 | tf_op jit(solution)/shard_map/all_to_all | solution.py:352
  103.3 2.1 %add_parts.1 = bf16[512,128]{1,0:T(8,128)(2,1)} custom-call(bf16[8,2,160,128]{3,2,1,0:T(8,128)(2,1)} %bitcast.24), custom_call_target="tpu_custom_call" | custom-call | tf_op jit(solution)/shard_map/add_parts/pallas_call | solution.py:220
  105.4 5.1 %all-to-all-start.2 = ((bf16[32,16,128]{2,1,0:T(8,128)(2,1)}), bf16[32,16,128]{2,1,0:T(8,128)(2,1)S(1)}, u32[]{:S(2)}, u32[]{:S(2)}) async-start(bf16[32,16,128]{2,1,0:T(8,128)(2,1)} %bitcast.32), calls=%async_computation.2 | async-start | bytes 262144 | tf_op jit(solution)/shard_map/all_to_all | solution.py:354
  111.4 4.1 %expert_weight_grads.1 = (bf16[2,2048,128]{2,1,0:T(8,128)(2,1)}, bf16[2,2048,128]{2,1,0:T(8,128)(2,1)}, bf16[128,2048]{1,0:T(8,128)(2,1)}, bf16[128,2048]{1,0:T(8,128)(2,1)}) custom-call(s32[1]{0:T(128)} %bitcast.chip, bf16[2,4,160,128]{3,2,1,0:T(8,128)(2,1)} %get-tuple-element.33.both, bf16[2,4,160,128]{3,2,1,0:T(8,128)(2,1)} %copy-done.5, ...), custom_call_target="tpu_custom_call" | custom-call | tf_op jit(solution)/shard_map/expert_weight_grads/pallas_call | solution.py:196
  115.5 1.9 %collective-permute-start.9 = (bf16[128,2048]{1,0:T(8,128)(2,1)}, bf16[128,2048]{1,0:T(8,128)(2,1)S(1)}, u32[]{:S(2)}, u32[]{:S(2)}) collective-permute-start(bf16[128,2048]{1,0:T(8,128)(2,1)} %get-tuple-element.43), channel_id=1, source_target_pairs={{0,1},{1,0},{2,3},{3,2},{4,5},{5,4},{6,7},{7,6},{8,9},{9,8},{10,11... | collective-permute-start | bytes 1572872 | tf_op jit(solution)/shard_map/ppermute | solution.py:332
  117.4 2.4 %collective-permute-start.8 = (bf16[2,2048,128]{2,1,0:T(8,128)(2,1)}, bf16[2,2048,128]{2,1,0:T(8,128)(2,1)S(1)}, u32[]{:S(2)}, u32[]{:S(2)}) collective-permute-start(bf16[2,2048,128]{2,1,0:T(8,128)(2,1)} %get-tuple-element.41), channel_id=1, source_target_pairs={{0,1},{1,0},{2,3},{3,2},{4,5},{5,4},{6,7},{7,6},{8,9},{9,8},{10,11... | collective-permute-start | bytes 3145736 | tf_op jit(solution)/shard_map/ppermute | solution.py:332
  121.6 19.3 %all_gather.3.mix = bf16[128,2048]{1,0:T(8,128)(2,1)} all-gather(bf16[128,128]{1,0:T(8,128)(2,1)S(1)} %fusion), channel_id=1, replica_groups=mesh['z'=8,'x'=4,'y'=8,'c'=2] {'y','c'}, dimensions={1}, use_global_device_ids=true | all-gather | bytes 557056 | tf_op jit(solution)/shard_map/all_gather | solution.py:359
  140.8 2.6 %chain_within.1 = (f32[128,128]{1,0:T(8,128)}, f32[128,128]{1,0:T(8,128)}, bf16[32,72,128]{2,1,0:T(8,128)(2,1)}) custom-call(bf16[128,2048]{1,0:T(8,128)(2,1)} %all_gather.3.mix, bf16[128,2048]{1,0:T(8,128)(2,1)} %out_proj.1, bf16[128,128]{1,0:T(8,128)(2,1)} %get-tuple-element.61.rec_state, f32[128,128]{1,0:T(8,128)} %get-tuple-element.60.decay), custom_call_target="tpu_custom_call" | custom-call | tf_op jit(solution)/shard_map/chain_within/pallas_call | solution.py:265
  143.5 9.5 %all-to-all-start.3 = ((bf16[32,72,128]{2,1,0:T(8,128)(2,1)}), bf16[32,72,128]{2,1,0:T(8,128)(2,1)S(1)}, u32[]{:S(2)}, u32[]{:S(2)}) async-start(bf16[32,72,128]{2,1,0:T(8,128)(2,1)} %get-tuple-element.46), calls=%async_computation.3 | async-start | bytes 1179648 | tf_op jit(solution)/shard_map/all_to_all | solution.py:376
  153.0 0.9 fusion.1
  154.6 1.0 fusion.11
  155.7 16.8 %all-to-all-done.3.last = bf16[32,72,128]{2,1,0:T(8,128)(2,1)S(1)} async-done(((bf16[32,72,128]{2,1,0:T(8,128)(2,1)}), bf16[32,72,128]{2,1,0:T(8,128)(2,1)S(1)}, u32[]{:S(2)}, u32[]{:S(2)}) %all-to-all-start.3) | async-done | bytes 589856 | tf_op jit(solution)/shard_map/all_to_all | solution.py:376
  173.3 2.0 %finish.1 = (f32[64,128]{1,0:T(8,128)}, bf16[128,128]{1,0:T(8,128)(2,1)}, bf16[128,128]{1,0:T(8,128)(2,1)}, bf16[128,128]{1,0:T(8,128)(2,1)}) custom-call(s32[1]{0:T(128)} %bitcast.15.here, bf16[32,72,128]{2,1,0:T(8,128)(2,1)} %copy-done.1, f32[128,128]{1,0:T(8,128)} %get-tuple-element.47.local, f32[128,128]{1,0:T(8,128)} %get-tuple-element.48.through, ...), custom_call_target="tpu_custom_call" | custom-call | tf_op jit(solution)/shard_map/finish/pallas_call | solution.py:297
  (61 shorter events, 7.7 us)
Async XLA Ops:
  0.6 17.3 %copy-start.2 = (bf16[1,2048,128]{2,1,0:T(8,128)(2,1)S(1)}, bf16[1,2048,128]{2,1,0:T(8,128)(2,1)}, u32[]{:S(2)}) copy-start(bf16[1,2048,128]{2,1,0:T(8,128)(2,1)} %param.18) | copy-start | bytes 1572868
  0.6 17.3 %copy-start.3 = (bf16[1,2048,128]{2,1,0:T(8,128)(2,1)S(1)}, bf16[1,2048,128]{2,1,0:T(8,128)(2,1)}, u32[]{:S(2)}) copy-start(bf16[1,2048,128]{2,1,0:T(8,128)(2,1)} %param.17) | copy-start | bytes 1572868
  1.5 10.1 %collective-permute-start = (bf16[2,128,128]{2,1,0:T(8,128)(2,1)S(1)}, bf16[2,128,128]{2,1,0:T(8,128)(2,1)S(1)}, u32[]{:S(2)}, u32[]{:S(2)}) collective-permute-start(bf16[2,128,128]{2,1,0:T(8,128)(2,1)S(1)} %get-tuple-element.59), channel_id=1, source_target_pairs={{0,8},{2,10},{4,12},{6,14},{8,0},{10,2},{12,4},{14,6},{1,9},{3,11}... | collective-permute-start | bytes 196616 | tf_op jit(solution)/shard_map/ppermute | solution.py:329
  11.6 3.6 %copy-start.14 = (bf16[2,2,128,128]{3,2,1,0:T(8,128)(2,1)}, bf16[2,2,128,128]{3,2,1,0:T(8,128)(2,1)S(1)}, u32[]{:S(2)}) copy-start(bf16[2,2,128,128]{3,2,1,0:T(8,128)(2,1)S(1)} %pad_maximum_fusion.1.mine) | copy-start | bytes 393220
  11.6 3.6 %collective-permute-start.1 = (bf16[2,2,128,128]{3,2,1,0:T(8,128)(2,1)S(1)}, bf16[2,2,128,128]{3,2,1,0:T(8,128)(2,1)S(1)}, u32[]{:S(2)}, u32[]{:S(2)}) collective-permute-start(bf16[2,2,128,128]{3,2,1,0:T(8,128)(2,1)S(1)} %pad_maximum_fusion.1.mine), channel_id=1, source_target_pairs={{0,1},{1,0},{2,3},{3,2},{4,5},{5,4},{6,7},{7,6},{8,9},{9,8},{10,11... | collective-permute-start | bytes 393224 | tf_op jit(solution)/shard_map/ppermute | solution.py:332
  17.9 15.8 %copy-start.12 = (bf16[1,128,2048]{2,1,0:T(8,128)(2,1)S(1)}, bf16[1,128,2048]{2,1,0:T(8,128)(2,1)}, u32[]{:S(2)}) copy-start(bf16[1,128,2048]{2,1,0:T(8,128)(2,1)} %param.19) | copy-start | bytes 1572868
  18.0 57.2 %collective-permute-start.6 = (bf16[2,2048,128]{2,1,0:T(8,128)(2,1)S(1)}, bf16[2,2048,128]{2,1,0:T(8,128)(2,1)S(1)}, u32[]{:S(2)}, u32[]{:S(2)}) collective-permute-start(bf16[2,2048,128]{2,1,0:T(8,128)(2,1)S(1)} %pad_maximum_fusion), channel_id=1, source_target_pairs={{0,1},{1,0},{2,3},{3,2},{4,5},{5,4},{6,7},{7,6},{8,9},{9,8},{10,11... | collective-permute-start | bytes 3145736 | tf_op jit(solution)/shard_map/ppermute | solution.py:332
  20.6 27.5 %all-to-all-start = ((bf16[32,40,128]{2,1,0:T(8,128)(2,1)}), bf16[32,40,128]{2,1,0:T(8,128)(2,1)S(1)}, u32[]{:S(2)}, u32[]{:S(2)}) async-start(bf16[32,40,128]{2,1,0:T(8,128)(2,1)} %bitcast.8), calls=%async_computation | async-start | bytes 655360 | tf_op jit(solution)/shard_map/all_to_all | solution.py:345
  33.7 30.3 %collective-permute-start.7 = (bf16[128,2048]{1,0:T(8,128)(2,1)S(1)}, bf16[128,2048]{1,0:T(8,128)(2,1)}, u32[]{:S(2)}, u32[]{:S(2)}) collective-permute-start(bf16[128,2048]{1,0:T(8,128)(2,1)S(1)} %bitcast.30), channel_id=1, source_target_pairs={{0,1},{1,0},{2,3},{3,2},{4,5},{5,4},{6,7},{7,6},{8,9},{9,8},{10,11... | collective-permute-start | bytes 1572872 | tf_op jit(solution)/shard_map/ppermute | solution.py:332
  50.7 24.5 %collective-permute-start.3 = (bf16[2,4,160,128]{3,2,1,0:T(8,128)(2,1)}, bf16[2,4,160,128]{3,2,1,0:T(8,128)(2,1)S(1)}, u32[]{:S(2)}, u32[]{:S(2)}) collective-permute-start(bf16[2,4,160,128]{3,2,1,0:T(8,128)(2,1)} %get-tuple-element.33.both), channel_id=1, source_target_pairs={{0,14},{2,0},{4,2},{6,4},{8,6},{10,8},{12,10},{14,12},{1,15},{3,1}... | collective-permute-start | bytes 983048 | tf_op jit(solution)/shard_map/ppermute | solution.py:329
  53.7 21.6 %collective-permute-start.2 = (bf16[2,4,160,128]{3,2,1,0:T(8,128)(2,1)}, bf16[2,4,160,128]{3,2,1,0:T(8,128)(2,1)S(1)}, u32[]{:S(2)}, u32[]{:S(2)}) collective-permute-start(bf16[2,4,160,128]{3,2,1,0:T(8,128)(2,1)} %get-tuple-element.33.both), channel_id=1, source_target_pairs={{0,2},{2,4},{4,6},{6,8},{8,10},{10,12},{12,14},{14,0},{1,3},{3,5},... | collective-permute-start | bytes 983048 | tf_op jit(solution)/shard_map/ppermute | solution.py:329
  57.1 11.7 %collective-permute-start.5 = (bf16[4,160,128]{2,1,0:T(8,128)(2,1)}, bf16[4,160,128]{2,1,0:T(8,128)(2,1)S(1)}, u32[]{:S(2)}, u32[]{:S(2)}) collective-permute-start(bf16[4,160,128]{2,1,0:T(8,128)(2,1)} %get-tuple-element.34), channel_id=1, source_target_pairs={{0,12},{2,14},{4,0},{6,2},{8,4},{10,6},{12,8},{14,10},{1,13},{3,15... | collective-permute-start | bytes 491528 | tf_op jit(solution)/shard_map/ppermute | solution.py:329
  64.0 11.2 %collective-permute-start.4 = (bf16[4,160,128]{2,1,0:T(8,128)(2,1)}, bf16[4,160,128]{2,1,0:T(8,128)(2,1)S(1)}, u32[]{:S(2)}, u32[]{:S(2)}) collective-permute-start(bf16[4,160,128]{2,1,0:T(8,128)(2,1)} %get-tuple-element.34), channel_id=1, source_target_pairs={{0,4},{2,6},{4,8},{6,10},{8,12},{10,14},{12,0},{14,2},{1,5},{3,7},... | collective-permute-start | bytes 491528 | tf_op jit(solution)/shard_map/ppermute | solution.py:329
  68.8 6.4 %copy-start.9 = (bf16[4,160,128]{2,1,0:T(8,128)(2,1)}, bf16[4,160,128]{2,1,0:T(8,128)(2,1)S(1)}, u32[]{:S(2)}) copy-start(bf16[4,160,128]{2,1,0:T(8,128)(2,1)S(1)} %collective-permute-done.5.b2) | copy-start | bytes 491524
  75.2 0.9 copy-start.5
  75.3 1.3 copy-start.8
  81.6 4.3 %copy-start.22 = (f32[128]{0:T(128)S(1)}, f32[128]{0:T(128)}, u32[]{:S(2)}) copy-start(f32[128]{0:T(128)} %param.25) | copy-start | bytes 1540
  81.6 28.9 %copy-start.18 = (bf16[128,128]{1,0:T(8,128)(2,1)S(1)}, bf16[128,128]{1,0:T(8,128)(2,1)}, u32[]{:S(2)}) copy-start(bf16[128,128]{1,0:T(8,128)(2,1)} %param.22) | copy-start | bytes 98308
  81.6 28.9 %copy-start.19 = (bf16[128,128]{1,0:T(8,128)(2,1)S(1)}, bf16[128,128]{1,0:T(8,128)(2,1)}, u32[]{:S(2)}) copy-start(bf16[128,128]{1,0:T(8,128)(2,1)} %param.21) | copy-start | bytes 98308
  81.6 28.9 %copy-start.20 = (bf16[128,128]{1,0:T(8,128)(2,1)S(1)}, bf16[128,128]{1,0:T(8,128)(2,1)}, u32[]{:S(2)}) copy-start(bf16[128,128]{1,0:T(8,128)(2,1)} %param.24) | copy-start | bytes 98308
  81.7 28.9 %copy-start.21 = (bf16[128,128]{1,0:T(8,128)(2,1)S(1)}, bf16[128,128]{1,0:T(8,128)(2,1)}, u32[]{:S(2)}) copy-start(bf16[128,128]{1,0:T(8,128)(2,1)} %param.23) | copy-start | bytes 98308
  81.7 20.8 %all-to-all-start.1 = ((bf16[16,160,128]{2,1,0:T(8,128)(2,1)}), bf16[16,160,128]{2,1,0:T(8,128)(2,1)S(1)}, u32[]{:S(2)}, u32[]{:S(2)}) async-start(bf16[16,160,128]{2,1,0:T(8,128)(2,1)} %bitcast.28), calls=%async_computation.1 | async-start | bytes 1310720 | tf_op jit(solution)/shard_map/all_to_all | solution.py:352
  102.5 0.9 copy-start
  105.4 15.9 %all-to-all-start.2 = ((bf16[32,16,128]{2,1,0:T(8,128)(2,1)}), bf16[32,16,128]{2,1,0:T(8,128)(2,1)S(1)}, u32[]{:S(2)}, u32[]{:S(2)}) async-start(bf16[32,16,128]{2,1,0:T(8,128)(2,1)} %bitcast.32), calls=%async_computation.2 | async-start | bytes 262144 | tf_op jit(solution)/shard_map/all_to_all | solution.py:354
  110.6 10.7 %copy-start.16 = (bf16[512,128]{1,0:T(8,128)(2,1)S(1)}, bf16[512,128]{1,0:T(8,128)(2,1)}, u32[]{:S(2)}) copy-start(bf16[512,128]{1,0:T(8,128)(2,1)} %get-tuple-element.44) | copy-start | bytes 393220
  110.6 10.7 %copy-start.17 = (bf16[128,128]{1,0:T(8,128)(2,1)S(1)}, bf16[128,128]{1,0:T(8,128)(2,1)}, u32[]{:S(2)}) copy-start(bf16[128,128]{1,0:T(8,128)(2,1)} %param.14) | copy-start | bytes 98308
  111.4 10.2 %copy-start.11 = (f32[128,128]{1,0:T(8,128)}, f32[128,128]{1,0:T(8,128)S(1)}, u32[]{:S(2)}) copy-start(f32[128,128]{1,0:T(8,128)S(1)} %get-tuple-element.54.value_by) | copy-start | bytes 196612
  115.5 37.5 %collective-permute-start.9 = (bf16[128,2048]{1,0:T(8,128)(2,1)}, bf16[128,2048]{1,0:T(8,128)(2,1)S(1)}, u32[]{:S(2)}, u32[]{:S(2)}) collective-permute-start(bf16[128,2048]{1,0:T(8,128)(2,1)} %get-tuple-element.43), channel_id=1, source_target_pairs={{0,1},{1,0},{2,3},{3,2},{4,5},{5,4},{6,7},{7,6},{8,9},{9,8},{10,11... | collective-permute-start | bytes 1572872 | tf_op jit(solution)/shard_map/ppermute | solution.py:332
  117.4 36.5 %collective-permute-start.8 = (bf16[2,2048,128]{2,1,0:T(8,128)(2,1)}, bf16[2,2048,128]{2,1,0:T(8,128)(2,1)S(1)}, u32[]{:S(2)}, u32[]{:S(2)}) collective-permute-start(bf16[2,2048,128]{2,1,0:T(8,128)(2,1)} %get-tuple-element.41), channel_id=1, source_target_pairs={{0,1},{1,0},{2,3},{3,2},{4,5},{5,4},{6,7},{7,6},{8,9},{9,8},{10,11... | collective-permute-start | bytes 3145736 | tf_op jit(solution)/shard_map/ppermute | solution.py:332
  140.8 12.1 %copy-start.13 = (bf16[128,2048]{1,0:T(8,128)(2,1)S(1)}, bf16[128,2048]{1,0:T(8,128)(2,1)}, u32[]{:S(2)}) copy-start(bf16[128,2048]{1,0:T(8,128)(2,1)} %get-tuple-element.42) | copy-start | bytes 1572868
  143.5 29.0 %all-to-all-start.3 = ((bf16[32,72,128]{2,1,0:T(8,128)(2,1)}), bf16[32,72,128]{2,1,0:T(8,128)(2,1)S(1)}, u32[]{:S(2)}, u32[]{:S(2)}) async-start(bf16[32,72,128]{2,1,0:T(8,128)(2,1)} %get-tuple-element.46), calls=%async_computation.3 | async-start | bytes 1179648 | tf_op jit(solution)/shard_map/all_to_all | solution.py:376
  152.9 1.4 copy-start.7
  (5 other events, 3.7 us)
where the time goes:
time: 176 us; the launch traced here: 175 us
  starting transfers between devices  64.7 us (37%)
  waiting for transfers between devices  59 us (34%)
  Pallas kernels  21.5 us (12%)
  blocking collectives  19.3 us (11%)
  local copies, waits for them, and re-layouts  5.86 us (3%)
  other arithmetic  3.64 us (2%)
    ppermute x5, starting transfers between devices, over_y(): return lax.ppermute(v, 'y', [(i, (i + step) % n_y) for i in range(n_y)])  22 us
    all_gather x1, blocking collectives, per_device(): mix_grad = lax.all_gather(own_grad, TP, axis=1, tiled=True)  19.3 us
    all_to_all x1, waiting for transfers between devices, per_device(): last = lax.all_to_all(last, SP, 0, 0, tiled=True)  16.8 us
    all_to_all x1, waiting for transfers between devices, per_device(): lax.all_to_all(part.reshape(2 * n_y, *part.shape[2:]), TP, 0, 0, tiled=True)  16.5 us
    all_to_all x1, starting transfers between devices, per_device(): lax.all_to_all(send.reshape(n_sp, -1, fw), SP, 0, 0, tiled=True)  13.2 us
    ppermute x5, waiting for transfers between devices, over_y(): return lax.ppermute(v, 'y', [(i, (i + step) % n_y) for i in range(n_y)])  12.5 us
    all_to_all x1, waiting for transfers between devices, per_device(): lax.all_to_all(send.reshape(n_sp, -1, fw), SP, 0, 0, tiled=True)  12.4 us
    ppermute x5, starting transfers between devices, over_cores(): return lax.ppermute(v, 'c', [(0, 1), (1, 0)])  10.7 us
  transfers between devices with their start and end apart: 14, of which 7 were waited for; matrix products, arithmetic and copies ran while one was open for 2% of the time, Pallas kernels for 6%

commit v1 on v0

--- a/solution.py
+++ b/solution.py
@@ -353,8 +353,10 @@
     back = add_parts(arrived.reshape(part.shape), n_sp, half)
     returned = lax.all_to_all(back.reshape(n_sp, 16, fw), SP, 0, 0, tiled=True).reshape(back.shape)
     dgu, dgu_send, dd, dd_send = expert_weight_grads(chip, blocks, gu_grad, hidden, d)
-    dgu_sum = (dgu.astype(F32) + over_cores(dgu_send).astype(F32)).astype(BF16)
-    d_down = (dd.astype(F32) + over_cores(dd_send).astype(F32)).astype(BF16)
+    dgu_peer = over_cores(dgu_send)
+    dd_peer = over_cores(dd_send)
+    dgu_sum = (dgu.astype(F32) + dgu_peer.astype(F32)).astype(BF16)
+    d_down = (dd.astype(F32) + dd_peer.astype(F32)).astype(BF16)
     own_grad = (dot(pick, returned, ((0,), (0,))) + out_grad.astype(F32)).astype(BF16)
     mix_grad = lax.all_gather(own_grad, TP, axis=1, tiled=True)
 

time: 176 us -> 176 us (level)
  no operation moved by 1% of the time
where the time goes in v1:
time: 176 us; the launch traced here: 175 us
  starting transfers between devices  64.7 us (37%)
  waiting for transfers between devices  59 us (34%)
  Pallas kernels  21.5 us (12%)
  blocking collectives  19.3 us (11%)
  local copies, waits for them, and re-layouts  5.86 us (3%)
  other arithmetic  3.64 us (2%)
    ppermute x5, starting transfers between devices, over_y(): return lax.ppermute(v, 'y', [(i, (i + step) % n_y) for i in range(n_y)])  22 us
    all_gather x1, blocking collectives, per_device(): mix_grad = lax.all_gather(own_grad, TP, axis=1, tiled=True)  19.3 us
    all_to_all x1, waiting for transfers between devices, per_device(): last = lax.all_to_all(last, SP, 0, 0, tiled=True)  16.8 us
    all_to_all x1, waiting for transfers between devices, per_device(): lax.all_to_all(part.reshape(2 * n_y, *part.shape[2:]), TP, 0, 0, tiled=True)  16.5 us
    all_to_all x1, starting transfers between devices, per_device(): lax.all_to_all(send.reshape(n_sp, -1, fw), SP, 0, 0, tiled=True)  13.2 us
    ppermute x5, waiting for transfers between devices, over_y(): return lax.ppermute(v, 'y', [(i, (i + step) % n_y) for i in range(n_y)])  12.5 us
    all_to_all x1, waiting for transfers between devices, per_device(): lax.all_to_all(send.reshape(n_sp, -1, fw), SP, 0, 0, tiled=True)  12.4 us
    ppermute x5, starting transfers between devices, over_cores(): return lax.ppermute(v, 'c', [(0, 1), (1, 0)])  10.7 us
  transfers between devices with their start and end apart: 14, of which 7 were waited for; matrix products, arithmetic and copies ran while one was open for 2% of the time, Pallas kernels for 6%

profile of v1, /device:TPU:8, one launch (start us, length us, event | category | flops | bytes accessed | tf_op | source)
XLA Modules:
  0.0 175.2 jit_solution(12934678302205156756)
XLA Ops:
  0.7 0.9 fusion.9
  1.5 6.8 %collective-permute-start = (bf16[2,128,128]{2,1,0:T(8,128)(2,1)S(1)}, bf16[2,128,128]{2,1,0:T(8,128)(2,1)S(1)}, u32[]{:S(2)}, u32[]{:S(2)}) collective-permute-start(bf16[2,128,128]{2,1,0:T(8,128)(2,1)S(1)} %get-tuple-element.59), channel_id=1, source_target_pairs={{0,8},{2,10},{4,12},{6,14},{8,0},{10,2},{12,4},{14,6},{1,9},{3,11}... | collective-permute-start | bytes 196616 | tf_op jit(solution)/shard_map/ppermute | solution.py:329
  8.4 3.2 %collective-permute-done = bf16[2,128,128]{2,1,0:T(8,128)(2,1)S(1)} collective-permute-done((bf16[2,128,128]{2,1,0:T(8,128)(2,1)S(1)}, bf16[2,128,128]{2,1,0:T(8,128)(2,1)S(1)}, u32[]{:S(2)}, u32[]{:S(2)}) %collective-permute-start) | collective-permute-done | bytes 65568 | tf_op jit(solution)/shard_map/ppermute | solution.py:329
  11.6 1.9 %collective-permute-start.1 = (bf16[2,2,128,128]{3,2,1,0:T(8,128)(2,1)S(1)}, bf16[2,2,128,128]{3,2,1,0:T(8,128)(2,1)S(1)}, u32[]{:S(2)}, u32[]{:S(2)}) collective-permute-start(bf16[2,2,128,128]{3,2,1,0:T(8,128)(2,1)S(1)} %pad_maximum_fusion.1.mine), channel_id=1, source_target_pairs={{0,1},{1,0},{2,3},{3,2},{4,5},{5,4},{6,7},{7,6},{8,9},{9,8},{10,11... | collective-permute-start | bytes 393224 | tf_op jit(solution)/shard_map/ppermute | solution.py:332
  13.6 1.6 route_slots.1
  15.9 2.0 %fill_slots.1 = bf16[1280,128]{1,0:T(8,128)(2,1)} custom-call(s32[1]{0:T(128)} %bitcast.1.core, bf16[160,128]{1,0:T(8,128)(2,1)} %get-tuple-element.30.choose, f32[160,1]{1,0:T(8,128)} %get-tuple-element.31.scale, bf16[2,2,128,128]{3,2,1,0:T(8,128)(2,1)} %copy-done.14, bf16[2,2,128,128]{3,2,1,0:T(8,128)(2,1)} %copy-done.15), custom_call_target="tpu_custom_call" | custom-call | tf_op jit(solution)/shard_map/fill_slots/pallas_call | solution.py:90
  18.0 2.5 %collective-permute-start.6 = (bf16[2,2048,128]{2,1,0:T(8,128)(2,1)S(1)}, bf16[2,2048,128]{2,1,0:T(8,128)(2,1)S(1)}, u32[]{:S(2)}, u32[]{:S(2)}) collective-permute-start(bf16[2,2048,128]{2,1,0:T(8,128)(2,1)S(1)} %pad_maximum_fusion), channel_id=1, source_target_pairs={{0,1},{1,0},{2,3},{3,2},{4,5},{5,4},{6,7},{7,6},{8,9},{9,8},{10,11... | collective-permute-start | bytes 3145736 | tf_op jit(solution)/shard_map/ppermute | solution.py:332
  20.6 13.2 %all-to-all-start = ((bf16[32,40,128]{2,1,0:T(8,128)(2,1)}), bf16[32,40,128]{2,1,0:T(8,128)(2,1)S(1)}, u32[]{:S(2)}, u32[]{:S(2)}) async-start(bf16[32,40,128]{2,1,0:T(8,128)(2,1)} %bitcast.8), calls=%async_computation | async-start | bytes 655360 | tf_op jit(solution)/shard_map/all_to_all | solution.py:345
  33.7 1.9 %collective-permute-start.7 = (bf16[128,2048]{1,0:T(8,128)(2,1)S(1)}, bf16[128,2048]{1,0:T(8,128)(2,1)}, u32[]{:S(2)}, u32[]{:S(2)}) collective-permute-start(bf16[128,2048]{1,0:T(8,128)(2,1)S(1)} %bitcast.30), channel_id=1, source_target_pairs={{0,1},{1,0},{2,3},{3,2},{4,5},{5,4},{6,7},{7,6},{8,9},{9,8},{10,11... | collective-permute-start | bytes 1572872 | tf_op jit(solution)/shard_map/ppermute | solution.py:332
  35.7 12.4 %all-to-all-done = bf16[32,40,128]{2,1,0:T(8,128)(2,1)S(1)} async-done(((bf16[32,40,128]{2,1,0:T(8,128)(2,1)}), bf16[32,40,128]{2,1,0:T(8,128)(2,1)S(1)}, u32[]{:S(2)}, u32[]{:S(2)}) %all-to-all-start) | async-done | bytes 327712 | tf_op jit(solution)/shard_map/all_to_all | solution.py:345
  48.8 1.9 %sort_pieces.1 = (bf16[2,4,160,128]{3,2,1,0:T(8,128)(2,1)}, bf16[4,160,128]{2,1,0:T(8,128)(2,1)}) custom-call(bf16[1280,128]{1,0:T(8,128)(2,1)} %bitcast.27), custom_call_target="tpu_custom_call" | custom-call | tf_op jit(solution)/shard_map/sort_pieces/pallas_call | solution.py:113
  50.7 3.0 %collective-permute-start.3 = (bf16[2,4,160,128]{3,2,1,0:T(8,128)(2,1)}, bf16[2,4,160,128]{3,2,1,0:T(8,128)(2,1)S(1)}, u32[]{:S(2)}, u32[]{:S(2)}) collective-permute-start(bf16[2,4,160,128]{3,2,1,0:T(8,128)(2,1)} %get-tuple-element.33.both), channel_id=1, source_target_pairs={{0,14},{2,0},{4,2},{6,4},{8,6},{10,8},{12,10},{14,12},{1,15},{3,1}... | collective-permute-start | bytes 983048 | tf_op jit(solution)/shard_map/ppermute | solution.py:329
  53.7 3.5 %collective-permute-start.2 = (bf16[2,4,160,128]{3,2,1,0:T(8,128)(2,1)}, bf16[2,4,160,128]{3,2,1,0:T(8,128)(2,1)S(1)}, u32[]{:S(2)}, u32[]{:S(2)}) collective-permute-start(bf16[2,4,160,128]{3,2,1,0:T(8,128)(2,1)} %get-tuple-element.33.both), channel_id=1, source_target_pairs={{0,2},{2,4},{4,6},{6,8},{8,10},{10,12},{12,14},{14,0},{1,3},{3,5},... | collective-permute-start | bytes 983048 | tf_op jit(solution)/shard_map/ppermute | solution.py:329
  57.1 6.9 %collective-permute-start.5 = (bf16[4,160,128]{2,1,0:T(8,128)(2,1)}, bf16[4,160,128]{2,1,0:T(8,128)(2,1)S(1)}, u32[]{:S(2)}, u32[]{:S(2)}) collective-permute-start(bf16[4,160,128]{2,1,0:T(8,128)(2,1)} %get-tuple-element.34), channel_id=1, source_target_pairs={{0,12},{2,14},{4,0},{6,2},{8,4},{10,6},{12,8},{14,10},{1,13},{3,15... | collective-permute-start | bytes 491528 | tf_op jit(solution)/shard_map/ppermute | solution.py:329
  64.0 1.9 %collective-permute-start.4 = (bf16[4,160,128]{2,1,0:T(8,128)(2,1)}, bf16[4,160,128]{2,1,0:T(8,128)(2,1)S(1)}, u32[]{:S(2)}, u32[]{:S(2)}) collective-permute-start(bf16[4,160,128]{2,1,0:T(8,128)(2,1)} %get-tuple-element.34), channel_id=1, source_target_pairs={{0,4},{2,6},{4,8},{6,10},{8,12},{10,14},{12,0},{14,2},{1,5},{3,7},... | collective-permute-start | bytes 491528 | tf_op jit(solution)/shard_map/ppermute | solution.py:329
  65.9 2.9 %collective-permute-done.5.b2 = bf16[4,160,128]{2,1,0:T(8,128)(2,1)S(1)} collective-permute-done((bf16[4,160,128]{2,1,0:T(8,128)(2,1)}, bf16[4,160,128]{2,1,0:T(8,128)(2,1)S(1)}, u32[]{:S(2)}, u32[]{:S(2)}) %collective-permute-start.5) | collective-permute-done | bytes 163872 | tf_op jit(solution)/shard_map/ppermute | solution.py:329
  68.8 6.4 %collective-permute-done.4.f2 = bf16[4,160,128]{2,1,0:T(8,128)(2,1)S(1)} collective-permute-done((bf16[4,160,128]{2,1,0:T(8,128)(2,1)}, bf16[4,160,128]{2,1,0:T(8,128)(2,1)S(1)}, u32[]{:S(2)}, u32[]{:S(2)}) %collective-permute-start.4) | collective-permute-done | bytes 163872 | tf_op jit(solution)/shard_map/ppermute | solution.py:329
  76.5 5.1 %expert_rows_grad.1 = (bf16[160,512]{1,0:T(8,128)(2,1)}, bf16[160,256]{1,0:T(8,128)(2,1)}, bf16[8,2,160,128]{3,2,1,0:T(8,128)(2,1)}) custom-call(s32[1]{0:T(128)} %bitcast.chip, bf16[2,4,160,128]{3,2,1,0:T(8,128)(2,1)} %get-tuple-element.33.both, bf16[2,4,160,128]{3,2,1,0:T(8,128)(2,1)} %copy-done.5, bf16[2,4,160,128]{3,2,1,0:T(8,128)(2,1)} %copy-done.4, ...), custom_call_target="tpu_custom_call" | custom-call | tf_op jit(solution)/shard_map/expert_rows_grad/pallas_call | solution.py:167
  81.7 4.3 %all-to-all-start.1 = ((bf16[16,160,128]{2,1,0:T(8,128)(2,1)}), bf16[16,160,128]{2,1,0:T(8,128)(2,1)S(1)}, u32[]{:S(2)}, u32[]{:S(2)}) async-start(bf16[16,160,128]{2,1,0:T(8,128)(2,1)} %bitcast.28), calls=%async_computation.1 | async-start | bytes 1310720 | tf_op jit(solution)/shard_map/all_to_all | solution.py:352
  86.0 16.5 %all-to-all-done.1 = bf16[16,160,128]{2,1,0:T(8,128)(2,1)S(1)} async-done(((bf16[16,160,128]{2,1,0:T(8,128)(2,1)}), bf16[16,160,128]{2,1,0:T(8,128)(2,1)S(1)}, u32[]{:S(2)}, u32[]{:S(2)}) %all-to-all-start.1) | async-done | bytes 655392 | tf_op jit(solution)/shard_map/all_to_all | solution.py:352
  103.3 2.1 %add_parts.1 = bf16[512,128]{1,0:T(8,128)(2,1)} custom-call(bf16[8,2,160,128]{3,2,1,0:T(8,128)(2,1)} %bitcast.24), custom_call_target="tpu_custom_call" | custom-call | tf_op jit(solution)/shard_map/add_parts/pallas_call | solution.py:220
  105.4 5.1 %all-to-all-start.2 = ((bf16[32,16,128]{2,1,0:T(8,128)(2,1)}), bf16[32,16,128]{2,1,0:T(8,128)(2,1)S(1)}, u32[]{:S(2)}, u32[]{:S(2)}) async-start(bf16[32,16,128]{2,1,0:T(8,128)(2,1)} %bitcast.32), calls=%async_computation.2 | async-start | bytes 262144 | tf_op jit(solution)/shard_map/all_to_all | solution.py:354
  111.4 4.1 %expert_weight_grads.1 = (bf16[2,2048,128]{2,1,0:T(8,128)(2,1)}, bf16[2,2048,128]{2,1,0:T(8,128)(2,1)}, bf16[128,2048]{1,0:T(8,128)(2,1)}, bf16[128,2048]{1,0:T(8,128)(2,1)}) custom-call(s32[1]{0:T(128)} %bitcast.chip, bf16[2,4,160,128]{3,2,1,0:T(8,128)(2,1)} %get-tuple-element.33.both, bf16[2,4,160,128]{3,2,1,0:T(8,128)(2,1)} %copy-done.5, ...), custom_call_target="tpu_custom_call" | custom-call | tf_op jit(solution)/shard_map/expert_weight_grads/pallas_call | solution.py:196
  115.5 1.9 %collective-permute-start.9 = (bf16[128,2048]{1,0:T(8,128)(2,1)}, bf16[128,2048]{1,0:T(8,128)(2,1)S(1)}, u32[]{:S(2)}, u32[]{:S(2)}) collective-permute-start(bf16[128,2048]{1,0:T(8,128)(2,1)} %get-tuple-element.43), channel_id=1, source_target_pairs={{0,1},{1,0},{2,3},{3,2},{4,5},{5,4},{6,7},{7,6},{8,9},{9,8},{10,11... | collective-permute-start | bytes 1572872 | tf_op jit(solution)/shard_map/ppermute | solution.py:332
  117.4 2.4 %collective-permute-start.8 = (bf16[2,2048,128]{2,1,0:T(8,128)(2,1)}, bf16[2,2048,128]{2,1,0:T(8,128)(2,1)S(1)}, u32[]{:S(2)}, u32[]{:S(2)}) collective-permute-start(bf16[2,2048,128]{2,1,0:T(8,128)(2,1)} %get-tuple-element.41), channel_id=1, source_target_pairs={{0,1},{1,0},{2,3},{3,2},{4,5},{5,4},{6,7},{7,6},{8,9},{9,8},{10,11... | collective-permute-start | bytes 3145736 | tf_op jit(solution)/shard_map/ppermute | solution.py:332
  121.6 19.3 %all_gather.3.mix = bf16[128,2048]{1,0:T(8,128)(2,1)} all-gather(bf16[128,128]{1,0:T(8,128)(2,1)S(1)} %fusion), channel_id=1, replica_groups=mesh['z'=8,'x'=4,'y'=8,'c'=2] {'y','c'}, dimensions={1}, use_global_device_ids=true | all-gather | bytes 557056 | tf_op jit(solution)/shard_map/all_gather | solution.py:361
  140.8 2.6 %chain_within.1 = (f32[128,128]{1,0:T(8,128)}, f32[128,128]{1,0:T(8,128)}, bf16[32,72,128]{2,1,0:T(8,128)(2,1)}) custom-call(bf16[128,2048]{1,0:T(8,128)(2,1)} %all_gather.3.mix, bf16[128,2048]{1,0:T(8,128)(2,1)} %out_proj.1, bf16[128,128]{1,0:T(8,128)(2,1)} %get-tuple-element.61.rec_state, f32[128,128]{1,0:T(8,128)} %get-tuple-element.60.decay), custom_call_target="tpu_custom_call" | custom-call | tf_op jit(solution)/shard_map/chain_within/pallas_call | solution.py:265
  143.5 9.5 %all-to-all-start.3 = ((bf16[32,72,128]{2,1,0:T(8,128)(2,1)}), bf16[32,72,128]{2,1,0:T(8,128)(2,1)S(1)}, u32[]{:S(2)}, u32[]{:S(2)}) async-start(bf16[32,72,128]{2,1,0:T(8,128)(2,1)} %get-tuple-element.46), calls=%async_computation.3 | async-start | bytes 1179648 | tf_op jit(solution)/shard_map/all_to_all | solution.py:378
  153.0 0.9 fusion.1
  154.6 1.0 fusion.11
  155.7 16.8 %all-to-all-done.3.last = bf16[32,72,128]{2,1,0:T(8,128)(2,1)S(1)} async-done(((bf16[32,72,128]{2,1,0:T(8,128)(2,1)}), bf16[32,72,128]{2,1,0:T(8,128)(2,1)S(1)}, u32[]{:S(2)}, u32[]{:S(2)}) %all-to-all-start.3) | async-done | bytes 589856 | tf_op jit(solution)/shard_map/all_to_all | solution.py:378
  173.3 2.0 %finish.1 = (f32[64,128]{1,0:T(8,128)}, bf16[128,128]{1,0:T(8,128)(2,1)}, bf16[128,128]{1,0:T(8,128)(2,1)}, bf16[128,128]{1,0:T(8,128)(2,1)}) custom-call(s32[1]{0:T(128)} %bitcast.15.here, bf16[32,72,128]{2,1,0:T(8,128)(2,1)} %copy-done.1, f32[128,128]{1,0:T(8,128)} %get-tuple-element.47.local, f32[128,128]{1,0:T(8,128)} %get-tuple-element.48.through, ...), custom_call_target="tpu_custom_call" | custom-call | tf_op jit(solution)/shard_map/finish/pallas_call | solution.py:297
  (61 shorter events, 7.7 us)
Async XLA Ops:
  0.6 17.3 %copy-start.2 = (bf16[1,2048,128]{2,1,0:T(8,128)(2,1)S(1)}, bf16[1,2048,128]{2,1,0:T(8,128)(2,1)}, u32[]{:S(2)}) copy-start(bf16[1,2048,128]{2,1,0:T(8,128)(2,1)} %param.18) | copy-start | bytes 1572868
  0.6 17.3 %copy-start.3 = (bf16[1,2048,128]{2,1,0:T(8,128)(2,1)S(1)}, bf16[1,2048,128]{2,1,0:T(8,128)(2,1)}, u32[]{:S(2)}) copy-start(bf16[1,2048,128]{2,1,0:T(8,128)(2,1)} %param.17) | copy-start | bytes 1572868
  1.5 10.1 %collective-permute-start = (bf16[2,128,128]{2,1,0:T(8,128)(2,1)S(1)}, bf16[2,128,128]{2,1,0:T(8,128)(2,1)S(1)}, u32[]{:S(2)}, u32[]{:S(2)}) collective-permute-start(bf16[2,128,128]{2,1,0:T(8,128)(2,1)S(1)} %get-tuple-element.59), channel_id=1, source_target_pairs={{0,8},{2,10},{4,12},{6,14},{8,0},{10,2},{12,4},{14,6},{1,9},{3,11}... | collective-permute-start | bytes 196616 | tf_op jit(solution)/shard_map/ppermute | solution.py:329
  11.6 3.6 %copy-start.14 = (bf16[2,2,128,128]{3,2,1,0:T(8,128)(2,1)}, bf16[2,2,128,128]{3,2,1,0:T(8,128)(2,1)S(1)}, u32[]{:S(2)}) copy-start(bf16[2,2,128,128]{3,2,1,0:T(8,128)(2,1)S(1)} %pad_maximum_fusion.1.mine) | copy-start | bytes 393220
  11.6 3.6 %collective-permute-start.1 = (bf16[2,2,128,128]{3,2,1,0:T(8,128)(2,1)S(1)}, bf16[2,2,128,128]{3,2,1,0:T(8,128)(2,1)S(1)}, u32[]{:S(2)}, u32[]{:S(2)}) collective-permute-start(bf16[2,2,128,128]{3,2,1,0:T(8,128)(2,1)S(1)} %pad_maximum_fusion.1.mine), channel_id=1, source_target_pairs={{0,1},{1,0},{2,3},{3,2},{4,5},{5,4},{6,7},{7,6},{8,9},{9,8},{10,11... | collective-permute-start | bytes 393224 | tf_op jit(solution)/shard_map/ppermute | solution.py:332
  17.9 15.8 %copy-start.12 = (bf16[1,128,2048]{2,1,0:T(8,128)(2,1)S(1)}, bf16[1,128,2048]{2,1,0:T(8,128)(2,1)}, u32[]{:S(2)}) copy-start(bf16[1,128,2048]{2,1,0:T(8,128)(2,1)} %param.19) | copy-start | bytes 1572868
  18.0 57.2 %collective-permute-start.6 = (bf16[2,2048,128]{2,1,0:T(8,128)(2,1)S(1)}, bf16[2,2048,128]{2,1,0:T(8,128)(2,1)S(1)}, u32[]{:S(2)}, u32[]{:S(2)}) collective-permute-start(bf16[2,2048,128]{2,1,0:T(8,128)(2,1)S(1)} %pad_maximum_fusion), channel_id=1, source_target_pairs={{0,1},{1,0},{2,3},{3,2},{4,5},{5,4},{6,7},{7,6},{8,9},{9,8},{10,11... | collective-permute-start | bytes 3145736 | tf_op jit(solution)/shard_map/ppermute | solution.py:332
  20.6 27.5 %all-to-all-start = ((bf16[32,40,128]{2,1,0:T(8,128)(2,1)}), bf16[32,40,128]{2,1,0:T(8,128)(2,1)S(1)}, u32[]{:S(2)}, u32[]{:S(2)}) async-start(bf16[32,40,128]{2,1,0:T(8,128)(2,1)} %bitcast.8), calls=%async_computation | async-start | bytes 655360 | tf_op jit(solution)/shard_map/all_to_all | solution.py:345
  33.7 30.3 %collective-permute-start.7 = (bf16[128,2048]{1,0:T(8,128)(2,1)S(1)}, bf16[128,2048]{1,0:T(8,128)(2,1)}, u32[]{:S(2)}, u32[]{:S(2)}) collective-permute-start(bf16[128,2048]{1,0:T(8,128)(2,1)S(1)} %bitcast.30), channel_id=1, source_target_pairs={{0,1},{1,0},{2,3},{3,2},{4,5},{5,4},{6,7},{7,6},{8,9},{9,8},{10,11... | collective-permute-start | bytes 1572872 | tf_op jit(solution)/shard_map/ppermute | solution.py:332
  50.7 24.5 %collective-permute-start.3 = (bf16[2,4,160,128]{3,2,1,0:T(8,128)(2,1)}, bf16[2,4,160,128]{3,2,1,0:T(8,128)(2,1)S(1)}, u32[]{:S(2)}, u32[]{:S(2)}) collective-permute-start(bf16[2,4,160,128]{3,2,1,0:T(8,128)(2,1)} %get-tuple-element.33.both), channel_id=1, source_target_pairs={{0,14},{2,0},{4,2},{6,4},{8,6},{10,8},{12,10},{14,12},{1,15},{3,1}... | collective-permute-start | bytes 983048 | tf_op jit(solution)/shard_map/ppermute | solution.py:329
  53.7 21.6 %collective-permute-start.2 = (bf16[2,4,160,128]{3,2,1,0:T(8,128)(2,1)}, bf16[2,4,160,128]{3,2,1,0:T(8,128)(2,1)S(1)}, u32[]{:S(2)}, u32[]{:S(2)}) collective-permute-start(bf16[2,4,160,128]{3,2,1,0:T(8,128)(2,1)} %get-tuple-element.33.both), channel_id=1, source_target_pairs={{0,2},{2,4},{4,6},{6,8},{8,10},{10,12},{12,14},{14,0},{1,3},{3,5},... | collective-permute-start | bytes 983048 | tf_op jit(solution)/shard_map/ppermute | solution.py:329
  57.1 11.7 %collective-permute-start.5 = (bf16[4,160,128]{2,1,0:T(8,128)(2,1)}, bf16[4,160,128]{2,1,0:T(8,128)(2,1)S(1)}, u32[]{:S(2)}, u32[]{:S(2)}) collective-permute-start(bf16[4,160,128]{2,1,0:T(8,128)(2,1)} %get-tuple-element.34), channel_id=1, source_target_pairs={{0,12},{2,14},{4,0},{6,2},{8,4},{10,6},{12,8},{14,10},{1,13},{3,15... | collective-permute-start | bytes 491528 | tf_op jit(solution)/shard_map/ppermute | solution.py:329
  64.0 11.2 %collective-permute-start.4 = (bf16[4,160,128]{2,1,0:T(8,128)(2,1)}, bf16[4,160,128]{2,1,0:T(8,128)(2,1)S(1)}, u32[]{:S(2)}, u32[]{:S(2)}) collective-permute-start(bf16[4,160,128]{2,1,0:T(8,128)(2,1)} %get-tuple-element.34), channel_id=1, source_target_pairs={{0,4},{2,6},{4,8},{6,10},{8,12},{10,14},{12,0},{14,2},{1,5},{3,7},... | collective-permute-start | bytes 491528 | tf_op jit(solution)/shard_map/ppermute | solution.py:329
  68.8 6.4 %copy-start.9 = (bf16[4,160,128]{2,1,0:T(8,128)(2,1)}, bf16[4,160,128]{2,1,0:T(8,128)(2,1)S(1)}, u32[]{:S(2)}) copy-start(bf16[4,160,128]{2,1,0:T(8,128)(2,1)S(1)} %collective-permute-done.5.b2) | copy-start | bytes 491524
  75.2 0.9 copy-start.5
  75.3 1.3 copy-start.8
  81.6 4.3 %copy-start.22 = (f32[128]{0:T(128)S(1)}, f32[128]{0:T(128)}, u32[]{:S(2)}) copy-start(f32[128]{0:T(128)} %param.25) | copy-start | bytes 1540
  81.6 28.9 %copy-start.18 = (bf16[128,128]{1,0:T(8,128)(2,1)S(1)}, bf16[128,128]{1,0:T(8,128)(2,1)}, u32[]{:S(2)}) copy-start(bf16[128,128]{1,0:T(8,128)(2,1)} %param.22) | copy-start | bytes 98308
  81.6 28.9 %copy-start.19 = (bf16[128,128]{1,0:T(8,128)(2,1)S(1)}, bf16[128,128]{1,0:T(8,128)(2,1)}, u32[]{:S(2)}) copy-start(bf16[128,128]{1,0:T(8,128)(2,1)} %param.21) | copy-start | bytes 98308
  81.6 28.9 %copy-start.20 = (bf16[128,128]{1,0:T(8,128)(2,1)S(1)}, bf16[128,128]{1,0:T(8,128)(2,1)}, u32[]{:S(2)}) copy-start(bf16[128,128]{1,0:T(8,128)(2,1)} %param.24) | copy-start | bytes 98308
  81.7 28.9 %copy-start.21 = (bf16[128,128]{1,0:T(8,128)(2,1)S(1)}, bf16[128,128]{1,0:T(8,128)(2,1)}, u32[]{:S(2)}) copy-start(bf16[128,128]{1,0:T(8,128)(2,1)} %param.23) | copy-start | bytes 98308
  81.7 20.8 %all-to-all-start.1 = ((bf16[16,160,128]{2,1,0:T(8,128)(2,1)}), bf16[16,160,128]{2,1,0:T(8,128)(2,1)S(1)}, u32[]{:S(2)}, u32[]{:S(2)}) async-start(bf16[16,160,128]{2,1,0:T(8,128)(2,1)} %bitcast.28), calls=%async_computation.1 | async-start | bytes 1310720 | tf_op jit(solution)/shard_map/all_to_all | solution.py:352
  102.5 0.9 copy-start
  105.4 15.9 %all-to-all-start.2 = ((bf16[32,16,128]{2,1,0:T(8,128)(2,1)}), bf16[32,16,128]{2,1,0:T(8,128)(2,1)S(1)}, u32[]{:S(2)}, u32[]{:S(2)}) async-start(bf16[32,16,128]{2,1,0:T(8,128)(2,1)} %bitcast.32), calls=%async_computation.2 | async-start | bytes 262144 | tf_op jit(solution)/shard_map/all_to_all | solution.py:354
  110.6 10.7 %copy-start.16 = (bf16[512,128]{1,0:T(8,128)(2,1)S(1)}, bf16[512,128]{1,0:T(8,128)(2,1)}, u32[]{:S(2)}) copy-start(bf16[512,128]{1,0:T(8,128)(2,1)} %get-tuple-element.44) | copy-start | bytes 393220
  110.6 10.7 %copy-start.17 = (bf16[128,128]{1,0:T(8,128)(2,1)S(1)}, bf16[128,128]{1,0:T(8,128)(2,1)}, u32[]{:S(2)}) copy-start(bf16[128,128]{1,0:T(8,128)(2,1)} %param.14) | copy-start | bytes 98308
  111.4 10.2 %copy-start.11 = (f32[128,128]{1,0:T(8,128)}, f32[128,128]{1,0:T(8,128)S(1)}, u32[]{:S(2)}) copy-start(f32[128,128]{1,0:T(8,128)S(1)} %get-tuple-element.54.value_by) | copy-start | bytes 196612
  115.5 37.5 %collective-permute-start.9 = (bf16[128,2048]{1,0:T(8,128)(2,1)}, bf16[128,2048]{1,0:T(8,128)(2,1)S(1)}, u32[]{:S(2)}, u32[]{:S(2)}) collective-permute-start(bf16[128,2048]{1,0:T(8,128)(2,1)} %get-tuple-element.43), channel_id=1, source_target_pairs={{0,1},{1,0},{2,3},{3,2},{4,5},{5,4},{6,7},{7,6},{8,9},{9,8},{10,11... | collective-permute-start | bytes 1572872 | tf_op jit(solution)/shard_map/ppermute | solution.py:332
  117.4 36.5 %collective-permute-start.8 = (bf16[2,2048,128]{2,1,0:T(8,128)(2,1)}, bf16[2,2048,128]{2,1,0:T(8,128)(2,1)S(1)}, u32[]{:S(2)}, u32[]{:S(2)}) collective-permute-start(bf16[2,2048,128]{2,1,0:T(8,128)(2,1)} %get-tuple-element.41), channel_id=1, source_target_pairs={{0,1},{1,0},{2,3},{3,2},{4,5},{5,4},{6,7},{7,6},{8,9},{9,8},{10,11... | collective-permute-start | bytes 3145736 | tf_op jit(solution)/shard_map/ppermute | solution.py:332
  140.8 12.1 %copy-start.13 = (bf16[128,2048]{1,0:T(8,128)(2,1)S(1)}, bf16[128,2048]{1,0:T(8,128)(2,1)}, u32[]{:S(2)}) copy-start(bf16[128,2048]{1,0:T(8,128)(2,1)} %get-tuple-element.42) | copy-start | bytes 1572868
  143.5 29.0 %all-to-all-start.3 = ((bf16[32,72,128]{2,1,0:T(8,128)(2,1)}), bf16[32,72,128]{2,1,0:T(8,128)(2,1)S(1)}, u32[]{:S(2)}, u32[]{:S(2)}) async-start(bf16[32,72,128]{2,1,0:T(8,128)(2,1)} %get-tuple-element.46), calls=%async_computation.3 | async-start | bytes 1179648 | tf_op jit(solution)/shard_map/all_to_all | solution.py:378
  152.9 1.4 copy-start.7
  (5 other events, 3.7 us)

commit v2 on v1

--- a/solution.py
+++ b/solution.py
@@ -20,6 +20,23 @@
 
 def whole(shape, dtype):
     return jax.ShapeDtypeStruct(shape, dtype)
+
+
+def call(body, out, *operands, scalars=0, scratch=(), loose=(), kept=()):
+    held = [
+        o if i < scalars or i in loose else pltpu.with_memory_space_constraint(o, pltpu.VMEM)
+        for i, o in enumerate(operands)
+    ]
+    outs = [(pltpu.VMEM if i in kept else pltpu.HBM)(o.shape, o.dtype) for i, o in enumerate(out)]
+    got = pl.pallas_call(
+        body,
+        out_shape=tuple(outs),
+        in_specs=[SMEM] * scalars + [VMEM] * (len(operands) - scalars),
+        out_specs=tuple([VMEM] * len(outs)),
+        scratch_shapes=list(scratch),
+        compiler_params=pltpu.CompilerParams(vmem_limit_bytes=16 * 2**20),
+    )(*held)
+    return got if len(out) > 1 else got[0]
 
 
 def dot(a, b, dims):
@@ -60,16 +77,9 @@
 
 def route_slots(core, routes, weights, experts, half):
     tokens, slots = routes.shape[1], experts * half
-    return pl.pallas_call(
-        functools.partial(route_body, experts=experts, half=half),
-        out_shape=(
-            whole((experts * 16, tokens), BF16),
-            whole((slots, tokens), BF16),
-            whole((slots, 1), F32),
-        ),
-        in_specs=[SMEM] + [VMEM] * 2,
-        name="route_slots",
-    )(core, routes, weights)
+    out = (whole((experts * 16, tokens), BF16), whole((slots, tokens), BF16), whole((slots, 1), F32))
+    body = functools.partial(route_body, experts=experts, half=half)
+    return call(body, out, core, routes, weights, scalars=1, loose=(1, 2), kept=(1, 2))
 
 
 def fill_body(core, choose, scale, mine, peer, send, rows):
@@ -87,13 +97,9 @@
 def fill_slots(core, choose, scale, mine, peer):
     fw = mine.shape[-1]
     total = choose.shape[0] * 8
-    return pl.pallas_call(
-        fill_body,
-        out_shape=whole((total, fw), BF16),
-        in_specs=[SMEM] + [VMEM] * 4,
-        scratch_shapes=[pltpu.VMEM((total, fw), F32)],
-        name="fill_slots",
-    )(core, choose, scale, mine, peer)
+    out = (whole((total, fw), BF16),)
+    scratch = [pltpu.VMEM((total, fw), F32)]
+    return call(fill_body, out, core, choose, scale, mine, peer, scalars=1, scratch=scratch)
 
 
 def sort_body(recv, both, near, rows):
@@ -110,12 +116,8 @@
 
 def sort_pieces(recv):
     slots, fw = recv.shape[0] // 8, recv.shape[1]
-    return pl.pallas_call(
-        sort_body,
-        out_shape=(whole((2, 4, slots, fw), BF16), whole((4, slots, fw), BF16)),
-        scratch_shapes=[pltpu.VMEM(recv.shape, F32)],
-        name="sort_pieces",
-    )(recv)
+    out = (whole((2, 4, slots, fw), BF16), whole((4, slots, fw), BF16))
+    return call(sort_body, out, recv, scratch=[pltpu.VMEM(recv.shape, F32)], kept=(0, 1))
 
 
 def shards(chip, both, f1, b1, f2, b2, n_y):
@@ -164,16 +166,9 @@
     rows, fw = blocks[0].shape[2:]
     hid = 2 * wg.shape[1]
 
-    return pl.pallas_call(
-        expert_body,
-        out_shape=(
-            whole((rows, 2 * hid), BF16),
-            whole((rows, hid), BF16),
-            whole((n_y, 2, rows, fw), BF16),
-        ),
-        in_specs=[SMEM] + [VMEM] * 10,
-        name="expert_rows_grad",
-    )(chip, *blocks, wgu_peer, wg, wu, wd, wd_peer)
+    out = (whole((rows, 2 * hid), BF16), whole((rows, hid), BF16), whole((n_y, 2, rows, fw), BF16))
+    weights = (wgu_peer, wg, wu, wd, wd_peer)
+    return call(expert_body, out, chip, *blocks, *weights, scalars=1)
 
 
 def weight_body(chip, both, f1, b1, f2, b2, gu_grad, hidden, dgu, dgu_send, dd, dd_send):
@@ -193,12 +188,8 @@
 
 def expert_weight_grads(chip, blocks, gu_grad, hidden, d):
     fw = blocks[0].shape[3]
-    return pl.pallas_call(
-        weight_body,
-        out_shape=(whole((2, d, fw), BF16), whole((2, d, fw), BF16), whole((fw, d), BF16), whole((fw, d), BF16)),
-        in_specs=[SMEM] + [VMEM] * 7,
-        name="expert_weight_grads",
-    )(chip, *blocks, gu_grad, hidden)
+    out = (whole((2, d, fw), BF16),) * 2 + (whole((fw, d), BF16),) * 2
+    return call(weight_body, out, chip, *blocks, gu_grad, hidden, scalars=1, loose=(6, 7))
 
 
 def add_body(parts, out, *, half):
@@ -217,11 +208,8 @@
 
 
 def add_parts(parts, blocks, half):
-    return pl.pallas_call(
-        functools.partial(add_body, half=half),
-        out_shape=whole((blocks * 16, parts.shape[3]), BF16),
-        name="add_parts",
-    )(parts)
+    out = (whole((blocks * 16, parts.shape[3]), BF16),)
+    return call(functools.partial(add_body, half=half), out, parts)
 
 
 def later(v, step, fill):
@@ -262,15 +250,9 @@
 
 def chain_within(mix, out_proj, rec_state, decay, n_sp):
     tokens, width = decay.shape
-    return pl.pallas_call(
-        chain_body,
-        out_shape=(
-            whole((tokens, width), F32),
-            whole((tokens, width), F32),
-            whole((n_sp, mix.shape[1] // n_sp + 8, width), BF16),
-        ),
-        name="chain_within",
-    )(mix, out_proj, rec_state, decay)
+    last = whole((n_sp, mix.shape[1] // n_sp + 8, width), BF16)
+    out = (whole((tokens, width), F32),) * 2 + (last,)
+    return call(chain_body, out, mix, out_proj, rec_state, decay, kept=(0, 1))
 
 
 def finish_body(here, last, local, through, value_by, input_by, rate_by, proj, value, inp, rate):
@@ -294,12 +276,8 @@
 
 def finish(here, last, local, through, value_by, input_by, rate_by):
     grid = whole(local.shape, BF16)
-    return pl.pallas_call(
-        finish_body,
-        out_shape=(whole((last.shape[1] - 8, last.shape[2]), F32), grid, grid, grid),
-        in_specs=[SMEM] + [VMEM] * 6,
-        name="finish",
-    )(here, last, local, through, value_by, input_by, rate_by)
+    out = (whole((last.shape[1] - 8, last.shape[2]), F32), grid, grid, grid)
+    return call(finish_body, out, here, last, local, through, value_by, input_by, rate_by, scalars=1)
 
 
 def per_device(
@@ -347,7 +325,7 @@
     blocks = (both, over_y(both, 1), over_y(both, -1), over_y(near, 2), over_y(near, -2))
 
     gu_grad, hidden, part = expert_rows_grad(
-        chip, blocks, wgu_peer, gate_w[0], up_w[0], down_w[0], wd_peer, n_y
+        chip, blocks, wgu_peer, late_gate[0], late_up[0], late_down[0], wd_peer, n_y
     )
     arrived = lax.all_to_all(part.reshape(2 * n_y, *part.shape[2:]), TP, 0, 0, tiled=True)
     back = add_parts(arrived.reshape(part.shape), n_sp, half)

time: 176 us -> 162 us (0.920)
  Pallas kernels: 21.5 us -> 12.6 us
  local copies, waits for them, and re-layouts: 5.86 us -> 2.46 us
  starting transfers between devices: 64.7 us -> 62 us
  other arithmetic: 3.64 us -> 5.71 us
    pallas_call x8, Pallas kernels: 21.5 us -> 12.6 us  [call(): pl.pallas_call(body, out_shape=tuple(outs), in_specs=[SMEM] * scalars + [...]
    unnamed x46 -> x32, local copies, waits for them, and re-layouts: 4.83 us -> 1.42 us
    all_to_all x1, waiting for transfers between devices: 0.82 us -> 3.44 us  [per_device(): lax.all_to_all(back.reshape(n_sp, 16, fw), SP, 0, 0, tiled=True)]
    all_to_all x1, starting transfers between devices: 9.49 us -> 7.13 us  [per_device(): last = lax.all_to_all(last, SP, 0, 0, tiled=True)]
    all_to_all x1, waiting for transfers between devices: 16.8 us -> 14.9 us  [per_device(): last = lax.all_to_all(last, SP, 0, 0, tiled=True)]
  transfers between devices with their start and end apart: 14 -> 14, of which waited for: 7 -> 7; matrix products, arithmetic and copies ran while one was open for 2% -> 3% of each run, Pallas kernels for 6% -> 4%
where the time goes in v2:
time: 162 us; the launch traced here: 161 us
  starting transfers between devices  62 us (38%)
  waiting for transfers between devices  59.8 us (37%)
  blocking collectives  17.6 us (11%)
  Pallas kernels  12.6 us (8%)
  other arithmetic  5.71 us (4%)
  local copies, waits for them, and re-layouts  2.46 us (2%)
    ppermute x5, starting transfers between devices, over_y(): return lax.ppermute(v, 'y', [(i, (i + step) % n_y) for i in range(n_y)])  22 us
    all_gather x1, blocking collectives, per_device(): mix_grad = lax.all_gather(own_grad, TP, axis=1, tiled=True)  17.6 us
    all_to_all x1, waiting for transfers between devices, per_device(): lax.all_to_all(part.reshape(2 * n_y, *part.shape[2:]), TP, 0, 0, tiled=True)  16.5 us
    all_to_all x1, waiting for transfers between devices, per_device(): last = lax.all_to_all(last, SP, 0, 0, tiled=True)  14.9 us
    all_to_all x1, starting transfers between devices, per_device(): lax.all_to_all(send.reshape(n_sp, -1, fw), SP, 0, 0, tiled=True)  13.2 us
    pallas_call x8, Pallas kernels, call(): pl.pallas_call(body, out_shape=tuple(outs), in_specs=[SMEM] * scalars + [...  12.6 us
    ppermute x5, waiting for transfers between devices, over_y(): return lax.ppermute(v, 'y', [(i, (i + step) % n_y) for i in range(n_y)])  12.5 us
    all_to_all x1, waiting for transfers between devices, per_device(): lax.all_to_all(send.reshape(n_sp, -1, fw), SP, 0, 0, tiled=True)  12.4 us
  transfers between devices with their start and end apart: 14, of which 7 were waited for; matrix products, arithmetic and copies ran while one was open for 3% of the time, Pallas kernels for 4%

profile of v2, /device:TPU:8, one launch (start us, length us, event | category | flops | bytes accessed | tf_op | source)
XLA Modules:
  0.0 161.4 jit_solution(7552296251570499559)
XLA Ops:
  1.5 6.8 %collective-permute-start = (bf16[2,128,128]{2,1,0:T(8,128)(2,1)S(1)}, bf16[2,128,128]{2,1,0:T(8,128)(2,1)S(1)}, u32[]{:S(2)}, u32[]{:S(2)}) collective-permute-start(bf16[2,128,128]{2,1,0:T(8,128)(2,1)S(1)} %get-tuple-element.59), channel_id=1, source_target_pairs={{0,8},{2,10},{4,12},{6,14},{8,0},{10,2},{12,4},{14,6},{1,9},{3,11}... | collective-permute-start | bytes 196616 | tf_op jit(solution)/shard_map/ppermute | solution.py:307
  8.4 3.2 %collective-permute-done = bf16[2,128,128]{2,1,0:T(8,128)(2,1)S(1)} collective-permute-done((bf16[2,128,128]{2,1,0:T(8,128)(2,1)S(1)}, bf16[2,128,128]{2,1,0:T(8,128)(2,1)S(1)}, u32[]{:S(2)}, u32[]{:S(2)}) %collective-permute-start) | collective-permute-done | bytes 65568 | tf_op jit(solution)/shard_map/ppermute | solution.py:307
  11.6 1.9 %collective-permute-start.1 = (bf16[2,2,128,128]{3,2,1,0:T(8,128)(2,1)S(1)}, bf16[2,2,128,128]{3,2,1,0:T(8,128)(2,1)S(1)}, u32[]{:S(2)}, u32[]{:S(2)}) collective-permute-start(bf16[2,2,128,128]{3,2,1,0:T(8,128)(2,1)S(1)} %pad_maximum_fusion.1.mine), channel_id=1, source_target_pairs={{0,1},{1,0},{2,3},{3,2},{4,5},{5,4},{6,7},{7,6},{8,9},{9,8},{10,11... | collective-permute-start | bytes 393224 | tf_op jit(solution)/shard_map/ppermute | solution.py:310
  14.9 0.9 shard_map.180
  15.8 1.0 shard_map.181
  16.8 1.1 pad_maximum_fusion
  17.9 2.4 %collective-permute-start.6 = (bf16[2,2048,128]{2,1,0:T(8,128)(2,1)}, bf16[2,2048,128]{2,1,0:T(8,128)(2,1)S(1)}, u32[]{:S(2)}, u32[]{:S(2)}) collective-permute-start(bf16[2,2048,128]{2,1,0:T(8,128)(2,1)} %pad_maximum_fusion), channel_id=1, source_target_pairs={{0,1},{1,0},{2,3},{3,2},{4,5},{5,4},{6,7},{7,6},{8,9},{9,8},{10,11... | collective-permute-start | bytes 3145736 | tf_op jit(solution)/shard_map/ppermute | solution.py:310
  20.3 13.2 %all-to-all-start = ((bf16[32,40,128]{2,1,0:T(8,128)(2,1)}), bf16[32,40,128]{2,1,0:T(8,128)(2,1)S(1)}, u32[]{:S(2)}, u32[]{:S(2)}) async-start(bf16[32,40,128]{2,1,0:T(8,128)(2,1)} %bitcast.8), calls=%async_computation | async-start | bytes 655360 | tf_op jit(solution)/shard_map/all_to_all | solution.py:323
  33.5 1.9 %collective-permute-start.7 = (bf16[128,2048]{1,0:T(8,128)(2,1)}, bf16[128,2048]{1,0:T(8,128)(2,1)}, u32[]{:S(2)}, u32[]{:S(2)}) collective-permute-start(bf16[128,2048]{1,0:T(8,128)(2,1)} %bitcast.12.wd), channel_id=1, source_target_pairs={{0,1},{1,0},{2,3},{3,2},{4,5},{5,4},{6,7},{7,6},{8,9},{9,8},{10,11... | collective-permute-start | bytes 1572872 | tf_op jit(solution)/shard_map/ppermute | solution.py:310
  35.4 12.4 %all-to-all-done = bf16[32,40,128]{2,1,0:T(8,128)(2,1)S(1)} async-done(((bf16[32,40,128]{2,1,0:T(8,128)(2,1)}), bf16[32,40,128]{2,1,0:T(8,128)(2,1)S(1)}, u32[]{:S(2)}, u32[]{:S(2)}) %all-to-all-start) | async-done | bytes 327712 | tf_op jit(solution)/shard_map/all_to_all | solution.py:323
  48.6 3.0 %collective-permute-start.3 = (bf16[2,4,160,128]{3,2,1,0:T(8,128)(2,1)S(1)}, bf16[2,4,160,128]{3,2,1,0:T(8,128)(2,1)S(1)}, u32[]{:S(2)}, u32[]{:S(2)}) collective-permute-start(bf16[2,4,160,128]{3,2,1,0:T(8,128)(2,1)S(1)} %get-tuple-element.33.both), channel_id=1, source_target_pairs={{0,14},{2,0},{4,2},{6,4},{8,6},{10,8},{12,10},{14,12},{1,15},{3,1}... | collective-permute-start | bytes 983048 | tf_op jit(solution)/shard_map/ppermute | solution.py:307
  51.6 3.5 %collective-permute-start.2 = (bf16[2,4,160,128]{3,2,1,0:T(8,128)(2,1)S(1)}, bf16[2,4,160,128]{3,2,1,0:T(8,128)(2,1)S(1)}, u32[]{:S(2)}, u32[]{:S(2)}) collective-permute-start(bf16[2,4,160,128]{3,2,1,0:T(8,128)(2,1)S(1)} %get-tuple-element.33.both), channel_id=1, source_target_pairs={{0,2},{2,4},{4,6},{6,8},{8,10},{10,12},{12,14},{14,0},{1,3},{3,5},... | collective-permute-start | bytes 983048 | tf_op jit(solution)/shard_map/ppermute | solution.py:307
  55.1 6.9 %collective-permute-start.5 = (bf16[4,160,128]{2,1,0:T(8,128)(2,1)}, bf16[4,160,128]{2,1,0:T(8,128)(2,1)S(1)}, u32[]{:S(2)}, u32[]{:S(2)}) collective-permute-start(bf16[4,160,128]{2,1,0:T(8,128)(2,1)} %get-tuple-element.34), channel_id=1, source_target_pairs={{0,12},{2,14},{4,0},{6,2},{8,4},{10,6},{12,8},{14,10},{1,13},{3,15... | collective-permute-start | bytes 491528 | tf_op jit(solution)/shard_map/ppermute | solution.py:307
  62.0 1.9 %collective-permute-start.4 = (bf16[4,160,128]{2,1,0:T(8,128)(2,1)}, bf16[4,160,128]{2,1,0:T(8,128)(2,1)S(1)}, u32[]{:S(2)}, u32[]{:S(2)}) collective-permute-start(bf16[4,160,128]{2,1,0:T(8,128)(2,1)} %get-tuple-element.34), channel_id=1, source_target_pairs={{0,4},{2,6},{4,8},{6,10},{8,12},{10,14},{12,0},{14,2},{1,5},{3,7},... | collective-permute-start | bytes 491528 | tf_op jit(solution)/shard_map/ppermute | solution.py:307
  63.9 2.5 %collective-permute-done.5.b2 = bf16[4,160,128]{2,1,0:T(8,128)(2,1)S(1)} collective-permute-done((bf16[4,160,128]{2,1,0:T(8,128)(2,1)}, bf16[4,160,128]{2,1,0:T(8,128)(2,1)S(1)}, u32[]{:S(2)}, u32[]{:S(2)}) %collective-permute-start.5) | collective-permute-done | bytes 163872 | tf_op jit(solution)/shard_map/ppermute | solution.py:307
  66.4 6.8 %collective-permute-done.4.f2 = bf16[4,160,128]{2,1,0:T(8,128)(2,1)S(1)} collective-permute-done((bf16[4,160,128]{2,1,0:T(8,128)(2,1)}, bf16[4,160,128]{2,1,0:T(8,128)(2,1)S(1)}, u32[]{:S(2)}, u32[]{:S(2)}) %collective-permute-start.4) | collective-permute-done | bytes 163872 | tf_op jit(solution)/shard_map/ppermute | solution.py:307
  73.2 4.1 %shard_map.183 = (bf16[160,512]{1,0:T(8,128)(2,1)}, bf16[160,256]{1,0:T(8,128)(2,1)}, bf16[8,2,160,128]{3,2,1,0:T(8,128)(2,1)}) custom-call(s32[1]{0:T(128)} %bitcast.chip, bf16[2,4,160,128]{3,2,1,0:T(8,128)(2,1)S(1)} %get-tuple-element.33.both, bf16[2,4,160,128]{3,2,1,0:T(8,128)(2,1)S(1)} %collective-permute-done.2.f1, ...), custom_call_target="tpu_custom_call" | custom-call | tf_op jit(solution)/shard_map/pallas_call | solution.py:31
  77.3 4.1 %all-to-all-start.1 = ((bf16[16,160,128]{2,1,0:T(8,128)(2,1)}), bf16[16,160,128]{2,1,0:T(8,128)(2,1)S(1)}, u32[]{:S(2)}, u32[]{:S(2)}) async-start(bf16[16,160,128]{2,1,0:T(8,128)(2,1)} %bitcast.29), calls=%async_computation.1 | async-start | bytes 1310720 | tf_op jit(solution)/shard_map/all_to_all | solution.py:330
  81.4 16.5 %all-to-all-done.1 = bf16[16,160,128]{2,1,0:T(8,128)(2,1)S(1)} async-done(((bf16[16,160,128]{2,1,0:T(8,128)(2,1)}), bf16[16,160,128]{2,1,0:T(8,128)(2,1)S(1)}, u32[]{:S(2)}, u32[]{:S(2)}) %all-to-all-start.1) | async-done | bytes 655392 | tf_op jit(solution)/shard_map/all_to_all | solution.py:330
  97.9 1.0 shard_map.185
  98.9 5.1 %all-to-all-start.2 = ((bf16[32,16,128]{2,1,0:T(8,128)(2,1)}), bf16[32,16,128]{2,1,0:T(8,128)(2,1)S(1)}, u32[]{:S(2)}, u32[]{:S(2)}) async-start(bf16[32,16,128]{2,1,0:T(8,128)(2,1)} %bitcast.31), calls=%async_computation.2 | async-start | bytes 262144 | tf_op jit(solution)/shard_map/all_to_all | solution.py:332
  104.3 2.7 %shard_map.184 = (bf16[2,2048,128]{2,1,0:T(8,128)(2,1)}, bf16[2,2048,128]{2,1,0:T(8,128)(2,1)}, bf16[128,2048]{1,0:T(8,128)(2,1)}, bf16[128,2048]{1,0:T(8,128)(2,1)}) custom-call(s32[1]{0:T(128)} %bitcast.chip, bf16[2,4,160,128]{3,2,1,0:T(8,128)(2,1)S(1)} %get-tuple-element.33.both, bf16[2,4,160,128]{3,2,1,0:T(8,128)(2,1)S(1)} %collective-permute-done.2.f1, ...), custom_call_target="tpu_custom_call" | custom-call | tf_op jit(solution)/shard_map/pallas_call | solution.py:31
  107.0 1.9 %collective-permute-start.9 = (bf16[128,2048]{1,0:T(8,128)(2,1)}, bf16[128,2048]{1,0:T(8,128)(2,1)}, u32[]{:S(2)}, u32[]{:S(2)}) collective-permute-start(bf16[128,2048]{1,0:T(8,128)(2,1)} %get-tuple-element.43), channel_id=1, source_target_pairs={{0,1},{1,0},{2,3},{3,2},{4,5},{5,4},{6,7},{7,6},{8,9},{9,8},{10,11... | collective-permute-start | bytes 1572872 | tf_op jit(solution)/shard_map/ppermute | solution.py:310
  108.9 2.4 %collective-permute-start.8 = (bf16[2,2048,128]{2,1,0:T(8,128)(2,1)}, bf16[2,2048,128]{2,1,0:T(8,128)(2,1)}, u32[]{:S(2)}, u32[]{:S(2)}) collective-permute-start(bf16[2,2048,128]{2,1,0:T(8,128)(2,1)} %get-tuple-element.41), channel_id=1, source_target_pairs={{0,1},{1,0},{2,3},{3,2},{4,5},{5,4},{6,7},{7,6},{8,9},{9,8},{10,11... | collective-permute-start | bytes 3145736 | tf_op jit(solution)/shard_map/ppermute | solution.py:310
  111.4 3.4 %all-to-all-done.2 = bf16[32,16,128]{2,1,0:T(8,128)(2,1)S(1)} async-done(((bf16[32,16,128]{2,1,0:T(8,128)(2,1)}), bf16[32,16,128]{2,1,0:T(8,128)(2,1)S(1)}, u32[]{:S(2)}, u32[]{:S(2)}) %all-to-all-start.2) | async-done | bytes 131104 | tf_op jit(solution)/shard_map/all_to_all | solution.py:332
  115.0 17.6 %all_gather.3.mix = bf16[128,2048]{1,0:T(8,128)(2,1)S(1)} all-gather(bf16[128,128]{1,0:T(8,128)(2,1)S(1)} %fusion), channel_id=1, replica_groups=mesh['z'=8,'x'=4,'y'=8,'c'=2] {'y','c'}, dimensions={1}, use_global_device_ids=true | all-gather | bytes 557056 | tf_op jit(solution)/shard_map/all_gather | solution.py:339
  132.7 1.3 shard_map.186
  134.0 7.1 %all-to-all-start.3 = ((bf16[32,72,128]{2,1,0:T(8,128)(2,1)}), bf16[32,72,128]{2,1,0:T(8,128)(2,1)S(1)}, u32[]{:S(2)}, u32[]{:S(2)}) async-start(bf16[32,72,128]{2,1,0:T(8,128)(2,1)} %get-tuple-element.46), calls=%async_computation.3 | async-start | bytes 1179648 | tf_op jit(solution)/shard_map/all_to_all | solution.py:356
  141.2 2.0 %fusion.1 = bf16[1,128,2048]{2,1,0:T(8,128)(2,1)} fusion(bf16[128,2048]{1,0:T(8,128)(2,1)} %collective-permute-done.9, bf16[128,2048]{1,0:T(8,128)(2,1)S(1)} %copy-done.8), kind=kLoop, calls=%fused_computation.5 | loop fusion | flops 1048576 | bytes 1572864 | tf_op jit(solution)/shard_map/broadcast_in_dim | solution.py:364
  143.2 1.5 add_convert_fusion
  144.7 1.0 fusion.11
  145.8 14.9 %all-to-all-done.3.last = bf16[32,72,128]{2,1,0:T(8,128)(2,1)S(1)} async-done(((bf16[32,72,128]{2,1,0:T(8,128)(2,1)}), bf16[32,72,128]{2,1,0:T(8,128)(2,1)S(1)}, u32[]{:S(2)}, u32[]{:S(2)}) %all-to-all-start.3) | async-done | bytes 589856 | tf_op jit(solution)/shard_map/all_to_all | solution.py:356
  (47 shorter events, 4.4 us)
Async XLA Ops:
  0.6 16.2 %copy-start = (bf16[1,2048,128]{2,1,0:T(8,128)(2,1)S(1)}, bf16[1,2048,128]{2,1,0:T(8,128)(2,1)}, u32[]{:S(2)}) copy-start(bf16[1,2048,128]{2,1,0:T(8,128)(2,1)} %param.18) | copy-start | bytes 1572868
  0.6 16.2 %copy-start.1 = (bf16[1,2048,128]{2,1,0:T(8,128)(2,1)S(1)}, bf16[1,2048,128]{2,1,0:T(8,128)(2,1)}, u32[]{:S(2)}) copy-start(bf16[1,2048,128]{2,1,0:T(8,128)(2,1)} %param.17) | copy-start | bytes 1572868
  1.5 10.1 %collective-permute-start = (bf16[2,128,128]{2,1,0:T(8,128)(2,1)S(1)}, bf16[2,128,128]{2,1,0:T(8,128)(2,1)S(1)}, u32[]{:S(2)}, u32[]{:S(2)}) collective-permute-start(bf16[2,128,128]{2,1,0:T(8,128)(2,1)S(1)} %get-tuple-element.59), channel_id=1, source_target_pairs={{0,8},{2,10},{4,12},{6,14},{8,0},{10,2},{12,4},{14,6},{1,9},{3,11}... | collective-permute-start | bytes 196616 | tf_op jit(solution)/shard_map/ppermute | solution.py:307
  11.6 4.2 %collective-permute-start.1 = (bf16[2,2,128,128]{3,2,1,0:T(8,128)(2,1)S(1)}, bf16[2,2,128,128]{3,2,1,0:T(8,128)(2,1)S(1)}, u32[]{:S(2)}, u32[]{:S(2)}) collective-permute-start(bf16[2,2,128,128]{3,2,1,0:T(8,128)(2,1)S(1)} %pad_maximum_fusion.1.mine), channel_id=1, source_target_pairs={{0,1},{1,0},{2,3},{3,2},{4,5},{5,4},{6,7},{7,6},{8,9},{9,8},{10,11... | collective-permute-start | bytes 393224 | tf_op jit(solution)/shard_map/ppermute | solution.py:310
  13.5 0.7 copy-start.5
  14.2 0.7 copy-start.6
  17.9 55.3 %collective-permute-start.6 = (bf16[2,2048,128]{2,1,0:T(8,128)(2,1)}, bf16[2,2048,128]{2,1,0:T(8,128)(2,1)S(1)}, u32[]{:S(2)}, u32[]{:S(2)}) collective-permute-start(bf16[2,2048,128]{2,1,0:T(8,128)(2,1)} %pad_maximum_fusion), channel_id=1, source_target_pairs={{0,1},{1,0},{2,3},{3,2},{4,5},{5,4},{6,7},{7,6},{8,9},{9,8},{10,11... | collective-permute-start | bytes 3145736 | tf_op jit(solution)/shard_map/ppermute | solution.py:310
  20.3 27.6 %all-to-all-start = ((bf16[32,40,128]{2,1,0:T(8,128)(2,1)}), bf16[32,40,128]{2,1,0:T(8,128)(2,1)S(1)}, u32[]{:S(2)}, u32[]{:S(2)}) async-start(bf16[32,40,128]{2,1,0:T(8,128)(2,1)} %bitcast.8), calls=%async_computation | async-start | bytes 655360 | tf_op jit(solution)/shard_map/all_to_all | solution.py:323
  33.5 28.5 %collective-permute-start.7 = (bf16[128,2048]{1,0:T(8,128)(2,1)}, bf16[128,2048]{1,0:T(8,128)(2,1)}, u32[]{:S(2)}, u32[]{:S(2)}) collective-permute-start(bf16[128,2048]{1,0:T(8,128)(2,1)} %bitcast.12.wd), channel_id=1, source_target_pairs={{0,1},{1,0},{2,3},{3,2},{4,5},{5,4},{6,7},{7,6},{8,9},{9,8},{10,11... | collective-permute-start | bytes 1572872 | tf_op jit(solution)/shard_map/ppermute | solution.py:310
  48.6 24.5 %collective-permute-start.3 = (bf16[2,4,160,128]{3,2,1,0:T(8,128)(2,1)S(1)}, bf16[2,4,160,128]{3,2,1,0:T(8,128)(2,1)S(1)}, u32[]{:S(2)}, u32[]{:S(2)}) collective-permute-start(bf16[2,4,160,128]{3,2,1,0:T(8,128)(2,1)S(1)} %get-tuple-element.33.both), channel_id=1, source_target_pairs={{0,14},{2,0},{4,2},{6,4},{8,6},{10,8},{12,10},{14,12},{1,15},{3,1}... | collective-permute-start | bytes 983048 | tf_op jit(solution)/shard_map/ppermute | solution.py:307
  51.6 21.6 %collective-permute-start.2 = (bf16[2,4,160,128]{3,2,1,0:T(8,128)(2,1)S(1)}, bf16[2,4,160,128]{3,2,1,0:T(8,128)(2,1)S(1)}, u32[]{:S(2)}, u32[]{:S(2)}) collective-permute-start(bf16[2,4,160,128]{3,2,1,0:T(8,128)(2,1)S(1)} %get-tuple-element.33.both), channel_id=1, source_target_pairs={{0,2},{2,4},{4,6},{6,8},{8,10},{10,12},{12,14},{14,0},{1,3},{3,5},... | collective-permute-start | bytes 983048 | tf_op jit(solution)/shard_map/ppermute | solution.py:307
  55.1 11.3 %collective-permute-start.5 = (bf16[4,160,128]{2,1,0:T(8,128)(2,1)}, bf16[4,160,128]{2,1,0:T(8,128)(2,1)S(1)}, u32[]{:S(2)}, u32[]{:S(2)}) collective-permute-start(bf16[4,160,128]{2,1,0:T(8,128)(2,1)} %get-tuple-element.34), channel_id=1, source_target_pairs={{0,12},{2,14},{4,0},{6,2},{8,4},{10,6},{12,8},{14,10},{1,13},{3,15... | collective-permute-start | bytes 491528 | tf_op jit(solution)/shard_map/ppermute | solution.py:307
  62.0 11.2 %collective-permute-start.4 = (bf16[4,160,128]{2,1,0:T(8,128)(2,1)}, bf16[4,160,128]{2,1,0:T(8,128)(2,1)S(1)}, u32[]{:S(2)}, u32[]{:S(2)}) collective-permute-start(bf16[4,160,128]{2,1,0:T(8,128)(2,1)} %get-tuple-element.34), channel_id=1, source_target_pairs={{0,4},{2,6},{4,8},{6,10},{8,12},{10,14},{12,0},{14,2},{1,5},{3,7},... | collective-permute-start | bytes 491528 | tf_op jit(solution)/shard_map/ppermute | solution.py:307
  77.3 4.1 %copy-start.15 = (f32[128]{0:T(128)S(1)}, f32[128]{0:T(128)}, u32[]{:S(2)}) copy-start(f32[128]{0:T(128)} %param.25) | copy-start | bytes 1540
  77.3 26.8 %copy-start.11 = (bf16[128,128]{1,0:T(8,128)(2,1)S(1)}, bf16[128,128]{1,0:T(8,128)(2,1)}, u32[]{:S(2)}) copy-start(bf16[128,128]{1,0:T(8,128)(2,1)} %param.22) | copy-start | bytes 98308
  77.3 26.8 %copy-start.12 = (bf16[128,128]{1,0:T(8,128)(2,1)S(1)}, bf16[128,128]{1,0:T(8,128)(2,1)}, u32[]{:S(2)}) copy-start(bf16[128,128]{1,0:T(8,128)(2,1)} %param.21) | copy-start | bytes 98308
  77.3 26.8 %copy-start.13 = (bf16[128,128]{1,0:T(8,128)(2,1)S(1)}, bf16[128,128]{1,0:T(8,128)(2,1)}, u32[]{:S(2)}) copy-start(bf16[128,128]{1,0:T(8,128)(2,1)} %param.24) | copy-start | bytes 98308
  77.3 26.8 %copy-start.14 = (bf16[128,128]{1,0:T(8,128)(2,1)S(1)}, bf16[128,128]{1,0:T(8,128)(2,1)}, u32[]{:S(2)}) copy-start(bf16[128,128]{1,0:T(8,128)(2,1)} %param.23) | copy-start | bytes 98308
  77.3 27.0 %copy-start.3 = (bf16[160,512]{1,0:T(8,128)(2,1)S(1)}, bf16[160,512]{1,0:T(8,128)(2,1)}, u32[]{:S(2)}) copy-start(bf16[160,512]{1,0:T(8,128)(2,1)} %get-tuple-element.38.gu_grad) | copy-start | bytes 491524
  77.3 27.0 %copy-start.4 = (bf16[160,256]{1,0:T(8,128)(2,1)S(1)}, bf16[160,256]{1,0:T(8,128)(2,1)}, u32[]{:S(2)}) copy-start(bf16[160,256]{1,0:T(8,128)(2,1)} %get-tuple-element.39.hidden) | copy-start | bytes 245764
  77.3 20.6 %all-to-all-start.1 = ((bf16[16,160,128]{2,1,0:T(8,128)(2,1)}), bf16[16,160,128]{2,1,0:T(8,128)(2,1)S(1)}, u32[]{:S(2)}, u32[]{:S(2)}) async-start(bf16[16,160,128]{2,1,0:T(8,128)(2,1)} %bitcast.29), calls=%async_computation.1 | async-start | bytes 1310720 | tf_op jit(solution)/shard_map/all_to_all | solution.py:330
  98.9 15.9 %all-to-all-start.2 = ((bf16[32,16,128]{2,1,0:T(8,128)(2,1)}), bf16[32,16,128]{2,1,0:T(8,128)(2,1)S(1)}, u32[]{:S(2)}, u32[]{:S(2)}) async-start(bf16[32,16,128]{2,1,0:T(8,128)(2,1)} %bitcast.31), calls=%async_computation.2 | async-start | bytes 262144 | tf_op jit(solution)/shard_map/all_to_all | solution.py:332
  104.1 10.7 %copy-start.9 = (bf16[512,128]{1,0:T(8,128)(2,1)S(1)}, bf16[512,128]{1,0:T(8,128)(2,1)}, u32[]{:S(2)}) copy-start(bf16[512,128]{1,0:T(8,128)(2,1)} %get-tuple-element.44) | copy-start | bytes 393220
  104.1 10.7 %copy-start.10 = (bf16[128,128]{1,0:T(8,128)(2,1)S(1)}, bf16[128,128]{1,0:T(8,128)(2,1)}, u32[]{:S(2)}) copy-start(bf16[128,128]{1,0:T(8,128)(2,1)} %param.14) | copy-start | bytes 98308
  104.3 28.4 %copy-start.2 = (bf16[128,2048]{1,0:T(8,128)(2,1)S(1)}, bf16[128,2048]{1,0:T(8,128)(2,1)}, u32[]{:S(2)}) copy-start(bf16[128,2048]{1,0:T(8,128)(2,1)} %out_proj.1) | copy-start | bytes 1572868
  107.0 34.2 %collective-permute-start.9 = (bf16[128,2048]{1,0:T(8,128)(2,1)}, bf16[128,2048]{1,0:T(8,128)(2,1)}, u32[]{:S(2)}, u32[]{:S(2)}) collective-permute-start(bf16[128,2048]{1,0:T(8,128)(2,1)} %get-tuple-element.43), channel_id=1, source_target_pairs={{0,1},{1,0},{2,3},{3,2},{4,5},{5,4},{6,7},{7,6},{8,9},{9,8},{10,11... | collective-permute-start | bytes 1572872 | tf_op jit(solution)/shard_map/ppermute | solution.py:310
  108.9 34.3 %collective-permute-start.8 = (bf16[2,2048,128]{2,1,0:T(8,128)(2,1)}, bf16[2,2048,128]{2,1,0:T(8,128)(2,1)}, u32[]{:S(2)}, u32[]{:S(2)}) collective-permute-start(bf16[2,2048,128]{2,1,0:T(8,128)(2,1)} %get-tuple-element.41), channel_id=1, source_target_pairs={{0,1},{1,0},{2,3},{3,2},{4,5},{5,4},{6,7},{7,6},{8,9},{9,8},{10,11... | collective-permute-start | bytes 3145736 | tf_op jit(solution)/shard_map/ppermute | solution.py:310
  132.7 8.5 %copy-start.8 = (bf16[128,2048]{1,0:T(8,128)(2,1)S(1)}, bf16[128,2048]{1,0:T(8,128)(2,1)}, u32[]{:S(2)}) copy-start(bf16[128,2048]{1,0:T(8,128)(2,1)} %get-tuple-element.42) | copy-start | bytes 1572868
  134.0 26.6 %all-to-all-start.3 = ((bf16[32,72,128]{2,1,0:T(8,128)(2,1)}), bf16[32,72,128]{2,1,0:T(8,128)(2,1)S(1)}, u32[]{:S(2)}, u32[]{:S(2)}) async-start(bf16[32,72,128]{2,1,0:T(8,128)(2,1)} %get-tuple-element.46), calls=%async_computation.3 | async-start | bytes 1179648 | tf_op jit(solution)/shard_map/all_to_all | solution.py:356
  141.1 2.1 %copy-start.7 = (bf16[2,2048,128]{2,1,0:T(8,128)(2,1)S(1)}, bf16[2,2048,128]{2,1,0:T(8,128)(2,1)}, u32[]{:S(2)}) copy-start(bf16[2,2048,128]{2,1,0:T(8,128)(2,1)} %get-tuple-element.40) | copy-start | bytes 3145732

commit v3 on v2

--- a/solution.py
+++ b/solution.py
@@ -50,7 +50,7 @@
 def route_body(core, routes, weights, pick, choose, scale, *, experts, half):
     me = core[0]
     count, tokens = routes.shape
-    slots = experts * half
+    slots = experts * (half + 1)
     here = [iota((experts, tokens), 0) == routes[k : k + 1, :] for k in range(count)]
     named = functools.reduce(jnp.logical_or, here)
     earlier = iota((tokens, tokens), 0) < iota((tokens, tokens), 1)
@@ -63,7 +63,7 @@
         name = routes[k : k + 1, :]
         back.append(name * 16 + rank + jnp.where(rank >= half, 8 - half, 0))
         at = rank - me * half
-        mine.append(jnp.where((at >= 0) & (at < half), name * half + at, -1))
+        mine.append(jnp.where((at >= 0) & (at < half), name * (half + 1) + at, -1))
     hit = functools.reduce(jnp.logical_or, [iota(pick.shape, 0) == b for b in back])
     pick[...] = jnp.where(hit, 1.0, 0.0).astype(BF16)
     row = iota((slots, tokens), 0)
@@ -76,63 +76,59 @@
 
 
 def route_slots(core, routes, weights, experts, half):
-    tokens, slots = routes.shape[1], experts * half
+    tokens, slots = routes.shape[1], experts * (half + 1)
     out = (whole((experts * 16, tokens), BF16), whole((slots, tokens), BF16), whole((slots, 1), F32))
     body = functools.partial(route_body, experts=experts, half=half)
     return call(body, out, core, routes, weights, scalars=1, loose=(1, 2), kept=(1, 2))
 
 
 def fill_body(core, choose, scale, mine, peer, send, rows):
-    me = core[0]
     slots = choose.shape[0]
     for a in range(2):
-        for n in range(2):
-            for c in range(2):
-                x = jnp.where(me == c, mine[n, a], peer[n, a])
-                r = dot(choose[...], x, ((1,), (0,)))
-                rows[pl.ds(4 * a + 2 * n + c, slots, stride=8), :] = scale[...] * r if a else r
+        for c in range(2):
+            r = dot(choose[...], jnp.where(core[0] == c, mine[a], peer[a]), ((1,), (0,)))
+            rows[pl.ds(2 * a + c, slots, stride=4), :] = scale[...] * r if a else r
     send[...] = rows[...].astype(BF16)
 
 
 def fill_slots(core, choose, scale, mine, peer):
-    fw = mine.shape[-1]
-    total = choose.shape[0] * 8
-    out = (whole((total, fw), BF16),)
-    scratch = [pltpu.VMEM((total, fw), F32)]
+    shape = (choose.shape[0] * 4, mine.shape[-1])
+    out = (whole(shape, BF16),)
+    scratch = [pltpu.VMEM(shape, F32)]
     return call(fill_body, out, core, choose, scale, mine, peer, scalars=1, scratch=scratch)
 
 
-def sort_body(recv, both, near, rows):
-    slots = recv.shape[0] // 8
+def sort_body(recv, pieces, rows, *, half):
+    slots = recv.shape[0] // 4
+    kept = pieces.shape[1]
     rows[...] = recv[...].astype(F32)
-    for a in range(2):
-        for n in range(2):
-            for c in range(2):
-                v = rows[pl.ds(4 * a + 2 * n + c, slots, stride=8), :].astype(BF16)
-                both[n, 2 * a + c] = v
-                if n == 0:
-                    near[2 * a + c] = v
-
-
-def sort_pieces(recv):
-    slots, fw = recv.shape[0] // 8, recv.shape[1]
-    out = (whole((2, 4, slots, fw), BF16), whole((4, slots, fw), BF16))
-    return call(sort_body, out, recv, scratch=[pltpu.VMEM(recv.shape, F32)], kept=(0, 1))
-
-
-def shards(chip, both, f1, b1, f2, b2, n_y):
-    found = []
-    for off, ref in ((0, both), (n_y - 1, f1), (1, b1)):
-        for n in range(2):
-            found.append((off + 4 * n, [ref[n, i] for i in range(4)]))
-    for off, ref in ((n_y - 2, f2), (2, b2)):
-        found.append((off, [ref[i] for i in range(4)]))
-    for off, p in found:
-        y = lax.rem(chip + off, n_y)
-        yield y, jnp.concatenate(p[:2], axis=1), jnp.concatenate(p[2:], axis=1)
-
-
-def expert_body(chip, both, f1, b1, f2, b2, wgu_peer, wg, wu, wd, wd_peer, gu_grad, hidden, part):
+    r, c = iota((kept, slots), 0), iota((kept, slots), 1)
+    block = (c * (65536 // (half + 1) + 1)) >> 16
+    hit = (c - block == r) & (c - block * (half + 1) < half)
+    keep = jnp.where(hit, 1.0, 0.0).astype(BF16)
+    for q in range(4):
+        v = rows[pl.ds(q, slots, stride=4), :].astype(BF16)
+        pieces[q] = dot(keep, v, ((1,), (0,))).astype(BF16)
+
+
+def sort_pieces(recv, half):
+    kept = recv.shape[0] // 4 // (half + 1) * half
+    out = (whole((4, kept, recv.shape[1]), BF16),)
+    body = functools.partial(sort_body, half=half)
+    return call(body, out, recv, scratch=[pltpu.VMEM(recv.shape, F32)], kept=(0,))
+
+
+OFFSETS = (0, -1, 1, -2, 2, 4, 3, 5)
+
+
+def shards(chip, blocks, n_y):
+    for off, ref in zip(OFFSETS, blocks):
+        y = lax.rem(chip + off % n_y, n_y)
+        yield y, jnp.concatenate([ref[0], ref[1]], axis=1), jnp.concatenate([ref[2], ref[3]], axis=1)
+
+
+def expert_body(chip, *refs):
+    blocks, (wgu_peer, wg, wu, wd, wd_peer, gu_grad, hidden, part) = refs[:8], refs[8:]
     n_y = part.shape[0]
     fw = wd.shape[0]
     rows, hid = hidden.shape
@@ -143,7 +139,7 @@
         at = pl.ds(pl.multiple_of(y * 2 * fw, 2 * fw), 2 * fw)
         return jnp.concatenate([wg[at, :], wgu_peer[0, at, :], wu[at, :], wgu_peer[1, at, :]], axis=1), at
 
-    for y, x_in, x_cot in shards(chip[0], both, f1, b1, f2, b2, n_y):
+    for y, x_in, x_cot in shards(chip[0], blocks, n_y):
         w, at = weights(y)
         acc = acc + dot(x_in, w, ((1,), (0,)))
         back = back + dot(x_cot, jnp.concatenate([wd[:, at], wd_peer[:, at]], axis=0), ((1,), (1,)))
@@ -163,7 +159,7 @@
 
 
 def expert_rows_grad(chip, blocks, wgu_peer, wg, wu, wd, wd_peer, n_y):
-    rows, fw = blocks[0].shape[2:]
+    rows, fw = blocks[0].shape[1:]
     hid = 2 * wg.shape[1]
 
     out = (whole((rows, 2 * hid), BF16), whole((rows, hid), BF16), whole((n_y, 2, rows, fw), BF16))
@@ -171,11 +167,12 @@
     return call(expert_body, out, chip, *blocks, *weights, scalars=1)
 
 
-def weight_body(chip, both, f1, b1, f2, b2, gu_grad, hidden, dgu, dgu_send, dd, dd_send):
+def weight_body(chip, *refs):
+    blocks, (gu_grad, hidden, dgu, dgu_send, dd, dd_send) = refs[:8], refs[8:]
     fw = dd.shape[0]
     hid = hidden.shape[1]
     n_y = dd.shape[1] // (2 * fw)
-    for y, x_in, x_cot in shards(chip[0], both, f1, b1, f2, b2, n_y):
+    for y, x_in, x_cot in shards(chip[0], blocks, n_y):
         at = pl.ds(pl.multiple_of(y * 2 * fw, 2 * fw), 2 * fw)
         r = dot(x_in, gu_grad[...], ((0,), (0,))).astype(BF16)
         for i in range(2):
@@ -187,9 +184,9 @@
 
 
 def expert_weight_grads(chip, blocks, gu_grad, hidden, d):
-    fw = blocks[0].shape[3]
+    fw = blocks[0].shape[2]
     out = (whole((2, d, fw), BF16),) * 2 + (whole((fw, d), BF16),) * 2
-    return call(weight_body, out, chip, *blocks, gu_grad, hidden, scalars=1, loose=(6, 7))
+    return call(weight_body, out, chip, *blocks, gu_grad, hidden, scalars=1, loose=(9, 10))
 
 
 def add_body(parts, out, *, half):
@@ -311,18 +308,25 @@
 
     own = jnp.stack([ffn_input, out_grad])
     far = over_y(own, n_y // 2)
-    mine = jnp.stack([own, far])
-    peer = over_cores(mine)
+    peer = over_cores(own)
     pick, choose, scale = route_slots(core, routes.T, route_weight.T, n_sp, half)
-    send = fill_slots(core, choose, scale, mine, peer)
-
-    send, late_gate, late_up, late_down = lax.optimization_barrier((send, gate_w, up_w, down_w))
+
+    def dispatch(mine, other):
+        send = fill_slots(core, choose, scale, mine, other)
+        recv = lax.all_to_all(send.reshape(n_sp, -1, fw), SP, 0, 0, tiled=True).reshape(send.shape)
+        return send, sort_pieces(recv, half)
+
+    near_send, near = dispatch(own, peer)
+    far_peer = over_cores(far)
+    _, beyond = dispatch(far, far_peer)
+
+    _, late_gate, late_up, late_down = lax.optimization_barrier((near_send, gate_w, up_w, down_w))
     wgu = jnp.concatenate([late_gate, late_up], axis=0)
     wgu_peer = over_cores(wgu)
     wd_peer = over_cores(late_down[0])
-    recv = lax.all_to_all(send.reshape(n_sp, -1, fw), SP, 0, 0, tiled=True).reshape(send.shape)
-    both, near = sort_pieces(recv)
-    blocks = (both, over_y(both, 1), over_y(both, -1), over_y(near, 2), over_y(near, -2))
+    near_blocks = [over_y(near, step) for step in (1, -1, 2, -2)]
+    far_blocks = [over_y(beyond, step) for step in (1, -1)]
+    blocks = (near, *near_blocks, beyond, *far_blocks)
 
     gu_grad, hidden, part = expert_rows_grad(
         chip, blocks, wgu_peer, late_gate[0], late_up[0], late_down[0], wd_peer, n_y

time: 162 us -> 177 us (1.093)
  starting transfers between devices: 62 us -> 86.6 us
  waiting for transfers between devices: 59.8 us -> 48.4 us
    all_to_all x1 -> x2, waiting for transfers between devices: 12.4 us -> 1.24 us  [dispatch(): lax.all_to_all(send.reshape(n_sp, -1, fw), SP, 0, 0, tiled=True)]
    all_to_all x1 -> x2, starting transfers between devices: 13.2 us -> 23 us  [dispatch(): lax.all_to_all(send.reshape(n_sp, -1, fw), SP, 0, 0, tiled=True)]
    ppermute x5 -> x7, starting transfers between devices: 22 us -> 27.3 us  [over_y(): return lax.ppermute(v, 'y', [(i, (i + step) % n_y) for i in range(n_y)])]
    all_to_all x1, starting transfers between devices: 4.05 us -> 8.78 us  [per_device(): lax.all_to_all(part.reshape(2 * n_y, *part.shape[2:]), TP, 0, 0, tiled=True)]
    ppermute x5 -> x7, waiting for transfers between devices: 12.5 us -> 9.21 us  [over_y(): return lax.ppermute(v, 'y', [(i, (i + step) % n_y) for i in range(n_y)])]
    all_to_all x1, starting transfers between devices: 5.1 us -> 7.87 us  [per_device(): lax.all_to_all(back.reshape(n_sp, 16, fw), SP, 0, 0, tiled=True)]
    ppermute x5 -> x6, starting transfers between devices: 10.6 us -> 12.6 us  [over_cores(): return lax.ppermute(v, 'c', [(0, 1), (1, 0)])]
    all_to_all x1, waiting for transfers between devices: 14.9 us -> 16.8 us  [per_device(): last = lax.all_to_all(last, SP, 0, 0, tiled=True)]
  transfers between devices with their start and end apart: 14 -> 18, of which waited for: 7 -> 9; matrix products, arithmetic and copies ran while one was open for 3% -> 2% of each run, Pallas kernels for 4% -> 4%
where the time goes in v3:
time: 177 us; the launch traced here: 175 us
  starting transfers between devices  86.6 us (49%)
  waiting for transfers between devices  48.4 us (27%)
  blocking collectives  17.7 us (10%)
  Pallas kernels  13.1 us (7%)
  other arithmetic  4.48 us (3%)
  local copies, waits for them, and re-layouts  2.92 us (2%)
    ppermute x7, starting transfers between devices, over_y(): return lax.ppermute(v, 'y', [(i, (i + step) % n_y) for i in range(n_y)])  27.3 us
    all_to_all x2, starting transfers between devices, dispatch(): lax.all_to_all(send.reshape(n_sp, -1, fw), SP, 0, 0, tiled=True)  23 us
    all_gather x1, blocking collectives, per_device(): mix_grad = lax.all_gather(own_grad, TP, axis=1, tiled=True)  17.7 us
    all_to_all x1, waiting for transfers between devices, per_device(): last = lax.all_to_all(last, SP, 0, 0, tiled=True)  16.8 us
    all_to_all x1, waiting for transfers between devices, per_device(): lax.all_to_all(part.reshape(2 * n_y, *part.shape[2:]), TP, 0, 0, tiled=True)  16.5 us
    pallas_call x10, Pallas kernels, call(): pl.pallas_call(body, out_shape=tuple(outs), in_specs=[SMEM] * scalars + [...  13.1 us
    ppermute x6, starting transfers between devices, over_cores(): return lax.ppermute(v, 'c', [(0, 1), (1, 0)])  12.6 us
    ppermute x7, waiting for transfers between devices, over_y(): return lax.ppermute(v, 'y', [(i, (i + step) % n_y) for i in range(n_y)])  9.21 us
  transfers between devices with their start and end apart: 18, of which 9 were waited for; matrix products, arithmetic and copies ran while one was open for 2% of the time, Pallas kernels for 4%

profile of v3, /device:TPU:8, one launch (start us, length us, event | category | flops | bytes accessed | tf_op | source)
XLA Modules:
  0.0 175.4 jit_solution(3300580540036339730)
XLA Ops:
  1.4 1.9 %collective-permute-start = (bf16[2,128,128]{2,1,0:T(8,128)(2,1)S(1)}, bf16[2,128,128]{2,1,0:T(8,128)(2,1)S(1)}, u32[]{:S(2)}, u32[]{:S(2)}) collective-permute-start(bf16[2,128,128]{2,1,0:T(8,128)(2,1)S(1)} %pad_maximum_fusion.1.mine), channel_id=1, source_target_pairs={{0,1},{1,0},{2,3},{3,2},{4,5},{5,4},{6,7},{7,6},{8,9},{9,8},{10,11... | collective-permute-start | bytes 196616 | tf_op jit(solution)/shard_map/ppermute | solution.py:307
  6.5 2.3 %pad_maximum_fusion = bf16[2,2048,128]{2,1,0:T(8,128)(2,1)} fusion(bf16[1,2048,128]{2,1,0:T(8,128)(2,1)} %param.18, bf16[1,2048,128]{2,1,0:T(8,128)(2,1)} %param.17), kind=kLoop, calls=%fused_computation.3 | loop fusion | flops 524288 | bytes 2097152 | tf_op jit(solution)/shard_map/concatenate | solution.py:324
  8.8 2.5 %collective-permute-start.9 = (bf16[2,2048,128]{2,1,0:T(8,128)(2,1)}, bf16[2,2048,128]{2,1,0:T(8,128)(2,1)S(1)}, u32[]{:S(2)}, u32[]{:S(2)}) collective-permute-start(bf16[2,2048,128]{2,1,0:T(8,128)(2,1)} %pad_maximum_fusion), channel_id=1, source_target_pairs={{0,1},{1,0},{2,3},{3,2},{4,5},{5,4},{6,7},{7,6},{8,9},{9,8},{10,11... | collective-permute-start | bytes 3145736 | tf_op jit(solution)/shard_map/ppermute | solution.py:307
  11.3 13.2 %all-to-all-start = ((bf16[32,24,128]{2,1,0:T(8,128)(2,1)}), bf16[32,24,128]{2,1,0:T(8,128)(2,1)S(1)}, u32[]{:S(2)}, u32[]{:S(2)}) async-start(bf16[32,24,128]{2,1,0:T(8,128)(2,1)} %bitcast.6), calls=%async_computation | async-start | bytes 393216 | tf_op jit(solution)/shard_map/all_to_all | solution.py:316
  24.5 1.9 %collective-permute-start.10 = (bf16[128,2048]{1,0:T(8,128)(2,1)}, bf16[128,2048]{1,0:T(8,128)(2,1)}, u32[]{:S(2)}, u32[]{:S(2)}) collective-permute-start(bf16[128,2048]{1,0:T(8,128)(2,1)} %bitcast.12.refs_11_), channel_id=1, source_target_pairs={{0,1},{1,0},{2,3},{3,2},{4,5},{5,4},{6,7},{7,6},{8,9},{9,8},{10,11... | collective-permute-start | bytes 1572872 | tf_op jit(solution)/shard_map/ppermute | solution.py:307
  26.4 6.8 %collective-permute-start.5 = (bf16[2,128,128]{2,1,0:T(8,128)(2,1)S(1)}, bf16[2,128,128]{2,1,0:T(8,128)(2,1)S(1)}, u32[]{:S(2)}, u32[]{:S(2)}) collective-permute-start(bf16[2,128,128]{2,1,0:T(8,128)(2,1)S(1)} %pad_maximum_fusion.1.mine), channel_id=1, source_target_pairs={{0,8},{2,10},{4,12},{6,14},{8,0},{10,2},{12,4},{14,6},{1,9},{3,11}... | collective-permute-start | bytes 196616 | tf_op jit(solution)/shard_map/ppermute | solution.py:304
  33.3 3.6 %collective-permute-done.5.mine = bf16[2,128,128]{2,1,0:T(8,128)(2,1)S(1)} collective-permute-done((bf16[2,128,128]{2,1,0:T(8,128)(2,1)S(1)}, bf16[2,128,128]{2,1,0:T(8,128)(2,1)S(1)}, u32[]{:S(2)}, u32[]{:S(2)}) %collective-permute-start.5) | collective-permute-done | bytes 65568 | tf_op jit(solution)/shard_map/ppermute | solution.py:304
  36.8 1.9 %collective-permute-start.6 = (bf16[2,128,128]{2,1,0:T(8,128)(2,1)S(1)}, bf16[2,128,128]{2,1,0:T(8,128)(2,1)S(1)}, u32[]{:S(2)}, u32[]{:S(2)}) collective-permute-start(bf16[2,128,128]{2,1,0:T(8,128)(2,1)S(1)} %collective-permute-done.5.mine), channel_id=1, source_target_pairs={{0,1},{1,0},{2,3},{3,2},{4,5},{5,4},{6,7},{7,6},{8,9},{9,8},{10,11... | collective-permute-start | bytes 196616 | tf_op jit(solution)/shard_map/ppermute | solution.py:307
  38.8 1.2 collective-permute-done.6.peer
  40.9 9.8 %all-to-all-start.1 = ((bf16[32,24,128]{2,1,0:T(8,128)(2,1)}), bf16[32,24,128]{2,1,0:T(8,128)(2,1)S(1)}, u32[]{:S(2)}, u32[]{:S(2)}) async-start(bf16[32,24,128]{2,1,0:T(8,128)(2,1)} %bitcast.29), calls=%async_computation.1 | async-start | bytes 393216 | tf_op jit(solution)/shard_map/all_to_all | solution.py:316
  50.9 6.6 %collective-permute-start.4 = (bf16[4,160,128]{2,1,0:T(8,128)(2,1)S(1)}, bf16[4,160,128]{2,1,0:T(8,128)(2,1)S(1)}, u32[]{:S(2)}, u32[]{:S(2)}) collective-permute-start(bf16[4,160,128]{2,1,0:T(8,128)(2,1)S(1)} %shard_map.182.refs_0_), channel_id=1, source_target_pairs={{0,12},{2,14},{4,0},{6,2},{8,4},{10,6},{12,8},{14,10},{1,13},{3,15... | collective-permute-start | bytes 491528 | tf_op jit(solution)/shard_map/ppermute | solution.py:304
  57.5 1.9 %collective-permute-start.3 = (bf16[4,160,128]{2,1,0:T(8,128)(2,1)S(1)}, bf16[4,160,128]{2,1,0:T(8,128)(2,1)S(1)}, u32[]{:S(2)}, u32[]{:S(2)}) collective-permute-start(bf16[4,160,128]{2,1,0:T(8,128)(2,1)S(1)} %shard_map.182.refs_0_), channel_id=1, source_target_pairs={{0,4},{2,6},{4,8},{6,10},{8,12},{10,14},{12,0},{14,2},{1,5},{3,7},... | collective-permute-start | bytes 491528 | tf_op jit(solution)/shard_map/ppermute | solution.py:304
  59.4 1.9 %collective-permute-start.2 = (bf16[4,160,128]{2,1,0:T(8,128)(2,1)S(1)}, bf16[4,160,128]{2,1,0:T(8,128)(2,1)S(1)}, u32[]{:S(2)}, u32[]{:S(2)}) collective-permute-start(bf16[4,160,128]{2,1,0:T(8,128)(2,1)S(1)} %shard_map.182.refs_0_), channel_id=1, source_target_pairs={{0,14},{2,0},{4,2},{6,4},{8,6},{10,8},{12,10},{14,12},{1,15},{3,1}... | collective-permute-start | bytes 491528 | tf_op jit(solution)/shard_map/ppermute | solution.py:304
  61.4 1.2 all-to-all-done.1
  62.9 4.8 %collective-permute-start.1 = (bf16[4,160,128]{2,1,0:T(8,128)(2,1)S(1)}, bf16[4,160,128]{2,1,0:T(8,128)(2,1)S(1)}, u32[]{:S(2)}, u32[]{:S(2)}) collective-permute-start(bf16[4,160,128]{2,1,0:T(8,128)(2,1)S(1)} %shard_map.182.refs_0_), channel_id=1, source_target_pairs={{0,2},{2,4},{4,6},{6,8},{8,10},{10,12},{12,14},{14,0},{1,3},{3,5},... | collective-permute-start | bytes 491528 | tf_op jit(solution)/shard_map/ppermute | solution.py:304
  67.7 2.4 %collective-permute-start.8 = (bf16[4,160,128]{2,1,0:T(8,128)(2,1)S(1)}, bf16[4,160,128]{2,1,0:T(8,128)(2,1)S(1)}, u32[]{:S(2)}, u32[]{:S(2)}) collective-permute-start(bf16[4,160,128]{2,1,0:T(8,128)(2,1)S(1)} %shard_map.184.refs_5_), channel_id=1, source_target_pairs={{0,14},{2,0},{4,2},{6,4},{8,6},{10,8},{12,10},{14,12},{1,15},{3,1}... | collective-permute-start | bytes 491528 | tf_op jit(solution)/shard_map/ppermute | solution.py:304
  70.8 2.8 %collective-permute-start.7 = (bf16[4,160,128]{2,1,0:T(8,128)(2,1)S(1)}, bf16[4,160,128]{2,1,0:T(8,128)(2,1)S(1)}, u32[]{:S(2)}, u32[]{:S(2)}) collective-permute-start(bf16[4,160,128]{2,1,0:T(8,128)(2,1)S(1)} %shard_map.184.refs_5_), channel_id=1, source_target_pairs={{0,2},{2,4},{4,6},{6,8},{8,10},{10,12},{12,14},{14,0},{1,3},{3,5},... | collective-permute-start | bytes 491528 | tf_op jit(solution)/shard_map/ppermute | solution.py:304
  73.6 1.3 collective-permute-done.8.refs_7_
  74.9 3.7 %collective-permute-done.7.refs_6_ = bf16[4,160,128]{2,1,0:T(8,128)(2,1)S(1)} collective-permute-done((bf16[4,160,128]{2,1,0:T(8,128)(2,1)S(1)}, bf16[4,160,128]{2,1,0:T(8,128)(2,1)S(1)}, u32[]{:S(2)}, u32[]{:S(2)}) %collective-permute-start.7) | collective-permute-done | bytes 163872 | tf_op jit(solution)/shard_map/ppermute | solution.py:304
  78.6 4.1 %shard_map.185 = (bf16[160,512]{1,0:T(8,128)(2,1)}, bf16[160,256]{1,0:T(8,128)(2,1)}, bf16[8,2,160,128]{3,2,1,0:T(8,128)(2,1)}) custom-call(s32[1]{0:T(128)} %bitcast.chip, bf16[4,160,128]{2,1,0:T(8,128)(2,1)S(1)} %shard_map.182.refs_0_, bf16[4,160,128]{2,1,0:T(8,128)(2,1)S(1)} %collective-permute-done.1.refs_1_, ...), custom_call_target="tpu_custom_call" | custom-call | tf_op jit(solution)/shard_map/pallas_call | solution.py:31
  82.7 8.8 %all-to-all-start.2 = ((bf16[16,160,128]{2,1,0:T(8,128)(2,1)}), bf16[16,160,128]{2,1,0:T(8,128)(2,1)S(1)}, u32[]{:S(2)}, u32[]{:S(2)}) async-start(bf16[16,160,128]{2,1,0:T(8,128)(2,1)} %bitcast.30), calls=%async_computation.2 | async-start | bytes 1310720 | tf_op jit(solution)/shard_map/all_to_all | solution.py:334
  91.5 16.5 %all-to-all-done.2 = bf16[16,160,128]{2,1,0:T(8,128)(2,1)S(1)} async-done(((bf16[16,160,128]{2,1,0:T(8,128)(2,1)}), bf16[16,160,128]{2,1,0:T(8,128)(2,1)S(1)}, u32[]{:S(2)}, u32[]{:S(2)}) %all-to-all-start.2) | async-done | bytes 655392 | tf_op jit(solution)/shard_map/all_to_all | solution.py:334
  109.1 7.9 %all-to-all-start.3 = ((bf16[32,16,128]{2,1,0:T(8,128)(2,1)}), bf16[32,16,128]{2,1,0:T(8,128)(2,1)}, u32[]{:S(2)}, u32[]{:S(2)}) async-start(bf16[32,16,128]{2,1,0:T(8,128)(2,1)} %bitcast.31), calls=%async_computation.3 | async-start | bytes 262144 | tf_op jit(solution)/shard_map/all_to_all | solution.py:336
  117.2 2.7 %shard_map.186 = (bf16[2,2048,128]{2,1,0:T(8,128)(2,1)}, bf16[2,2048,128]{2,1,0:T(8,128)(2,1)}, bf16[128,2048]{1,0:T(8,128)(2,1)}, bf16[128,2048]{1,0:T(8,128)(2,1)}) custom-call(s32[1]{0:T(128)} %bitcast.chip, bf16[4,160,128]{2,1,0:T(8,128)(2,1)S(1)} %shard_map.182.refs_0_, bf16[4,160,128]{2,1,0:T(8,128)(2,1)S(1)} %collective-permute-done.1.refs_1_, ...), custom_call_target="tpu_custom_call" | custom-call | tf_op jit(solution)/shard_map/pallas_call | solution.py:31
  119.9 1.9 %collective-permute-start.12 = (bf16[128,2048]{1,0:T(8,128)(2,1)}, bf16[128,2048]{1,0:T(8,128)(2,1)S(1)}, u32[]{:S(2)}, u32[]{:S(2)}) collective-permute-start(bf16[128,2048]{1,0:T(8,128)(2,1)} %get-tuple-element.37), channel_id=1, source_target_pairs={{0,1},{1,0},{2,3},{3,2},{4,5},{5,4},{6,7},{7,6},{8,9},{9,8},{10,11... | collective-permute-start | bytes 1572872 | tf_op jit(solution)/shard_map/ppermute | solution.py:307
  121.8 2.4 %collective-permute-start.11 = (bf16[2,2048,128]{2,1,0:T(8,128)(2,1)}, bf16[2,2048,128]{2,1,0:T(8,128)(2,1)S(1)}, u32[]{:S(2)}, u32[]{:S(2)}) collective-permute-start(bf16[2,2048,128]{2,1,0:T(8,128)(2,1)} %get-tuple-element.35), channel_id=1, source_target_pairs={{0,1},{1,0},{2,3},{3,2},{4,5},{5,4},{6,7},{7,6},{8,9},{9,8},{10,11... | collective-permute-start | bytes 3145736 | tf_op jit(solution)/shard_map/ppermute | solution.py:307
  124.3 3.4 %all-to-all-done.3 = bf16[32,16,128]{2,1,0:T(8,128)(2,1)} async-done(((bf16[32,16,128]{2,1,0:T(8,128)(2,1)}), bf16[32,16,128]{2,1,0:T(8,128)(2,1)}, u32[]{:S(2)}, u32[]{:S(2)}) %all-to-all-start.3) | async-done | bytes 131104 | tf_op jit(solution)/shard_map/all_to_all | solution.py:336
  127.7 1.2 fusion
  128.9 17.7 %all_gather.3.mix = bf16[128,2048]{1,0:T(8,128)(2,1)S(1)} all-gather(bf16[128,128]{1,0:T(8,128)(2,1)S(1)} %fusion), channel_id=1, replica_groups=mesh['z'=8,'x'=4,'y'=8,'c'=2] {'y','c'}, dimensions={1}, use_global_device_ids=true | all-gather | bytes 557056 | tf_op jit(solution)/shard_map/all_gather | solution.py:343
  146.6 1.3 shard_map.188
  147.9 7.2 %all-to-all-start.4 = ((bf16[32,72,128]{2,1,0:T(8,128)(2,1)}), bf16[32,72,128]{2,1,0:T(8,128)(2,1)S(1)}, u32[]{:S(2)}, u32[]{:S(2)}) async-start(bf16[32,72,128]{2,1,0:T(8,128)(2,1)} %get-tuple-element.40), calls=%async_computation.4 | async-start | bytes 1179648 | tf_op jit(solution)/shard_map/all_to_all | solution.py:360
  157.8 16.8 %all-to-all-done.4.last = bf16[32,72,128]{2,1,0:T(8,128)(2,1)S(1)} async-done(((bf16[32,72,128]{2,1,0:T(8,128)(2,1)}), bf16[32,72,128]{2,1,0:T(8,128)(2,1)S(1)}, u32[]{:S(2)}, u32[]{:S(2)}) %all-to-all-start.4) | async-done | bytes 589856 | tf_op jit(solution)/shard_map/all_to_all | solution.py:360
  (58 shorter events, 10.8 us)
Async XLA Ops:
  1.4 4.2 %collective-permute-start = (bf16[2,128,128]{2,1,0:T(8,128)(2,1)S(1)}, bf16[2,128,128]{2,1,0:T(8,128)(2,1)S(1)}, u32[]{:S(2)}, u32[]{:S(2)}) collective-permute-start(bf16[2,128,128]{2,1,0:T(8,128)(2,1)S(1)} %pad_maximum_fusion.1.mine), channel_id=1, source_target_pairs={{0,1},{1,0},{2,3},{3,2},{4,5},{5,4},{6,7},{7,6},{8,9},{9,8},{10,11... | collective-permute-start | bytes 196616 | tf_op jit(solution)/shard_map/ppermute | solution.py:307
  8.8 69.8 %copy-start = (bf16[1,2048,128]{2,1,0:T(8,128)(2,1)S(1)}, bf16[1,2048,128]{2,1,0:T(8,128)(2,1)}, u32[]{:S(2)}) copy-start(bf16[1,2048,128]{2,1,0:T(8,128)(2,1)} %param.18) | copy-start | bytes 1572868
  8.8 69.8 %copy-start.1 = (bf16[1,2048,128]{2,1,0:T(8,128)(2,1)S(1)}, bf16[1,2048,128]{2,1,0:T(8,128)(2,1)}, u32[]{:S(2)}) copy-start(bf16[1,2048,128]{2,1,0:T(8,128)(2,1)} %param.17) | copy-start | bytes 1572868
  8.8 69.8 %collective-permute-start.9 = (bf16[2,2048,128]{2,1,0:T(8,128)(2,1)}, bf16[2,2048,128]{2,1,0:T(8,128)(2,1)S(1)}, u32[]{:S(2)}, u32[]{:S(2)}) collective-permute-start(bf16[2,2048,128]{2,1,0:T(8,128)(2,1)} %pad_maximum_fusion), channel_id=1, source_target_pairs={{0,1},{1,0},{2,3},{3,2},{4,5},{5,4},{6,7},{7,6},{8,9},{9,8},{10,11... | collective-permute-start | bytes 3145736 | tf_op jit(solution)/shard_map/ppermute | solution.py:307
  11.3 29.6 %all-to-all-start = ((bf16[32,24,128]{2,1,0:T(8,128)(2,1)}), bf16[32,24,128]{2,1,0:T(8,128)(2,1)S(1)}, u32[]{:S(2)}, u32[]{:S(2)}) async-start(bf16[32,24,128]{2,1,0:T(8,128)(2,1)} %bitcast.6), calls=%async_computation | async-start | bytes 393216 | tf_op jit(solution)/shard_map/all_to_all | solution.py:316
  24.5 38.3 %collective-permute-start.10 = (bf16[128,2048]{1,0:T(8,128)(2,1)}, bf16[128,2048]{1,0:T(8,128)(2,1)}, u32[]{:S(2)}, u32[]{:S(2)}) collective-permute-start(bf16[128,2048]{1,0:T(8,128)(2,1)} %bitcast.12.refs_11_), channel_id=1, source_target_pairs={{0,1},{1,0},{2,3},{3,2},{4,5},{5,4},{6,7},{7,6},{8,9},{9,8},{10,11... | collective-permute-start | bytes 1572872 | tf_op jit(solution)/shard_map/ppermute | solution.py:307
  26.4 10.4 %collective-permute-start.5 = (bf16[2,128,128]{2,1,0:T(8,128)(2,1)S(1)}, bf16[2,128,128]{2,1,0:T(8,128)(2,1)S(1)}, u32[]{:S(2)}, u32[]{:S(2)}) collective-permute-start(bf16[2,128,128]{2,1,0:T(8,128)(2,1)S(1)} %pad_maximum_fusion.1.mine), channel_id=1, source_target_pairs={{0,8},{2,10},{4,12},{6,14},{8,0},{10,2},{12,4},{14,6},{1,9},{3,11}... | collective-permute-start | bytes 196616 | tf_op jit(solution)/shard_map/ppermute | solution.py:304
  36.8 3.1 %collective-permute-start.6 = (bf16[2,128,128]{2,1,0:T(8,128)(2,1)S(1)}, bf16[2,128,128]{2,1,0:T(8,128)(2,1)S(1)}, u32[]{:S(2)}, u32[]{:S(2)}) collective-permute-start(bf16[2,128,128]{2,1,0:T(8,128)(2,1)S(1)} %collective-permute-done.5.mine), channel_id=1, source_target_pairs={{0,1},{1,0},{2,3},{3,2},{4,5},{5,4},{6,7},{7,6},{8,9},{9,8},{10,11... | collective-permute-start | bytes 196616 | tf_op jit(solution)/shard_map/ppermute | solution.py:307
  40.9 21.7 %all-to-all-start.1 = ((bf16[32,24,128]{2,1,0:T(8,128)(2,1)}), bf16[32,24,128]{2,1,0:T(8,128)(2,1)S(1)}, u32[]{:S(2)}, u32[]{:S(2)}) async-start(bf16[32,24,128]{2,1,0:T(8,128)(2,1)} %bitcast.29), calls=%async_computation.1 | async-start | bytes 393216 | tf_op jit(solution)/shard_map/all_to_all | solution.py:316
  50.9 16.8 %collective-permute-start.4 = (bf16[4,160,128]{2,1,0:T(8,128)(2,1)S(1)}, bf16[4,160,128]{2,1,0:T(8,128)(2,1)S(1)}, u32[]{:S(2)}, u32[]{:S(2)}) collective-permute-start(bf16[4,160,128]{2,1,0:T(8,128)(2,1)S(1)} %shard_map.182.refs_0_), channel_id=1, source_target_pairs={{0,12},{2,14},{4,0},{6,2},{8,4},{10,6},{12,8},{14,10},{1,13},{3,15... | collective-permute-start | bytes 491528 | tf_op jit(solution)/shard_map/ppermute | solution.py:304
  57.5 13.3 %collective-permute-start.3 = (bf16[4,160,128]{2,1,0:T(8,128)(2,1)S(1)}, bf16[4,160,128]{2,1,0:T(8,128)(2,1)S(1)}, u32[]{:S(2)}, u32[]{:S(2)}) collective-permute-start(bf16[4,160,128]{2,1,0:T(8,128)(2,1)S(1)} %shard_map.182.refs_0_), channel_id=1, source_target_pairs={{0,4},{2,6},{4,8},{6,10},{8,12},{10,14},{12,0},{14,2},{1,5},{3,7},... | collective-permute-start | bytes 491528 | tf_op jit(solution)/shard_map/ppermute | solution.py:304
  59.4 14.2 %collective-permute-start.2 = (bf16[4,160,128]{2,1,0:T(8,128)(2,1)S(1)}, bf16[4,160,128]{2,1,0:T(8,128)(2,1)S(1)}, u32[]{:S(2)}, u32[]{:S(2)}) collective-permute-start(bf16[4,160,128]{2,1,0:T(8,128)(2,1)S(1)} %shard_map.182.refs_0_), channel_id=1, source_target_pairs={{0,14},{2,0},{4,2},{6,4},{8,6},{10,8},{12,10},{14,12},{1,15},{3,1}... | collective-permute-start | bytes 491528 | tf_op jit(solution)/shard_map/ppermute | solution.py:304
  62.9 10.7 %collective-permute-start.1 = (bf16[4,160,128]{2,1,0:T(8,128)(2,1)S(1)}, bf16[4,160,128]{2,1,0:T(8,128)(2,1)S(1)}, u32[]{:S(2)}, u32[]{:S(2)}) collective-permute-start(bf16[4,160,128]{2,1,0:T(8,128)(2,1)S(1)} %shard_map.182.refs_0_), channel_id=1, source_target_pairs={{0,2},{2,4},{4,6},{6,8},{8,10},{10,12},{12,14},{14,0},{1,3},{3,5},... | collective-permute-start | bytes 491528 | tf_op jit(solution)/shard_map/ppermute | solution.py:304
  67.7 7.2 %collective-permute-start.8 = (bf16[4,160,128]{2,1,0:T(8,128)(2,1)S(1)}, bf16[4,160,128]{2,1,0:T(8,128)(2,1)S(1)}, u32[]{:S(2)}, u32[]{:S(2)}) collective-permute-start(bf16[4,160,128]{2,1,0:T(8,128)(2,1)S(1)} %shard_map.184.refs_5_), channel_id=1, source_target_pairs={{0,14},{2,0},{4,2},{6,4},{8,6},{10,8},{12,10},{14,12},{1,15},{3,1}... | collective-permute-start | bytes 491528 | tf_op jit(solution)/shard_map/ppermute | solution.py:304
  70.8 7.8 %collective-permute-start.7 = (bf16[4,160,128]{2,1,0:T(8,128)(2,1)S(1)}, bf16[4,160,128]{2,1,0:T(8,128)(2,1)S(1)}, u32[]{:S(2)}, u32[]{:S(2)}) collective-permute-start(bf16[4,160,128]{2,1,0:T(8,128)(2,1)S(1)} %shard_map.184.refs_5_), channel_id=1, source_target_pairs={{0,2},{2,4},{4,6},{6,8},{8,10},{10,12},{12,14},{14,0},{1,3},{3,5},... | collective-permute-start | bytes 491528 | tf_op jit(solution)/shard_map/ppermute | solution.py:304
  82.7 8.8 %copy-start.16 = (f32[128]{0:T(128)S(1)}, f32[128]{0:T(128)}, u32[]{:S(2)}) copy-start(f32[128]{0:T(128)} %param.25) | copy-start | bytes 1540
  82.7 34.3 %copy-start.10 = (bf16[128,128]{1,0:T(8,128)(2,1)S(1)}, bf16[128,128]{1,0:T(8,128)(2,1)}, u32[]{:S(2)}) copy-start(bf16[128,128]{1,0:T(8,128)(2,1)} %param.22) | copy-start | bytes 98308
  82.7 34.3 %copy-start.11 = (bf16[128,128]{1,0:T(8,128)(2,1)S(1)}, bf16[128,128]{1,0:T(8,128)(2,1)}, u32[]{:S(2)}) copy-start(bf16[128,128]{1,0:T(8,128)(2,1)} %param.21) | copy-start | bytes 98308
  82.7 34.3 %copy-start.13 = (bf16[128,128]{1,0:T(8,128)(2,1)S(1)}, bf16[128,128]{1,0:T(8,128)(2,1)}, u32[]{:S(2)}) copy-start(bf16[128,128]{1,0:T(8,128)(2,1)} %param.24) | copy-start | bytes 98308
  82.7 34.3 %copy-start.15 = (bf16[128,128]{1,0:T(8,128)(2,1)S(1)}, bf16[128,128]{1,0:T(8,128)(2,1)}, u32[]{:S(2)}) copy-start(bf16[128,128]{1,0:T(8,128)(2,1)} %param.23) | copy-start | bytes 98308
  82.7 34.5 %copy-start.3 = (bf16[160,512]{1,0:T(8,128)(2,1)S(1)}, bf16[160,512]{1,0:T(8,128)(2,1)}, u32[]{:S(2)}) copy-start(bf16[160,512]{1,0:T(8,128)(2,1)} %get-tuple-element.32.refs_8_) | copy-start | bytes 491524
  82.7 34.5 %copy-start.4 = (bf16[160,256]{1,0:T(8,128)(2,1)S(1)}, bf16[160,256]{1,0:T(8,128)(2,1)}, u32[]{:S(2)}) copy-start(bf16[160,256]{1,0:T(8,128)(2,1)} %get-tuple-element.33.refs_9_) | copy-start | bytes 245764
  82.7 25.3 %all-to-all-start.2 = ((bf16[16,160,128]{2,1,0:T(8,128)(2,1)}), bf16[16,160,128]{2,1,0:T(8,128)(2,1)S(1)}, u32[]{:S(2)}, u32[]{:S(2)}) async-start(bf16[16,160,128]{2,1,0:T(8,128)(2,1)} %bitcast.30), calls=%async_computation.2 | async-start | bytes 1310720 | tf_op jit(solution)/shard_map/all_to_all | solution.py:334
  109.1 18.6 %all-to-all-start.3 = ((bf16[32,16,128]{2,1,0:T(8,128)(2,1)}), bf16[32,16,128]{2,1,0:T(8,128)(2,1)}, u32[]{:S(2)}, u32[]{:S(2)}) async-start(bf16[32,16,128]{2,1,0:T(8,128)(2,1)} %bitcast.31), calls=%async_computation.3 | async-start | bytes 262144 | tf_op jit(solution)/shard_map/all_to_all | solution.py:336
  117.0 7.2 %copy-start.12 = (bf16[128,128]{1,0:T(8,128)(2,1)S(1)}, bf16[128,128]{1,0:T(8,128)(2,1)}, u32[]{:S(2)}) copy-start(bf16[128,128]{1,0:T(8,128)(2,1)} %param.21) | copy-start | bytes 98308
  117.0 7.2 %copy-start.14 = (bf16[128,128]{1,0:T(8,128)(2,1)S(1)}, bf16[128,128]{1,0:T(8,128)(2,1)}, u32[]{:S(2)}) copy-start(bf16[128,128]{1,0:T(8,128)(2,1)} %param.24) | copy-start | bytes 98308
  117.0 10.7 %copy-start.9 = (bf16[128,128]{1,0:T(8,128)(2,1)S(1)}, bf16[128,128]{1,0:T(8,128)(2,1)}, u32[]{:S(2)}) copy-start(bf16[128,128]{1,0:T(8,128)(2,1)} %param.14) | copy-start | bytes 98308
  117.2 29.4 %copy-start.2 = (bf16[128,2048]{1,0:T(8,128)(2,1)S(1)}, bf16[128,2048]{1,0:T(8,128)(2,1)}, u32[]{:S(2)}) copy-start(bf16[128,2048]{1,0:T(8,128)(2,1)} %out_proj.1) | copy-start | bytes 1572868
  119.9 35.2 %collective-permute-start.12 = (bf16[128,2048]{1,0:T(8,128)(2,1)}, bf16[128,2048]{1,0:T(8,128)(2,1)S(1)}, u32[]{:S(2)}, u32[]{:S(2)}) collective-permute-start(bf16[128,2048]{1,0:T(8,128)(2,1)} %get-tuple-element.37), channel_id=1, source_target_pairs={{0,1},{1,0},{2,3},{3,2},{4,5},{5,4},{6,7},{7,6},{8,9},{9,8},{10,11... | collective-permute-start | bytes 1572872 | tf_op jit(solution)/shard_map/ppermute | solution.py:307
  121.8 34.3 %collective-permute-start.11 = (bf16[2,2048,128]{2,1,0:T(8,128)(2,1)}, bf16[2,2048,128]{2,1,0:T(8,128)(2,1)S(1)}, u32[]{:S(2)}, u32[]{:S(2)}) collective-permute-start(bf16[2,2048,128]{2,1,0:T(8,128)(2,1)} %get-tuple-element.35), channel_id=1, source_target_pairs={{0,1},{1,0},{2,3},{3,2},{4,5},{5,4},{6,7},{7,6},{8,9},{9,8},{10,11... | collective-permute-start | bytes 3145736 | tf_op jit(solution)/shard_map/ppermute | solution.py:307
  146.6 8.6 %copy-start.8 = (bf16[128,2048]{1,0:T(8,128)(2,1)S(1)}, bf16[128,2048]{1,0:T(8,128)(2,1)}, u32[]{:S(2)}) copy-start(bf16[128,2048]{1,0:T(8,128)(2,1)} %get-tuple-element.36) | copy-start | bytes 1572868
  147.9 26.7 %all-to-all-start.4 = ((bf16[32,72,128]{2,1,0:T(8,128)(2,1)}), bf16[32,72,128]{2,1,0:T(8,128)(2,1)S(1)}, u32[]{:S(2)}, u32[]{:S(2)}) async-start(bf16[32,72,128]{2,1,0:T(8,128)(2,1)} %get-tuple-element.40), calls=%async_computation.4 | async-start | bytes 1179648 | tf_op jit(solution)/shard_map/all_to_all | solution.py:360
  (3 other events, 2.8 us)

commit v4 on v2

--- a/solution.py
+++ b/solution.py
@@ -209,7 +209,7 @@
 
 def add_parts(parts, blocks, half):
     out = (whole((blocks * 16, parts.shape[3]), BF16),)
-    return call(functools.partial(add_body, half=half), out, parts)
+    return call(functools.partial(add_body, half=half), out, parts, kept=(0,))
 
 
 def later(v, step, fill):
@@ -252,7 +252,7 @@
     tokens, width = decay.shape
     last = whole((n_sp, mix.shape[1] // n_sp + 8, width), BF16)
     out = (whole((tokens, width), F32),) * 2 + (last,)
-    return call(chain_body, out, mix, out_proj, rec_state, decay, kept=(0, 1))
+    return call(chain_body, out, mix, out_proj, rec_state, decay, kept=(0, 1, 2))
 
 
 def finish_body(here, last, local, through, value_by, input_by, rate_by, proj, value, inp, rate):
@@ -327,17 +327,6 @@
     gu_grad, hidden, part = expert_rows_grad(
         chip, blocks, wgu_peer, late_gate[0], late_up[0], late_down[0], wd_peer, n_y
     )
-    arrived = lax.all_to_all(part.reshape(2 * n_y, *part.shape[2:]), TP, 0, 0, tiled=True)
-    back = add_parts(arrived.reshape(part.shape), n_sp, half)
-    returned = lax.all_to_all(back.reshape(n_sp, 16, fw), SP, 0, 0, tiled=True).reshape(back.shape)
-    dgu, dgu_send, dd, dd_send = expert_weight_grads(chip, blocks, gu_grad, hidden, d)
-    dgu_peer = over_cores(dgu_send)
-    dd_peer = over_cores(dd_send)
-    dgu_sum = (dgu.astype(F32) + dgu_peer.astype(F32)).astype(BF16)
-    d_down = (dd.astype(F32) + dd_peer.astype(F32)).astype(BF16)
-    own_grad = (dot(pick, returned, ((0,), (0,))) + out_grad.astype(F32)).astype(BF16)
-    mix_grad = lax.all_gather(own_grad, TP, axis=1, tiled=True)
-
     rate_gate = jax.nn.sigmoid(rate_pre.astype(F32))
     input_gate = jax.nn.sigmoid(input_pre.astype(F32))
     decay_speed = jax.nn.softplus(-decay_param)[None, :]
@@ -351,17 +340,28 @@
     input_by = value_by * signal * (1.0 - input_gate)
     decay_part = decay * before_state - input_gate * signal * decay * decay / scale_in
     rate_by = decay_part * (-decay_scale * decay_speed) * rate_gate * (1.0 - rate_gate)
+    here = lax.axis_index(SP).reshape(1).astype(jnp.int32)
+    part, here = lax.optimization_barrier((part, here))
+    arrived = lax.all_to_all(part.reshape(2 * n_y, *part.shape[2:]), TP, 0, 0, tiled=True)
+    back = add_parts(arrived.reshape(part.shape), n_sp, half)
+    returned = lax.all_to_all(back.reshape(n_sp, 16, fw), SP, 0, 0, tiled=True).reshape(back.shape)
+    dgu, dgu_send, dd, dd_send = expert_weight_grads(chip, blocks, gu_grad, hidden, d)
+    dgu_peer = over_cores(dgu_send)
+    dd_peer = over_cores(dd_send)
+    d_gate, d_up = [(dgu[i].astype(F32) + dgu_peer[i].astype(F32)).astype(BF16)[None] for i in range(2)]
+    d_down = (dd.astype(F32) + dd_peer.astype(F32)).astype(BF16)[None]
+    own_grad = (dot(pick, returned, ((0,), (0,))) + out_grad.astype(F32)).astype(BF16)
+    mix_grad = lax.all_gather(own_grad, TP, axis=1, tiled=True)
 
     local, through, last = chain_within(mix_grad, out_proj, rec_state, decay, n_sp)
     last = lax.all_to_all(last, SP, 0, 0, tiled=True)
-    here = lax.axis_index(SP).reshape(1).astype(jnp.int32)
     out_proj_grad, rec_value_grad, input_pre_grad, rate_pre_grad = finish(
         here, last, local, through, value_by, input_by, rate_by
     )
     return (
-        dgu_sum[0][None],
-        dgu_sum[1][None],
-        d_down[None],
+        d_gate,
+        d_up,
+        d_down,
         out_proj_grad,
         rec_value_grad,
         rate_pre_grad,

time: 162 us -> 164 us (1.012)
    all_to_all x1, waiting for transfers between devices: 14.9 us -> 16.8 us  [per_device(): last = lax.all_to_all(last, SP, 0, 0, tiled=True)]
  transfers between devices with their start and end apart: 14 -> 14, of which waited for: 7 -> 7; matrix products, arithmetic and copies ran while one was open for 3% -> 2% of each run, Pallas kernels for 4% -> 3%
where the time goes in v4:
time: 164 us; the launch traced here: 163 us
  starting transfers between devices  63.5 us (39%)
  waiting for transfers between devices  60.8 us (37%)
  blocking collectives  17.6 us (11%)
  Pallas kernels  12.6 us (8%)
  other arithmetic  4.3 us (3%)
  local copies, waits for them, and re-layouts  2.76 us (2%)
    ppermute x5, starting transfers between devices, over_y(): return lax.ppermute(v, 'y', [(i, (i + step) % n_y) for i in range(n_y)])  22.2 us
    all_gather x1, blocking collectives, per_device(): mix_grad = lax.all_gather(own_grad, TP, axis=1, tiled=True)  17.6 us
    all_to_all x1, waiting for transfers between devices, per_device(): last = lax.all_to_all(last, SP, 0, 0, tiled=True)  16.8 us
    all_to_all x1, waiting for transfers between devices, per_device(): lax.all_to_all(part.reshape(2 * n_y, *part.shape[2:]), TP, 0, 0, tiled=True)  16.5 us
    all_to_all x1, starting transfers between devices, per_device(): lax.all_to_all(send.reshape(n_sp, -1, fw), SP, 0, 0, tiled=True)  13.2 us
    pallas_call x8, Pallas kernels, call(): pl.pallas_call(body, out_shape=tuple(outs), in_specs=[SMEM] * scalars + [...  12.6 us
    ppermute x5, waiting for transfers between devices, over_y(): return lax.ppermute(v, 'y', [(i, (i + step) % n_y) for i in range(n_y)])  12.5 us
    all_to_all x1, waiting for transfers between devices, per_device(): lax.all_to_all(send.reshape(n_sp, -1, fw), SP, 0, 0, tiled=True)  12.4 us
  transfers between devices with their start and end apart: 14, of which 7 were waited for; matrix products, arithmetic and copies ran while one was open for 2% of the time, Pallas kernels for 3%

profile of v4, /device:TPU:8, one launch (start us, length us, event | category | flops | bytes accessed | tf_op | source)
XLA Modules:
  0.0 162.8 jit_solution(5875985512290877570)
XLA Ops:
  0.6 0.8 fusion.9
  1.5 7.0 %collective-permute-start = (bf16[2,128,128]{2,1,0:T(8,128)(2,1)S(1)}, bf16[2,128,128]{2,1,0:T(8,128)(2,1)S(1)}, u32[]{:S(2)}, u32[]{:S(2)}) collective-permute-start(bf16[2,128,128]{2,1,0:T(8,128)(2,1)S(1)} %get-tuple-element.63), channel_id=1, source_target_pairs={{0,8},{2,10},{4,12},{6,14},{8,0},{10,2},{12,4},{14,6},{1,9},{3,11}... | collective-permute-start | bytes 196616 | tf_op jit(solution)/shard_map/ppermute | solution.py:307
  8.5 3.2 %collective-permute-done = bf16[2,128,128]{2,1,0:T(8,128)(2,1)S(1)} collective-permute-done((bf16[2,128,128]{2,1,0:T(8,128)(2,1)S(1)}, bf16[2,128,128]{2,1,0:T(8,128)(2,1)S(1)}, u32[]{:S(2)}, u32[]{:S(2)}) %collective-permute-start) | collective-permute-done | bytes 65568 | tf_op jit(solution)/shard_map/ppermute | solution.py:307
  11.7 1.9 %collective-permute-start.1 = (bf16[2,2,128,128]{3,2,1,0:T(8,128)(2,1)S(1)}, bf16[2,2,128,128]{3,2,1,0:T(8,128)(2,1)S(1)}, u32[]{:S(2)}, u32[]{:S(2)}) collective-permute-start(bf16[2,2,128,128]{3,2,1,0:T(8,128)(2,1)S(1)} %pad_maximum_fusion.1.mine), channel_id=1, source_target_pairs={{0,1},{1,0},{2,3},{3,2},{4,5},{5,4},{6,7},{7,6},{8,9},{9,8},{10,11... | collective-permute-start | bytes 393224 | tf_op jit(solution)/shard_map/ppermute | solution.py:310
  15.0 0.9 shard_map.180
  15.9 1.0 shard_map.181
  16.9 1.1 pad_maximum_fusion
  18.0 2.4 %collective-permute-start.6 = (bf16[2,2048,128]{2,1,0:T(8,128)(2,1)}, bf16[2,2048,128]{2,1,0:T(8,128)(2,1)S(1)}, u32[]{:S(2)}, u32[]{:S(2)}) collective-permute-start(bf16[2,2048,128]{2,1,0:T(8,128)(2,1)} %pad_maximum_fusion), channel_id=1, source_target_pairs={{0,1},{1,0},{2,3},{3,2},{4,5},{5,4},{6,7},{7,6},{8,9},{9,8},{10,11... | collective-permute-start | bytes 3145736 | tf_op jit(solution)/shard_map/ppermute | solution.py:310
  20.4 13.2 %all-to-all-start = ((bf16[32,40,128]{2,1,0:T(8,128)(2,1)}), bf16[32,40,128]{2,1,0:T(8,128)(2,1)S(1)}, u32[]{:S(2)}, u32[]{:S(2)}) async-start(bf16[32,40,128]{2,1,0:T(8,128)(2,1)} %bitcast.8), calls=%async_computation | async-start | bytes 655360 | tf_op jit(solution)/shard_map/all_to_all | solution.py:323
  33.6 1.9 %collective-permute-start.7 = (bf16[128,2048]{1,0:T(8,128)(2,1)}, bf16[128,2048]{1,0:T(8,128)(2,1)}, u32[]{:S(2)}, u32[]{:S(2)}) collective-permute-start(bf16[128,2048]{1,0:T(8,128)(2,1)} %bitcast.12.wd), channel_id=1, source_target_pairs={{0,1},{1,0},{2,3},{3,2},{4,5},{5,4},{6,7},{7,6},{8,9},{9,8},{10,11... | collective-permute-start | bytes 1572872 | tf_op jit(solution)/shard_map/ppermute | solution.py:310
  35.5 12.4 %all-to-all-done = bf16[32,40,128]{2,1,0:T(8,128)(2,1)S(1)} async-done(((bf16[32,40,128]{2,1,0:T(8,128)(2,1)}), bf16[32,40,128]{2,1,0:T(8,128)(2,1)S(1)}, u32[]{:S(2)}, u32[]{:S(2)}) %all-to-all-start) | async-done | bytes 327712 | tf_op jit(solution)/shard_map/all_to_all | solution.py:323
  48.8 3.0 %collective-permute-start.3 = (bf16[2,4,160,128]{3,2,1,0:T(8,128)(2,1)S(1)}, bf16[2,4,160,128]{3,2,1,0:T(8,128)(2,1)S(1)}, u32[]{:S(2)}, u32[]{:S(2)}) collective-permute-start(bf16[2,4,160,128]{3,2,1,0:T(8,128)(2,1)S(1)} %get-tuple-element.35.both), channel_id=1, source_target_pairs={{0,14},{2,0},{4,2},{6,4},{8,6},{10,8},{12,10},{14,12},{1,15},{3,1}... | collective-permute-start | bytes 983048 | tf_op jit(solution)/shard_map/ppermute | solution.py:307
  51.7 3.5 %collective-permute-start.2 = (bf16[2,4,160,128]{3,2,1,0:T(8,128)(2,1)S(1)}, bf16[2,4,160,128]{3,2,1,0:T(8,128)(2,1)S(1)}, u32[]{:S(2)}, u32[]{:S(2)}) collective-permute-start(bf16[2,4,160,128]{3,2,1,0:T(8,128)(2,1)S(1)} %get-tuple-element.35.both), channel_id=1, source_target_pairs={{0,2},{2,4},{4,6},{6,8},{8,10},{10,12},{12,14},{14,0},{1,3},{3,5},... | collective-permute-start | bytes 983048 | tf_op jit(solution)/shard_map/ppermute | solution.py:307
  55.2 6.9 %collective-permute-start.5 = (bf16[4,160,128]{2,1,0:T(8,128)(2,1)}, bf16[4,160,128]{2,1,0:T(8,128)(2,1)S(1)}, u32[]{:S(2)}, u32[]{:S(2)}) collective-permute-start(bf16[4,160,128]{2,1,0:T(8,128)(2,1)} %get-tuple-element.36), channel_id=1, source_target_pairs={{0,12},{2,14},{4,0},{6,2},{8,4},{10,6},{12,8},{14,10},{1,13},{3,15... | collective-permute-start | bytes 491528 | tf_op jit(solution)/shard_map/ppermute | solution.py:307
  62.1 1.9 %collective-permute-start.4 = (bf16[4,160,128]{2,1,0:T(8,128)(2,1)}, bf16[4,160,128]{2,1,0:T(8,128)(2,1)S(1)}, u32[]{:S(2)}, u32[]{:S(2)}) collective-permute-start(bf16[4,160,128]{2,1,0:T(8,128)(2,1)} %get-tuple-element.36), channel_id=1, source_target_pairs={{0,4},{2,6},{4,8},{6,10},{8,12},{10,14},{12,0},{14,2},{1,5},{3,7},... | collective-permute-start | bytes 491528 | tf_op jit(solution)/shard_map/ppermute | solution.py:307
  64.0 2.5 %collective-permute-done.5.b2 = bf16[4,160,128]{2,1,0:T(8,128)(2,1)S(1)} collective-permute-done((bf16[4,160,128]{2,1,0:T(8,128)(2,1)}, bf16[4,160,128]{2,1,0:T(8,128)(2,1)S(1)}, u32[]{:S(2)}, u32[]{:S(2)}) %collective-permute-start.5) | collective-permute-done | bytes 163872 | tf_op jit(solution)/shard_map/ppermute | solution.py:307
  66.5 6.8 %collective-permute-done.4.f2 = bf16[4,160,128]{2,1,0:T(8,128)(2,1)S(1)} collective-permute-done((bf16[4,160,128]{2,1,0:T(8,128)(2,1)}, bf16[4,160,128]{2,1,0:T(8,128)(2,1)S(1)}, u32[]{:S(2)}, u32[]{:S(2)}) %collective-permute-start.4) | collective-permute-done | bytes 163872 | tf_op jit(solution)/shard_map/ppermute | solution.py:307
  73.3 4.1 %shard_map.183 = (bf16[160,512]{1,0:T(8,128)(2,1)}, bf16[160,256]{1,0:T(8,128)(2,1)}, bf16[8,2,160,128]{3,2,1,0:T(8,128)(2,1)}) custom-call(s32[1]{0:T(128)} %bitcast.chip, bf16[2,4,160,128]{3,2,1,0:T(8,128)(2,1)S(1)} %get-tuple-element.35.both, bf16[2,4,160,128]{3,2,1,0:T(8,128)(2,1)S(1)} %collective-permute-done.2.f1, ...), custom_call_target="tpu_custom_call" | custom-call | tf_op jit(solution)/shard_map/pallas_call | solution.py:31
  77.4 4.0 %all-to-all-start.1 = ((bf16[16,160,128]{2,1,0:T(8,128)(2,1)}), bf16[16,160,128]{2,1,0:T(8,128)(2,1)S(1)}, u32[]{:S(2)}, u32[]{:S(2)}) async-start(bf16[16,160,128]{2,1,0:T(8,128)(2,1)} %bitcast.29), calls=%async_computation.1 | async-start | bytes 1310720 | tf_op jit(solution)/shard_map/all_to_all | solution.py:345
  81.4 16.5 %all-to-all-done.1 = bf16[16,160,128]{2,1,0:T(8,128)(2,1)S(1)} async-done(((bf16[16,160,128]{2,1,0:T(8,128)(2,1)}), bf16[16,160,128]{2,1,0:T(8,128)(2,1)S(1)}, u32[]{:S(2)}, u32[]{:S(2)}) %all-to-all-start.1) | async-done | bytes 655392 | tf_op jit(solution)/shard_map/all_to_all | solution.py:345
  97.9 1.0 shard_map.185
  99.0 5.2 %all-to-all-start.2 = ((bf16[32,16,128]{2,1,0:T(8,128)(2,1)}), bf16[32,16,128]{2,1,0:T(8,128)(2,1)S(1)}, u32[]{:S(2)}, u32[]{:S(2)}) async-start(bf16[32,16,128]{2,1,0:T(8,128)(2,1)} %bitcast.17), calls=%async_computation.2 | async-start | bytes 262144 | tf_op jit(solution)/shard_map/all_to_all | solution.py:347
  105.4 2.7 %shard_map.184 = (bf16[2,2048,128]{2,1,0:T(8,128)(2,1)}, bf16[2,2048,128]{2,1,0:T(8,128)(2,1)}, bf16[128,2048]{1,0:T(8,128)(2,1)}, bf16[128,2048]{1,0:T(8,128)(2,1)}) custom-call(s32[1]{0:T(128)} %bitcast.chip, bf16[2,4,160,128]{3,2,1,0:T(8,128)(2,1)S(1)} %get-tuple-element.35.both, bf16[2,4,160,128]{3,2,1,0:T(8,128)(2,1)S(1)} %collective-permute-done.2.f1, ...), custom_call_target="tpu_custom_call" | custom-call | tf_op jit(solution)/shard_map/pallas_call | solution.py:31
  108.1 2.0 %collective-permute-start.9 = (bf16[128,2048]{1,0:T(8,128)(2,1)}, bf16[128,2048]{1,0:T(8,128)(2,1)S(1)}, u32[]{:S(2)}, u32[]{:S(2)}) collective-permute-start(bf16[128,2048]{1,0:T(8,128)(2,1)} %get-tuple-element.45), channel_id=1, source_target_pairs={{0,1},{1,0},{2,3},{3,2},{4,5},{5,4},{6,7},{7,6},{8,9},{9,8},{10,11... | collective-permute-start | bytes 1572872 | tf_op jit(solution)/shard_map/ppermute | solution.py:310
  110.1 2.4 %collective-permute-start.8 = (bf16[2,2048,128]{2,1,0:T(8,128)(2,1)}, bf16[2,2048,128]{2,1,0:T(8,128)(2,1)S(1)}, u32[]{:S(2)}, u32[]{:S(2)}) collective-permute-start(bf16[2,2048,128]{2,1,0:T(8,128)(2,1)} %get-tuple-element.43), channel_id=1, source_target_pairs={{0,1},{1,0},{2,3},{3,2},{4,5},{5,4},{6,7},{7,6},{8,9},{9,8},{10,11... | collective-permute-start | bytes 3145736 | tf_op jit(solution)/shard_map/ppermute | solution.py:310
  112.5 2.5 %all-to-all-done.2 = bf16[32,16,128]{2,1,0:T(8,128)(2,1)S(1)} async-done(((bf16[32,16,128]{2,1,0:T(8,128)(2,1)}), bf16[32,16,128]{2,1,0:T(8,128)(2,1)S(1)}, u32[]{:S(2)}, u32[]{:S(2)}) %all-to-all-start.2) | async-done | bytes 131104 | tf_op jit(solution)/shard_map/all_to_all | solution.py:347
  115.2 17.6 %all_gather.3.mix = bf16[128,2048]{1,0:T(8,128)(2,1)S(1)} all-gather(bf16[128,128]{1,0:T(8,128)(2,1)S(1)} %fusion), channel_id=1, replica_groups=mesh['z'=8,'x'=4,'y'=8,'c'=2] {'y','c'}, dimensions={1}, use_global_device_ids=true | all-gather | bytes 557056 | tf_op jit(solution)/shard_map/all_gather | solution.py:354
  132.9 1.3 shard_map.186
  134.2 8.2 %all-to-all-start.3 = ((bf16[32,72,128]{2,1,0:T(8,128)(2,1)}), bf16[32,72,128]{2,1,0:T(8,128)(2,1)S(1)}, u32[]{:S(2)}, u32[]{:S(2)}) async-start(bf16[32,72,128]{2,1,0:T(8,128)(2,1)} %get-tuple-element.50), calls=%async_computation.3 | async-start | bytes 1179648 | tf_op jit(solution)/shard_map/all_to_all | solution.py:357
  142.5 0.9 fusion.1
  143.9 1.2 add_convert_fusion.1
  145.1 16.8 %all-to-all-done.3.last = bf16[32,72,128]{2,1,0:T(8,128)(2,1)S(1)} async-done(((bf16[32,72,128]{2,1,0:T(8,128)(2,1)}), bf16[32,72,128]{2,1,0:T(8,128)(2,1)S(1)}, u32[]{:S(2)}, u32[]{:S(2)}) %all-to-all-start.3) | async-done | bytes 589856 | tf_op jit(solution)/shard_map/all_to_all | solution.py:357
  (46 shorter events, 4.8 us)
Async XLA Ops:
  0.6 16.3 %copy-start.1 = (bf16[1,2048,128]{2,1,0:T(8,128)(2,1)S(1)}, bf16[1,2048,128]{2,1,0:T(8,128)(2,1)}, u32[]{:S(2)}) copy-start(bf16[1,2048,128]{2,1,0:T(8,128)(2,1)} %param.17) | copy-start | bytes 1572868
  1.5 15.4 %copy-start = (bf16[1,2048,128]{2,1,0:T(8,128)(2,1)S(1)}, bf16[1,2048,128]{2,1,0:T(8,128)(2,1)}, u32[]{:S(2)}) copy-start(bf16[1,2048,128]{2,1,0:T(8,128)(2,1)} %param.18) | copy-start | bytes 1572868
  1.5 10.2 %collective-permute-start = (bf16[2,128,128]{2,1,0:T(8,128)(2,1)S(1)}, bf16[2,128,128]{2,1,0:T(8,128)(2,1)S(1)}, u32[]{:S(2)}, u32[]{:S(2)}) collective-permute-start(bf16[2,128,128]{2,1,0:T(8,128)(2,1)S(1)} %get-tuple-element.63), channel_id=1, source_target_pairs={{0,8},{2,10},{4,12},{6,14},{8,0},{10,2},{12,4},{14,6},{1,9},{3,11}... | collective-permute-start | bytes 196616 | tf_op jit(solution)/shard_map/ppermute | solution.py:307
  11.7 4.2 %collective-permute-start.1 = (bf16[2,2,128,128]{3,2,1,0:T(8,128)(2,1)S(1)}, bf16[2,2,128,128]{3,2,1,0:T(8,128)(2,1)S(1)}, u32[]{:S(2)}, u32[]{:S(2)}) collective-permute-start(bf16[2,2,128,128]{3,2,1,0:T(8,128)(2,1)S(1)} %pad_maximum_fusion.1.mine), channel_id=1, source_target_pairs={{0,1},{1,0},{2,3},{3,2},{4,5},{5,4},{6,7},{7,6},{8,9},{9,8},{10,11... | collective-permute-start | bytes 393224 | tf_op jit(solution)/shard_map/ppermute | solution.py:310
  13.7 0.7 copy-start.5
  14.3 0.7 copy-start.6
  18.0 55.3 %collective-permute-start.6 = (bf16[2,2048,128]{2,1,0:T(8,128)(2,1)}, bf16[2,2048,128]{2,1,0:T(8,128)(2,1)S(1)}, u32[]{:S(2)}, u32[]{:S(2)}) collective-permute-start(bf16[2,2048,128]{2,1,0:T(8,128)(2,1)} %pad_maximum_fusion), channel_id=1, source_target_pairs={{0,1},{1,0},{2,3},{3,2},{4,5},{5,4},{6,7},{7,6},{8,9},{9,8},{10,11... | collective-permute-start | bytes 3145736 | tf_op jit(solution)/shard_map/ppermute | solution.py:310
  20.4 27.6 %all-to-all-start = ((bf16[32,40,128]{2,1,0:T(8,128)(2,1)}), bf16[32,40,128]{2,1,0:T(8,128)(2,1)S(1)}, u32[]{:S(2)}, u32[]{:S(2)}) async-start(bf16[32,40,128]{2,1,0:T(8,128)(2,1)} %bitcast.8), calls=%async_computation | async-start | bytes 655360 | tf_op jit(solution)/shard_map/all_to_all | solution.py:323
  33.6 28.5 %collective-permute-start.7 = (bf16[128,2048]{1,0:T(8,128)(2,1)}, bf16[128,2048]{1,0:T(8,128)(2,1)}, u32[]{:S(2)}, u32[]{:S(2)}) collective-permute-start(bf16[128,2048]{1,0:T(8,128)(2,1)} %bitcast.12.wd), channel_id=1, source_target_pairs={{0,1},{1,0},{2,3},{3,2},{4,5},{5,4},{6,7},{7,6},{8,9},{9,8},{10,11... | collective-permute-start | bytes 1572872 | tf_op jit(solution)/shard_map/ppermute | solution.py:310
  48.8 24.5 %collective-permute-start.3 = (bf16[2,4,160,128]{3,2,1,0:T(8,128)(2,1)S(1)}, bf16[2,4,160,128]{3,2,1,0:T(8,128)(2,1)S(1)}, u32[]{:S(2)}, u32[]{:S(2)}) collective-permute-start(bf16[2,4,160,128]{3,2,1,0:T(8,128)(2,1)S(1)} %get-tuple-element.35.both), channel_id=1, source_target_pairs={{0,14},{2,0},{4,2},{6,4},{8,6},{10,8},{12,10},{14,12},{1,15},{3,1}... | collective-permute-start | bytes 983048 | tf_op jit(solution)/shard_map/ppermute | solution.py:307
  51.7 21.6 %collective-permute-start.2 = (bf16[2,4,160,128]{3,2,1,0:T(8,128)(2,1)S(1)}, bf16[2,4,160,128]{3,2,1,0:T(8,128)(2,1)S(1)}, u32[]{:S(2)}, u32[]{:S(2)}) collective-permute-start(bf16[2,4,160,128]{3,2,1,0:T(8,128)(2,1)S(1)} %get-tuple-element.35.both), channel_id=1, source_target_pairs={{0,2},{2,4},{4,6},{6,8},{8,10},{10,12},{12,14},{14,0},{1,3},{3,5},... | collective-permute-start | bytes 983048 | tf_op jit(solution)/shard_map/ppermute | solution.py:307
  55.2 11.3 %collective-permute-start.5 = (bf16[4,160,128]{2,1,0:T(8,128)(2,1)}, bf16[4,160,128]{2,1,0:T(8,128)(2,1)S(1)}, u32[]{:S(2)}, u32[]{:S(2)}) collective-permute-start(bf16[4,160,128]{2,1,0:T(8,128)(2,1)} %get-tuple-element.36), channel_id=1, source_target_pairs={{0,12},{2,14},{4,0},{6,2},{8,4},{10,6},{12,8},{14,10},{1,13},{3,15... | collective-permute-start | bytes 491528 | tf_op jit(solution)/shard_map/ppermute | solution.py:307
  62.1 11.2 %collective-permute-start.4 = (bf16[4,160,128]{2,1,0:T(8,128)(2,1)}, bf16[4,160,128]{2,1,0:T(8,128)(2,1)S(1)}, u32[]{:S(2)}, u32[]{:S(2)}) collective-permute-start(bf16[4,160,128]{2,1,0:T(8,128)(2,1)} %get-tuple-element.36), channel_id=1, source_target_pairs={{0,4},{2,6},{4,8},{6,10},{8,12},{10,14},{12,0},{14,2},{1,5},{3,7},... | collective-permute-start | bytes 491528 | tf_op jit(solution)/shard_map/ppermute | solution.py:307
  77.4 4.0 %copy-start.15 = (f32[128]{0:T(128)S(1)}, f32[128]{0:T(128)}, u32[]{:S(2)}) copy-start(f32[128]{0:T(128)} %param.25) | copy-start | bytes 1540
  77.4 20.6 %all-to-all-start.1 = ((bf16[16,160,128]{2,1,0:T(8,128)(2,1)}), bf16[16,160,128]{2,1,0:T(8,128)(2,1)S(1)}, u32[]{:S(2)}, u32[]{:S(2)}) async-start(bf16[16,160,128]{2,1,0:T(8,128)(2,1)} %bitcast.29), calls=%async_computation.1 | async-start | bytes 1310720 | tf_op jit(solution)/shard_map/all_to_all | solution.py:345
  99.0 5.3 %copy-start.11 = (bf16[128,128]{1,0:T(8,128)(2,1)S(1)}, bf16[128,128]{1,0:T(8,128)(2,1)}, u32[]{:S(2)}) copy-start(bf16[128,128]{1,0:T(8,128)(2,1)} %param.22) | copy-start | bytes 98308
  99.0 5.3 %copy-start.12 = (bf16[128,128]{1,0:T(8,128)(2,1)S(1)}, bf16[128,128]{1,0:T(8,128)(2,1)}, u32[]{:S(2)}) copy-start(bf16[128,128]{1,0:T(8,128)(2,1)} %param.21) | copy-start | bytes 98308
  99.0 5.3 %copy-start.13 = (bf16[128,128]{1,0:T(8,128)(2,1)S(1)}, bf16[128,128]{1,0:T(8,128)(2,1)}, u32[]{:S(2)}) copy-start(bf16[128,128]{1,0:T(8,128)(2,1)} %param.24) | copy-start | bytes 98308
  99.0 5.3 %copy-start.14 = (bf16[128,128]{1,0:T(8,128)(2,1)S(1)}, bf16[128,128]{1,0:T(8,128)(2,1)}, u32[]{:S(2)}) copy-start(bf16[128,128]{1,0:T(8,128)(2,1)} %param.23) | copy-start | bytes 98308
  99.0 16.0 %all-to-all-start.2 = ((bf16[32,16,128]{2,1,0:T(8,128)(2,1)}), bf16[32,16,128]{2,1,0:T(8,128)(2,1)S(1)}, u32[]{:S(2)}, u32[]{:S(2)}) async-start(bf16[32,16,128]{2,1,0:T(8,128)(2,1)} %bitcast.17), calls=%async_computation.2 | async-start | bytes 262144 | tf_op jit(solution)/shard_map/all_to_all | solution.py:347
  104.4 0.9 copy-start.3
  104.4 1.0 copy-start.4
  105.4 9.6 %copy-start.9 = (bf16[512,128]{1,0:T(8,128)(2,1)S(1)}, bf16[512,128]{1,0:T(8,128)(2,1)}, u32[]{:S(2)}) copy-start(bf16[512,128]{1,0:T(8,128)(2,1)} %get-tuple-element.48) | copy-start | bytes 393220
  105.4 9.6 %copy-start.10 = (bf16[128,128]{1,0:T(8,128)(2,1)S(1)}, bf16[128,128]{1,0:T(8,128)(2,1)}, u32[]{:S(2)}) copy-start(bf16[128,128]{1,0:T(8,128)(2,1)} %param.14) | copy-start | bytes 98308
  108.1 24.8 %copy-start.2 = (bf16[128,2048]{1,0:T(8,128)(2,1)S(1)}, bf16[128,2048]{1,0:T(8,128)(2,1)}, u32[]{:S(2)}) copy-start(bf16[128,2048]{1,0:T(8,128)(2,1)} %out_proj.1) | copy-start | bytes 1572868
  108.1 34.4 %collective-permute-start.9 = (bf16[128,2048]{1,0:T(8,128)(2,1)}, bf16[128,2048]{1,0:T(8,128)(2,1)S(1)}, u32[]{:S(2)}, u32[]{:S(2)}) collective-permute-start(bf16[128,2048]{1,0:T(8,128)(2,1)} %get-tuple-element.45), channel_id=1, source_target_pairs={{0,1},{1,0},{2,3},{3,2},{4,5},{5,4},{6,7},{7,6},{8,9},{9,8},{10,11... | collective-permute-start | bytes 1572872 | tf_op jit(solution)/shard_map/ppermute | solution.py:310
  110.1 33.3 %collective-permute-start.8 = (bf16[2,2048,128]{2,1,0:T(8,128)(2,1)}, bf16[2,2048,128]{2,1,0:T(8,128)(2,1)S(1)}, u32[]{:S(2)}, u32[]{:S(2)}) collective-permute-start(bf16[2,2048,128]{2,1,0:T(8,128)(2,1)} %get-tuple-element.43), channel_id=1, source_target_pairs={{0,1},{1,0},{2,3},{3,2},{4,5},{5,4},{6,7},{7,6},{8,9},{9,8},{10,11... | collective-permute-start | bytes 3145736 | tf_op jit(solution)/shard_map/ppermute | solution.py:310
  134.2 8.3 %copy-start.8 = (bf16[128,2048]{1,0:T(8,128)(2,1)S(1)}, bf16[128,2048]{1,0:T(8,128)(2,1)}, u32[]{:S(2)}) copy-start(bf16[128,2048]{1,0:T(8,128)(2,1)} %get-tuple-element.44) | copy-start | bytes 1572868
  134.2 27.7 %all-to-all-start.3 = ((bf16[32,72,128]{2,1,0:T(8,128)(2,1)}), bf16[32,72,128]{2,1,0:T(8,128)(2,1)S(1)}, u32[]{:S(2)}, u32[]{:S(2)}) async-start(bf16[32,72,128]{2,1,0:T(8,128)(2,1)} %get-tuple-element.50), calls=%async_computation.3 | async-start | bytes 1179648 | tf_op jit(solution)/shard_map/all_to_all | solution.py:357
  142.5 1.4 copy-start.7

commit v5 on v4

--- a/solution.py
+++ b/solution.py
@@ -99,7 +99,7 @@
     total = choose.shape[0] * 8
     out = (whole((total, fw), BF16),)
     scratch = [pltpu.VMEM((total, fw), F32)]
-    return call(fill_body, out, core, choose, scale, mine, peer, scalars=1, scratch=scratch)
+    return call(fill_body, out, core, choose, scale, mine, peer, scalars=1, scratch=scratch, kept=(0,))
 
 
 def sort_body(recv, both, near, rows):
@@ -316,13 +316,15 @@
     pick, choose, scale = route_slots(core, routes.T, route_weight.T, n_sp, half)
     send = fill_slots(core, choose, scale, mine, peer)
 
-    send, late_gate, late_up, late_down = lax.optimization_barrier((send, gate_w, up_w, down_w))
+    recv = lax.all_to_all(send.reshape(n_sp, -1, fw), SP, 0, 0, tiled=True).reshape(send.shape)
+    both, near = sort_pieces(recv)
+
+    near, late_gate, late_up, late_down = lax.optimization_barrier((near, gate_w, up_w, down_w))
     wgu = jnp.concatenate([late_gate, late_up], axis=0)
     wgu_peer = over_cores(wgu)
     wd_peer = over_cores(late_down[0])
-    recv = lax.all_to_all(send.reshape(n_sp, -1, fw), SP, 0, 0, tiled=True).reshape(send.shape)
-    both, near = sort_pieces(recv)
-    blocks = (both, over_y(both, 1), over_y(both, -1), over_y(near, 2), over_y(near, -2))
+    first = (both, over_y(both, 1), over_y(both, -1))
+    blocks = (*first, over_y(near, 2), over_y(near, -2))
 
     gu_grad, hidden, part = expert_rows_grad(
         chip, blocks, wgu_peer, late_gate[0], late_up[0], late_down[0], wd_peer, n_y

time: 164 us -> 168 us (1.024)
  blocking collectives: 17.6 us -> 45.5 us
  starting transfers between devices: 63.5 us -> 48.7 us
  waiting for transfers between devices: 60.8 us -> 53.9 us
    all_to_all x0 -> x1, blocking collectives: none -> 27.9 us  [per_device(): lax.all_to_all(send.reshape(n_sp, -1, fw), SP, 0, 0, tiled=True)]
    all_to_all x1 -> x0, starting transfers between devices: 13.2 us -> none  [per_device(): lax.all_to_all(send.reshape(n_sp, -1, fw), SP, 0, 0, tiled=True)]
    all_to_all x1 -> x0, waiting for transfers between devices: 12.4 us -> none  [per_device(): lax.all_to_all(send.reshape(n_sp, -1, fw), SP, 0, 0, tiled=True)]
    ppermute x5, waiting for transfers between devices: 12.5 us -> 17.9 us  [over_y(): return lax.ppermute(v, 'y', [(i, (i + step) % n_y) for i in range(n_y)])]
  transfers between devices with their start and end apart: 14 -> 13, of which waited for: 7 -> 6; matrix products, arithmetic and copies ran while one was open for 2% -> 2% of each run, Pallas kernels for 3% -> 3%
where the time goes in v5:
time: 168 us; the launch traced here: 167 us
  waiting for transfers between devices  53.9 us (32%)
  starting transfers between devices  48.7 us (29%)
  blocking collectives  45.5 us (27%)
  Pallas kernels  11.9 us (7%)
  other arithmetic  4.24 us (3%)
  local copies, waits for them, and re-layouts  2.09 us (1%)
    all_to_all x1, blocking collectives, per_device(): lax.all_to_all(send.reshape(n_sp, -1, fw), SP, 0, 0, tiled=True)  27.9 us
    ppermute x5, starting transfers between devices, over_y(): return lax.ppermute(v, 'y', [(i, (i + step) % n_y) for i in range(n_y)])  20.8 us
    ppermute x5, waiting for transfers between devices, over_y(): return lax.ppermute(v, 'y', [(i, (i + step) % n_y) for i in range(n_y)])  17.9 us
    all_gather x1, blocking collectives, per_device(): mix_grad = lax.all_gather(own_grad, TP, axis=1, tiled=True)  17.6 us
    all_to_all x1, waiting for transfers between devices, per_device(): last = lax.all_to_all(last, SP, 0, 0, tiled=True)  16.8 us
    all_to_all x1, waiting for transfers between devices, per_device(): lax.all_to_all(part.reshape(2 * n_y, *part.shape[2:]), TP, 0, 0, tiled=True)  16.5 us
    pallas_call x8, Pallas kernels, call(): pl.pallas_call(body, out_shape=tuple(outs), in_specs=[SMEM] * scalars + [...  11.9 us
    ppermute x5, starting transfers between devices, over_cores(): return lax.ppermute(v, 'c', [(0, 1), (1, 0)])  10.7 us
  transfers between devices with their start and end apart: 13, of which 6 were waited for; matrix products, arithmetic and copies ran while one was open for 2% of the time, Pallas kernels for 3%

profile of v5, /device:TPU:8, one launch (start us, length us, event | category | flops | bytes accessed | tf_op | source)
XLA Modules:
  0.0 167.4 jit_solution(3080697607561666892)
XLA Ops:
  1.4 6.8 %collective-permute-start = (bf16[2,128,128]{2,1,0:T(8,128)(2,1)S(1)}, bf16[2,128,128]{2,1,0:T(8,128)(2,1)S(1)}, u32[]{:S(2)}, u32[]{:S(2)}) collective-permute-start(bf16[2,128,128]{2,1,0:T(8,128)(2,1)S(1)} %get-tuple-element.63), channel_id=1, source_target_pairs={{0,8},{2,10},{4,12},{6,14},{8,0},{10,2},{12,4},{14,6},{1,9},{3,11}... | collective-permute-start | bytes 196616 | tf_op jit(solution)/shard_map/ppermute | solution.py:307
  8.3 3.2 %collective-permute-done = bf16[2,128,128]{2,1,0:T(8,128)(2,1)S(1)} collective-permute-done((bf16[2,128,128]{2,1,0:T(8,128)(2,1)S(1)}, bf16[2,128,128]{2,1,0:T(8,128)(2,1)S(1)}, u32[]{:S(2)}, u32[]{:S(2)}) %collective-permute-start) | collective-permute-done | bytes 65568 | tf_op jit(solution)/shard_map/ppermute | solution.py:307
  11.5 1.9 %collective-permute-start.1 = (bf16[2,2,128,128]{3,2,1,0:T(8,128)(2,1)S(1)}, bf16[2,2,128,128]{3,2,1,0:T(8,128)(2,1)S(1)}, u32[]{:S(2)}, u32[]{:S(2)}) collective-permute-start(bf16[2,2,128,128]{3,2,1,0:T(8,128)(2,1)S(1)} %pad_maximum_fusion.1.mine), channel_id=1, source_target_pairs={{0,1},{1,0},{2,3},{3,2},{4,5},{5,4},{6,7},{7,6},{8,9},{9,8},{10,11... | collective-permute-start | bytes 393224 | tf_op jit(solution)/shard_map/ppermute | solution.py:310
  14.1 0.9 shard_map.180
  15.3 27.9 %all_to_all.20 = bf16[32,40,128]{2,1,0:T(8,128)(2,1)S(1)} all-to-all(bf16[32,40,128]{2,1,0:T(8,128)(2,1)S(1)} %bitcast.26), channel_id=1, replica_groups=mesh['z'=8,'x'=4,'y'=8,'c'=2] {'z','x'}, dimensions={0} | all-to-all | bytes 655360 | tf_op jit(solution)/shard_map/all_to_all | solution.py:319
  43.2 0.8 shard_map.182
  44.0 1.1 pad_maximum_fusion
  45.1 1.9 %collective-permute-start.6 = (bf16[2,2048,128]{2,1,0:T(8,128)(2,1)}, bf16[2,2048,128]{2,1,0:T(8,128)(2,1)S(1)}, u32[]{:S(2)}, u32[]{:S(2)}) collective-permute-start(bf16[2,2048,128]{2,1,0:T(8,128)(2,1)} %pad_maximum_fusion), channel_id=1, source_target_pairs={{0,1},{1,0},{2,3},{3,2},{4,5},{5,4},{6,7},{7,6},{8,9},{9,8},{10,11... | collective-permute-start | bytes 3145736 | tf_op jit(solution)/shard_map/ppermute | solution.py:310
  47.0 2.4 %collective-permute-start.7 = (bf16[128,2048]{1,0:T(8,128)(2,1)}, bf16[128,2048]{1,0:T(8,128)(2,1)}, u32[]{:S(2)}, u32[]{:S(2)}) collective-permute-start(bf16[128,2048]{1,0:T(8,128)(2,1)} %bitcast.12.wd), channel_id=1, source_target_pairs={{0,1},{1,0},{2,3},{3,2},{4,5},{5,4},{6,7},{7,6},{8,9},{9,8},{10,11... | collective-permute-start | bytes 1572872 | tf_op jit(solution)/shard_map/ppermute | solution.py:310
  49.5 6.2 %collective-permute-start.5 = (bf16[4,160,128]{2,1,0:T(8,128)(2,1)}, bf16[4,160,128]{2,1,0:T(8,128)(2,1)S(1)}, u32[]{:S(2)}, u32[]{:S(2)}) collective-permute-start(bf16[4,160,128]{2,1,0:T(8,128)(2,1)} %get-tuple-element.36), channel_id=1, source_target_pairs={{0,12},{2,14},{4,0},{6,2},{8,4},{10,6},{12,8},{14,10},{1,13},{3,15... | collective-permute-start | bytes 491528 | tf_op jit(solution)/shard_map/ppermute | solution.py:307
  55.7 3.0 %collective-permute-start.3 = (bf16[2,4,160,128]{3,2,1,0:T(8,128)(2,1)S(1)}, bf16[2,4,160,128]{3,2,1,0:T(8,128)(2,1)S(1)}, u32[]{:S(2)}, u32[]{:S(2)}) collective-permute-start(bf16[2,4,160,128]{3,2,1,0:T(8,128)(2,1)S(1)} %get-tuple-element.34.both), channel_id=1, source_target_pairs={{0,14},{2,0},{4,2},{6,4},{8,6},{10,8},{12,10},{14,12},{1,15},{3,1}... | collective-permute-start | bytes 983048 | tf_op jit(solution)/shard_map/ppermute | solution.py:307
  58.7 2.9 %collective-permute-start.2 = (bf16[2,4,160,128]{3,2,1,0:T(8,128)(2,1)S(1)}, bf16[2,4,160,128]{3,2,1,0:T(8,128)(2,1)S(1)}, u32[]{:S(2)}, u32[]{:S(2)}) collective-permute-start(bf16[2,4,160,128]{3,2,1,0:T(8,128)(2,1)S(1)} %get-tuple-element.34.both), channel_id=1, source_target_pairs={{0,2},{2,4},{4,6},{6,8},{8,10},{10,12},{12,14},{14,0},{1,3},{3,5},... | collective-permute-start | bytes 983048 | tf_op jit(solution)/shard_map/ppermute | solution.py:307
  61.6 2.4 %collective-permute-done.5.b2 = bf16[4,160,128]{2,1,0:T(8,128)(2,1)S(1)} collective-permute-done((bf16[4,160,128]{2,1,0:T(8,128)(2,1)}, bf16[4,160,128]{2,1,0:T(8,128)(2,1)S(1)}, u32[]{:S(2)}, u32[]{:S(2)}) %collective-permute-start.5) | collective-permute-done | bytes 163872 | tf_op jit(solution)/shard_map/ppermute | solution.py:307
  64.0 1.9 %collective-permute-start.4 = (bf16[4,160,128]{2,1,0:T(8,128)(2,1)}, bf16[4,160,128]{2,1,0:T(8,128)(2,1)S(1)}, u32[]{:S(2)}, u32[]{:S(2)}) collective-permute-start(bf16[4,160,128]{2,1,0:T(8,128)(2,1)} %get-tuple-element.36), channel_id=1, source_target_pairs={{0,4},{2,6},{4,8},{6,10},{8,12},{10,14},{12,0},{14,2},{1,5},{3,7},... | collective-permute-start | bytes 491528 | tf_op jit(solution)/shard_map/ppermute | solution.py:307
  65.9 12.2 %collective-permute-done.4.f2 = bf16[4,160,128]{2,1,0:T(8,128)(2,1)S(1)} collective-permute-done((bf16[4,160,128]{2,1,0:T(8,128)(2,1)}, bf16[4,160,128]{2,1,0:T(8,128)(2,1)S(1)}, u32[]{:S(2)}, u32[]{:S(2)}) %collective-permute-start.4) | collective-permute-done | bytes 163872 | tf_op jit(solution)/shard_map/ppermute | solution.py:307
  78.2 4.1 %shard_map.183 = (bf16[160,512]{1,0:T(8,128)(2,1)}, bf16[160,256]{1,0:T(8,128)(2,1)}, bf16[8,2,160,128]{3,2,1,0:T(8,128)(2,1)}) custom-call(s32[1]{0:T(128)} %bitcast.chip, bf16[2,4,160,128]{3,2,1,0:T(8,128)(2,1)S(1)} %get-tuple-element.34.both, bf16[2,4,160,128]{3,2,1,0:T(8,128)(2,1)S(1)} %collective-permute-done.2.f1, ...), custom_call_target="tpu_custom_call" | custom-call | tf_op jit(solution)/shard_map/pallas_call | solution.py:31
  82.3 4.7 %all-to-all-start.1 = ((bf16[16,160,128]{2,1,0:T(8,128)(2,1)}), bf16[16,160,128]{2,1,0:T(8,128)(2,1)S(1)}, u32[]{:S(2)}, u32[]{:S(2)}) async-start(bf16[16,160,128]{2,1,0:T(8,128)(2,1)} %bitcast.30), calls=%async_computation.1 | async-start | bytes 1310720 | tf_op jit(solution)/shard_map/all_to_all | solution.py:347
  86.9 16.5 %all-to-all-done.1 = bf16[16,160,128]{2,1,0:T(8,128)(2,1)S(1)} async-done(((bf16[16,160,128]{2,1,0:T(8,128)(2,1)}), bf16[16,160,128]{2,1,0:T(8,128)(2,1)S(1)}, u32[]{:S(2)}, u32[]{:S(2)}) %all-to-all-start.1) | async-done | bytes 655392 | tf_op jit(solution)/shard_map/all_to_all | solution.py:347
  103.4 1.1 shard_map.185
  104.5 4.2 %all-to-all-start.2 = ((bf16[32,16,128]{2,1,0:T(8,128)(2,1)}), bf16[32,16,128]{2,1,0:T(8,128)(2,1)S(1)}, u32[]{:S(2)}, u32[]{:S(2)}) async-start(bf16[32,16,128]{2,1,0:T(8,128)(2,1)} %bitcast.17), calls=%async_computation.2 | async-start | bytes 262144 | tf_op jit(solution)/shard_map/all_to_all | solution.py:349
  108.9 0.8 copy-done.3
  109.8 2.7 %shard_map.184 = (bf16[2,2048,128]{2,1,0:T(8,128)(2,1)}, bf16[2,2048,128]{2,1,0:T(8,128)(2,1)}, bf16[128,2048]{1,0:T(8,128)(2,1)}, bf16[128,2048]{1,0:T(8,128)(2,1)}) custom-call(s32[1]{0:T(128)} %bitcast.chip, bf16[2,4,160,128]{3,2,1,0:T(8,128)(2,1)S(1)} %get-tuple-element.34.both, bf16[2,4,160,128]{3,2,1,0:T(8,128)(2,1)S(1)} %collective-permute-done.2.f1, ...), custom_call_target="tpu_custom_call" | custom-call | tf_op jit(solution)/shard_map/pallas_call | solution.py:31
  112.5 2.0 %collective-permute-start.9 = (bf16[128,2048]{1,0:T(8,128)(2,1)}, bf16[128,2048]{1,0:T(8,128)(2,1)S(1)}, u32[]{:S(2)}, u32[]{:S(2)}) collective-permute-start(bf16[128,2048]{1,0:T(8,128)(2,1)} %get-tuple-element.45), channel_id=1, source_target_pairs={{0,1},{1,0},{2,3},{3,2},{4,5},{5,4},{6,7},{7,6},{8,9},{9,8},{10,11... | collective-permute-start | bytes 1572872 | tf_op jit(solution)/shard_map/ppermute | solution.py:310
  114.6 2.4 %collective-permute-start.8 = (bf16[2,2048,128]{2,1,0:T(8,128)(2,1)}, bf16[2,2048,128]{2,1,0:T(8,128)(2,1)S(1)}, u32[]{:S(2)}, u32[]{:S(2)}) collective-permute-start(bf16[2,2048,128]{2,1,0:T(8,128)(2,1)} %get-tuple-element.43), channel_id=1, source_target_pairs={{0,1},{1,0},{2,3},{3,2},{4,5},{5,4},{6,7},{7,6},{8,9},{9,8},{10,11... | collective-permute-start | bytes 3145736 | tf_op jit(solution)/shard_map/ppermute | solution.py:310
  117.0 2.6 %all-to-all-done.2 = bf16[32,16,128]{2,1,0:T(8,128)(2,1)S(1)} async-done(((bf16[32,16,128]{2,1,0:T(8,128)(2,1)}), bf16[32,16,128]{2,1,0:T(8,128)(2,1)S(1)}, u32[]{:S(2)}, u32[]{:S(2)}) %all-to-all-start.2) | async-done | bytes 131104 | tf_op jit(solution)/shard_map/all_to_all | solution.py:349
  119.9 17.6 %all_gather.3.mix = bf16[128,2048]{1,0:T(8,128)(2,1)S(1)} all-gather(bf16[128,128]{1,0:T(8,128)(2,1)S(1)} %fusion), channel_id=1, replica_groups=mesh['z'=8,'x'=4,'y'=8,'c'=2] {'y','c'}, dimensions={1}, use_global_device_ids=true | all-gather | bytes 557056 | tf_op jit(solution)/shard_map/all_gather | solution.py:356
  137.4 1.3 shard_map.186
  138.8 8.4 %all-to-all-start.3 = ((bf16[32,72,128]{2,1,0:T(8,128)(2,1)}), bf16[32,72,128]{2,1,0:T(8,128)(2,1)S(1)}, u32[]{:S(2)}, u32[]{:S(2)}) async-start(bf16[32,72,128]{2,1,0:T(8,128)(2,1)} %get-tuple-element.50), calls=%async_computation.3 | async-start | bytes 1179648 | tf_op jit(solution)/shard_map/all_to_all | solution.py:359
  147.2 0.9 fusion.1
  148.6 1.2 add_convert_fusion.1
  149.8 16.8 %all-to-all-done.3.last = bf16[32,72,128]{2,1,0:T(8,128)(2,1)S(1)} async-done(((bf16[32,72,128]{2,1,0:T(8,128)(2,1)}), bf16[32,72,128]{2,1,0:T(8,128)(2,1)S(1)}, u32[]{:S(2)}, u32[]{:S(2)}) %all-to-all-start.3) | async-done | bytes 589856 | tf_op jit(solution)/shard_map/all_to_all | solution.py:359
  166.6 0.8 shard_map.187
  (45 shorter events, 2.8 us)
Async XLA Ops:
  1.4 10.1 %collective-permute-start = (bf16[2,128,128]{2,1,0:T(8,128)(2,1)S(1)}, bf16[2,128,128]{2,1,0:T(8,128)(2,1)S(1)}, u32[]{:S(2)}, u32[]{:S(2)}) collective-permute-start(bf16[2,128,128]{2,1,0:T(8,128)(2,1)S(1)} %get-tuple-element.63), channel_id=1, source_target_pairs={{0,8},{2,10},{4,12},{6,14},{8,0},{10,2},{12,4},{14,6},{1,9},{3,11}... | collective-permute-start | bytes 196616 | tf_op jit(solution)/shard_map/ppermute | solution.py:307
  11.5 3.5 %collective-permute-start.1 = (bf16[2,2,128,128]{3,2,1,0:T(8,128)(2,1)S(1)}, bf16[2,2,128,128]{3,2,1,0:T(8,128)(2,1)S(1)}, u32[]{:S(2)}, u32[]{:S(2)}) collective-permute-start(bf16[2,2,128,128]{3,2,1,0:T(8,128)(2,1)S(1)} %pad_maximum_fusion.1.mine), channel_id=1, source_target_pairs={{0,1},{1,0},{2,3},{3,2},{4,5},{5,4},{6,7},{7,6},{8,9},{9,8},{10,11... | collective-permute-start | bytes 393224 | tf_op jit(solution)/shard_map/ppermute | solution.py:310
  13.4 0.7 copy-start.6
  13.5 0.7 copy-start.5
  15.0 29.0 %copy-start.1 = (bf16[1,2048,128]{2,1,0:T(8,128)(2,1)S(1)}, bf16[1,2048,128]{2,1,0:T(8,128)(2,1)}, u32[]{:S(2)}) copy-start(bf16[1,2048,128]{2,1,0:T(8,128)(2,1)} %param.17) | copy-start | bytes 1572868
  15.3 28.7 %copy-start = (bf16[1,2048,128]{2,1,0:T(8,128)(2,1)S(1)}, bf16[1,2048,128]{2,1,0:T(8,128)(2,1)}, u32[]{:S(2)}) copy-start(bf16[1,2048,128]{2,1,0:T(8,128)(2,1)} %param.18) | copy-start | bytes 1572868
  45.1 33.0 %collective-permute-start.6 = (bf16[2,2048,128]{2,1,0:T(8,128)(2,1)}, bf16[2,2048,128]{2,1,0:T(8,128)(2,1)S(1)}, u32[]{:S(2)}, u32[]{:S(2)}) collective-permute-start(bf16[2,2048,128]{2,1,0:T(8,128)(2,1)} %pad_maximum_fusion), channel_id=1, source_target_pairs={{0,1},{1,0},{2,3},{3,2},{4,5},{5,4},{6,7},{7,6},{8,9},{9,8},{10,11... | collective-permute-start | bytes 3145736 | tf_op jit(solution)/shard_map/ppermute | solution.py:310
  47.0 31.1 %collective-permute-start.7 = (bf16[128,2048]{1,0:T(8,128)(2,1)}, bf16[128,2048]{1,0:T(8,128)(2,1)}, u32[]{:S(2)}, u32[]{:S(2)}) collective-permute-start(bf16[128,2048]{1,0:T(8,128)(2,1)} %bitcast.12.wd), channel_id=1, source_target_pairs={{0,1},{1,0},{2,3},{3,2},{4,5},{5,4},{6,7},{7,6},{8,9},{9,8},{10,11... | collective-permute-start | bytes 1572872 | tf_op jit(solution)/shard_map/ppermute | solution.py:310
  49.5 14.5 %collective-permute-start.5 = (bf16[4,160,128]{2,1,0:T(8,128)(2,1)}, bf16[4,160,128]{2,1,0:T(8,128)(2,1)S(1)}, u32[]{:S(2)}, u32[]{:S(2)}) collective-permute-start(bf16[4,160,128]{2,1,0:T(8,128)(2,1)} %get-tuple-element.36), channel_id=1, source_target_pairs={{0,12},{2,14},{4,0},{6,2},{8,4},{10,6},{12,8},{14,10},{1,13},{3,15... | collective-permute-start | bytes 491528 | tf_op jit(solution)/shard_map/ppermute | solution.py:307
  55.7 22.5 %collective-permute-start.3 = (bf16[2,4,160,128]{3,2,1,0:T(8,128)(2,1)S(1)}, bf16[2,4,160,128]{3,2,1,0:T(8,128)(2,1)S(1)}, u32[]{:S(2)}, u32[]{:S(2)}) collective-permute-start(bf16[2,4,160,128]{3,2,1,0:T(8,128)(2,1)S(1)} %get-tuple-element.34.both), channel_id=1, source_target_pairs={{0,14},{2,0},{4,2},{6,4},{8,6},{10,8},{12,10},{14,12},{1,15},{3,1}... | collective-permute-start | bytes 983048 | tf_op jit(solution)/shard_map/ppermute | solution.py:307
  58.7 19.5 %collective-permute-start.2 = (bf16[2,4,160,128]{3,2,1,0:T(8,128)(2,1)S(1)}, bf16[2,4,160,128]{3,2,1,0:T(8,128)(2,1)S(1)}, u32[]{:S(2)}, u32[]{:S(2)}) collective-permute-start(bf16[2,4,160,128]{3,2,1,0:T(8,128)(2,1)S(1)} %get-tuple-element.34.both), channel_id=1, source_target_pairs={{0,2},{2,4},{4,6},{6,8},{8,10},{10,12},{12,14},{14,0},{1,3},{3,5},... | collective-permute-start | bytes 983048 | tf_op jit(solution)/shard_map/ppermute | solution.py:307
  64.0 14.1 %collective-permute-start.4 = (bf16[4,160,128]{2,1,0:T(8,128)(2,1)}, bf16[4,160,128]{2,1,0:T(8,128)(2,1)S(1)}, u32[]{:S(2)}, u32[]{:S(2)}) collective-permute-start(bf16[4,160,128]{2,1,0:T(8,128)(2,1)} %get-tuple-element.36), channel_id=1, source_target_pairs={{0,4},{2,6},{4,8},{6,10},{8,12},{10,14},{12,0},{14,2},{1,5},{3,7},... | collective-permute-start | bytes 491528 | tf_op jit(solution)/shard_map/ppermute | solution.py:307
  82.3 4.7 %copy-start.15 = (f32[128]{0:T(128)S(1)}, f32[128]{0:T(128)}, u32[]{:S(2)}) copy-start(f32[128]{0:T(128)} %param.25) | copy-start | bytes 1540
  82.3 21.2 %all-to-all-start.1 = ((bf16[16,160,128]{2,1,0:T(8,128)(2,1)}), bf16[16,160,128]{2,1,0:T(8,128)(2,1)S(1)}, u32[]{:S(2)}, u32[]{:S(2)}) async-start(bf16[16,160,128]{2,1,0:T(8,128)(2,1)} %bitcast.30), calls=%async_computation.1 | async-start | bytes 1310720 | tf_op jit(solution)/shard_map/all_to_all | solution.py:347
  104.5 4.2 %copy-start.11 = (bf16[128,128]{1,0:T(8,128)(2,1)S(1)}, bf16[128,128]{1,0:T(8,128)(2,1)}, u32[]{:S(2)}) copy-start(bf16[128,128]{1,0:T(8,128)(2,1)} %param.22) | copy-start | bytes 98308
  104.5 4.2 %copy-start.12 = (bf16[128,128]{1,0:T(8,128)(2,1)S(1)}, bf16[128,128]{1,0:T(8,128)(2,1)}, u32[]{:S(2)}) copy-start(bf16[128,128]{1,0:T(8,128)(2,1)} %param.21) | copy-start | bytes 98308
  104.5 4.2 %copy-start.13 = (bf16[128,128]{1,0:T(8,128)(2,1)S(1)}, bf16[128,128]{1,0:T(8,128)(2,1)}, u32[]{:S(2)}) copy-start(bf16[128,128]{1,0:T(8,128)(2,1)} %param.24) | copy-start | bytes 98308
  104.5 4.2 %copy-start.14 = (bf16[128,128]{1,0:T(8,128)(2,1)S(1)}, bf16[128,128]{1,0:T(8,128)(2,1)}, u32[]{:S(2)}) copy-start(bf16[128,128]{1,0:T(8,128)(2,1)} %param.23) | copy-start | bytes 98308
  104.5 15.1 %all-to-all-start.2 = ((bf16[32,16,128]{2,1,0:T(8,128)(2,1)}), bf16[32,16,128]{2,1,0:T(8,128)(2,1)S(1)}, u32[]{:S(2)}, u32[]{:S(2)}) async-start(bf16[32,16,128]{2,1,0:T(8,128)(2,1)} %bitcast.17), calls=%async_computation.2 | async-start | bytes 262144 | tf_op jit(solution)/shard_map/all_to_all | solution.py:349
  108.8 0.9 copy-start.3
  108.9 1.0 copy-start.4
  109.8 9.8 %copy-start.9 = (bf16[512,128]{1,0:T(8,128)(2,1)S(1)}, bf16[512,128]{1,0:T(8,128)(2,1)}, u32[]{:S(2)}) copy-start(bf16[512,128]{1,0:T(8,128)(2,1)} %get-tuple-element.48) | copy-start | bytes 393220
  109.8 9.8 %copy-start.10 = (bf16[128,128]{1,0:T(8,128)(2,1)S(1)}, bf16[128,128]{1,0:T(8,128)(2,1)}, u32[]{:S(2)}) copy-start(bf16[128,128]{1,0:T(8,128)(2,1)} %param.14) | copy-start | bytes 98308
  112.5 24.9 %copy-start.2 = (bf16[128,2048]{1,0:T(8,128)(2,1)S(1)}, bf16[128,2048]{1,0:T(8,128)(2,1)}, u32[]{:S(2)}) copy-start(bf16[128,2048]{1,0:T(8,128)(2,1)} %out_proj.1) | copy-start | bytes 1572868
  112.5 34.6 %collective-permute-start.9 = (bf16[128,2048]{1,0:T(8,128)(2,1)}, bf16[128,2048]{1,0:T(8,128)(2,1)S(1)}, u32[]{:S(2)}, u32[]{:S(2)}) collective-permute-start(bf16[128,2048]{1,0:T(8,128)(2,1)} %get-tuple-element.45), channel_id=1, source_target_pairs={{0,1},{1,0},{2,3},{3,2},{4,5},{5,4},{6,7},{7,6},{8,9},{9,8},{10,11... | collective-permute-start | bytes 1572872 | tf_op jit(solution)/shard_map/ppermute | solution.py:310
  114.6 33.5 %collective-permute-start.8 = (bf16[2,2048,128]{2,1,0:T(8,128)(2,1)}, bf16[2,2048,128]{2,1,0:T(8,128)(2,1)S(1)}, u32[]{:S(2)}, u32[]{:S(2)}) collective-permute-start(bf16[2,2048,128]{2,1,0:T(8,128)(2,1)} %get-tuple-element.43), channel_id=1, source_target_pairs={{0,1},{1,0},{2,3},{3,2},{4,5},{5,4},{6,7},{7,6},{8,9},{9,8},{10,11... | collective-permute-start | bytes 3145736 | tf_op jit(solution)/shard_map/ppermute | solution.py:310
  138.7 8.4 %copy-start.8 = (bf16[128,2048]{1,0:T(8,128)(2,1)S(1)}, bf16[128,2048]{1,0:T(8,128)(2,1)}, u32[]{:S(2)}) copy-start(bf16[128,2048]{1,0:T(8,128)(2,1)} %get-tuple-element.44) | copy-start | bytes 1572868
  138.8 27.9 %all-to-all-start.3 = ((bf16[32,72,128]{2,1,0:T(8,128)(2,1)}), bf16[32,72,128]{2,1,0:T(8,128)(2,1)S(1)}, u32[]{:S(2)}, u32[]{:S(2)}) async-start(bf16[32,72,128]{2,1,0:T(8,128)(2,1)} %get-tuple-element.50), calls=%async_computation.3 | async-start | bytes 1179648 | tf_op jit(solution)/shard_map/all_to_all | solution.py:359
  147.1 1.4 copy-start.7

commit v6 on v5

--- a/solution.py
+++ b/solution.py
@@ -120,11 +120,11 @@
     return call(sort_body, out, recv, scratch=[pltpu.VMEM(recv.shape, F32)], kept=(0, 1))
 
 
-def shards(chip, both, f1, b1, f2, b2, n_y):
+def shards(chip, both, f1, b1, f2, b2, near, n_y):
     found = []
     for off, ref in ((0, both), (n_y - 1, f1), (1, b1)):
         for n in range(2):
-            found.append((off + 4 * n, [ref[n, i] for i in range(4)]))
+            found.append((off + 4 * n, [near[i] if off == n == 0 else ref[n, i] for i in range(4)]))
     for off, ref in ((n_y - 2, f2), (2, b2)):
         found.append((off, [ref[i] for i in range(4)]))
     for off, p in found:
@@ -132,7 +132,7 @@
         yield y, jnp.concatenate(p[:2], axis=1), jnp.concatenate(p[2:], axis=1)
 
 
-def expert_body(chip, both, f1, b1, f2, b2, wgu_peer, wg, wu, wd, wd_peer, gu_grad, hidden, part):
+def expert_body(chip, both, f1, b1, f2, b2, near, wgu_peer, wg, wu, wd, wd_peer, gu_grad, hidden, part):
     n_y = part.shape[0]
     fw = wd.shape[0]
     rows, hid = hidden.shape
@@ -143,7 +143,7 @@
         at = pl.ds(pl.multiple_of(y * 2 * fw, 2 * fw), 2 * fw)
         return jnp.concatenate([wg[at, :], wgu_peer[0, at, :], wu[at, :], wgu_peer[1, at, :]], axis=1), at
 
-    for y, x_in, x_cot in shards(chip[0], both, f1, b1, f2, b2, n_y):
+    for y, x_in, x_cot in shards(chip[0], both, f1, b1, f2, b2, near, n_y):
         w, at = weights(y)
         acc = acc + dot(x_in, w, ((1,), (0,)))
         back = back + dot(x_cot, jnp.concatenate([wd[:, at], wd_peer[:, at]], axis=0), ((1,), (1,)))
@@ -171,11 +171,11 @@
     return call(expert_body, out, chip, *blocks, *weights, scalars=1)
 
 
-def weight_body(chip, both, f1, b1, f2, b2, gu_grad, hidden, dgu, dgu_send, dd, dd_send):
+def weight_body(chip, both, f1, b1, f2, b2, near, gu_grad, hidden, dgu, dgu_send, dd, dd_send):
     fw = dd.shape[0]
     hid = hidden.shape[1]
     n_y = dd.shape[1] // (2 * fw)
-    for y, x_in, x_cot in shards(chip[0], both, f1, b1, f2, b2, n_y):
+    for y, x_in, x_cot in shards(chip[0], both, f1, b1, f2, b2, near, n_y):
         at = pl.ds(pl.multiple_of(y * 2 * fw, 2 * fw), 2 * fw)
         r = dot(x_in, gu_grad[...], ((0,), (0,))).astype(BF16)
         for i in range(2):
@@ -189,7 +189,7 @@
 def expert_weight_grads(chip, blocks, gu_grad, hidden, d):
     fw = blocks[0].shape[3]
     out = (whole((2, d, fw), BF16),) * 2 + (whole((fw, d), BF16),) * 2
-    return call(weight_body, out, chip, *blocks, gu_grad, hidden, scalars=1, loose=(6, 7))
+    return call(weight_body, out, chip, *blocks, gu_grad, hidden, scalars=1, loose=(7, 8))
 
 
 def add_body(parts, out, *, half):
@@ -223,12 +223,25 @@
     return [p.astype(F32) for p in (hi, mid, lo)]
 
 
+def chain_rows(mult, add, shape):
+    row = iota(shape, 0)
+    chain = jnp.zeros(shape, F32)
+    for i, piece in enumerate(in_three(mult) + in_three(add)):
+        chain = jnp.where(row == i, piece, chain)
+    return chain.astype(BF16)
+
+
+def chain_of(rows):
+    c = rows.astype(F32)
+    return (c[2:3] + c[1:2]) + c[0:1], (c[5:6] + c[4:5]) + c[3:4]
+
+
 def chain_body(mix, out_proj, rec_state, decay, local, through, last):
-    n_sp, width = last.shape[0], last.shape[2]
-    keep = mix.shape[1] // n_sp
+    n_x, n_z, _, width = last.shape
+    keep = mix.shape[1] // (n_x * n_z)
     proj = dot(mix[...], rec_state[...], ((0,), (0,))).astype(BF16)
-    for k in range(n_sp):
-        last[k, :keep, :] = proj[k * keep : (k + 1) * keep, :]
+    for k in range(n_x * n_z):
+        last[k % n_x, k // n_x, :keep, :] = proj[k * keep : (k + 1) * keep, :]
     grad = dot(mix[...], out_proj[...], ((1,), (1,)))
     mult = later(decay[...], 1, 1.0)
     step = 1
@@ -239,45 +252,67 @@
     local[...] = grad
     through[...] = mult
     first = decay[0:1, :]
-    row = iota((last.shape[1] - keep, width), 0)
-    chain = jnp.zeros(row.shape, F32)
-    for i, piece in enumerate(in_three(first * mult[0:1, :]) + in_three(first * grad[0:1, :])):
-        chain = jnp.where(row == i, piece, chain)
-    chain = chain.astype(BF16)
-    for k in range(n_sp):
-        last[k, keep:, :] = chain
-
-
-def chain_within(mix, out_proj, rec_state, decay, n_sp):
+    chain = chain_rows(first * mult[0:1, :], first * grad[0:1, :], (last.shape[2] - keep, width))
+    for k in range(n_x * n_z):
+        last[k % n_x, k // n_x, keep:, :] = chain
+
+
+def chain_within(mix, out_proj, rec_state, decay, n_x, n_z):
     tokens, width = decay.shape
-    last = whole((n_sp, mix.shape[1] // n_sp + 8, width), BF16)
+    last = whole((n_x, n_z, mix.shape[1] // (n_x * n_z) + 8, width), BF16)
     out = (whole((tokens, width), F32),) * 2 + (last,)
     return call(chain_body, out, mix, out_proj, rec_state, decay, kept=(0, 1, 2))
 
 
-def finish_body(here, last, local, through, value_by, input_by, rate_by, proj, value, inp, rate):
-    n_sp = last.shape[0]
+def join_body(here, last, sent, within):
+    n_x, n_z, rows, width = last.shape
+    keep = rows - 8
+    for z in range(n_z):
+        total = last[0, z, :keep, :].astype(F32)
+        for x in range(1, n_x):
+            total = total + last[x, z, :keep, :].astype(F32)
+        sent[z, :keep, :] = total.astype(BF16)
+    mult, add = jnp.ones((1, width), F32), jnp.zeros((1, width), F32)
+    after = [mult, add]
+    for x in reversed(range(n_x)):
+        m, a = chain_of(last[x, 0, keep:, :])
+        passed = x > here[0]
+        after = [jnp.where(passed, m * after[0], after[0]), jnp.where(passed, a + m * after[1], after[1])]
+        mult, add = m * mult, a + m * add
+    row = iota(within.shape, 0)
+    within[...] = jnp.where(row == 0, after[0], after[1])
+    chain = chain_rows(mult, add, (8, width))
+    for z in range(n_z):
+        sent[z, keep:, :] = chain
+
+
+def join(here, last):
+    out = (whole(last.shape[1:], BF16), whole((8, last.shape[3]), F32))
+    return call(join_body, out, here, last, scalars=1, kept=(0, 1))
+
+
+def finish_body(here, last, within, local, through, value_by, input_by, rate_by, proj, value, inp, rate):
+    n_z = last.shape[0]
     keep = proj.shape[0]
     incoming = jnp.zeros((1, last.shape[2]), F32)
-    for k in reversed(range(n_sp)):
-        c = last[k, keep:, :].astype(F32)
-        mult = (c[2:3] + c[1:2]) + c[0:1]
-        add = (c[5:6] + c[4:5]) + c[3:4]
+    for k in reversed(range(n_z)):
+        mult, add = chain_of(last[k, keep:, :])
         incoming = jnp.where(k > here[0], add + mult * incoming, incoming)
+    incoming = within[1:2, :] + within[0:1, :] * incoming
     carried = local[...] + through[...] * incoming
     value[...] = (carried * value_by[...]).astype(BF16)
     inp[...] = (carried * input_by[...]).astype(BF16)
     rate[...] = (carried * rate_by[...]).astype(BF16)
     total = last[0, :keep, :].astype(F32)
-    for k in range(1, n_sp):
+    for k in range(1, n_z):
         total = total + last[k, :keep, :].astype(F32)
     proj[...] = total
 
 
-def finish(here, last, local, through, value_by, input_by, rate_by):
+def finish(here, last, within, local, through, value_by, input_by, rate_by):
     grid = whole(local.shape, BF16)
     out = (whole((last.shape[1] - 8, last.shape[2]), F32), grid, grid, grid)
-    return call(finish_body, out, here, last, local, through, value_by, input_by, rate_by, scalars=1)
+    return call(finish_body, out, here, last, within, local, through, value_by, input_by, rate_by, scalars=1)
 
 
 def per_device(
@@ -324,7 +359,7 @@
     wgu_peer = over_cores(wgu)
     wd_peer = over_cores(late_down[0])
     first = (both, over_y(both, 1), over_y(both, -1))
-    blocks = (*first, over_y(near, 2), over_y(near, -2))
+    blocks = (*first, over_y(near, 2), over_y(near, -2), near)
 
     gu_grad, hidden, part = expert_rows_grad(
         chip, blocks, wgu_peer, late_gate[0], late_up[0], late_down[0], wd_peer, n_y
@@ -342,8 +377,9 @@
     input_by = value_by * signal * (1.0 - input_gate)
     decay_part = decay * before_state - input_gate * signal * decay * decay / scale_in
     rate_by = decay_part * (-decay_scale * decay_speed) * rate_gate * (1.0 - rate_gate)
-    here = lax.axis_index(SP).reshape(1).astype(jnp.int32)
-    part, here = lax.optimization_barrier((part, here))
+    my_z = lax.axis_index("z").reshape(1).astype(jnp.int32)
+    my_x = lax.axis_index("x").reshape(1).astype(jnp.int32)
+    part, my_z, my_x = lax.optimization_barrier((part, my_z, my_x))
     arrived = lax.all_to_all(part.reshape(2 * n_y, *part.shape[2:]), TP, 0, 0, tiled=True)
     back = add_parts(arrived.reshape(part.shape), n_sp, half)
     returned = lax.all_to_all(back.reshape(n_sp, 16, fw), SP, 0, 0, tiled=True).reshape(back.shape)
@@ -355,10 +391,13 @@
     own_grad = (dot(pick, returned, ((0,), (0,))) + out_grad.astype(F32)).astype(BF16)
     mix_grad = lax.all_gather(own_grad, TP, axis=1, tiled=True)
 
-    local, through, last = chain_within(mix_grad, out_proj, rec_state, decay, n_sp)
-    last = lax.all_to_all(last, SP, 0, 0, tiled=True)
+    n_x, n_z = lax.axis_size("x"), lax.axis_size("z")
+    local, through, last = chain_within(mix_grad, out_proj, rec_state, decay, n_x, n_z)
+    over_x = lax.all_to_all(last.reshape(n_x, -1, fw), "x", 0, 0, tiled=True)
+    sent, within = join(my_x, over_x.reshape(last.shape))
+    last = lax.all_to_all(sent, "z", 0, 0, tiled=True)
     out_proj_grad, rec_value_grad, input_pre_grad, rate_pre_grad = finish(
-        here, last, local, through, value_by, input_by, rate_by
+        my_z, last, within, local, through, value_by, input_by, rate_by
     )
     return (
         d_gate,

time: 168 us -> 172 us (1.024)
  starting transfers between devices: 48.7 us -> 50.8 us
    all_to_all x1 -> x2, starting transfers between devices: 8.38 us -> 10.5 us  [the longest x1 6.73 us: per_device(): last = lax.all_to_all(sent, 'z', 0, 0, tiled=True)]
    pallas_call x8 -> x9, Pallas kernels: 11.9 us -> 12.9 us  [call(): pl.pallas_call(body, out_shape=tuple(outs), in_specs=[SMEM] * scalars + [...]
    all_to_all x1 -> x2, waiting for transfers between devices: 16.8 us -> 16.5 us  [the longest x1 8.47 us: per_device(): over_x = lax.all_to_all(last.reshape(n_x, -1, fw), 'x', 0, 0, tiled=True)]
  transfers between devices with their start and end apart: 13 -> 14, of which waited for: 6 -> 7; matrix products, arithmetic and copies ran while one was open for 2% -> 3% of each run, Pallas kernels for 3% -> 4%
where the time goes in v6:
time: 172 us; the launch traced here: 171 us
  waiting for transfers between devices  52.7 us (31%)
  starting transfers between devices  50.8 us (30%)
  blocking collectives  45.5 us (26%)
  Pallas kernels  12.9 us (8%)
  other arithmetic  5.53 us (3%)
    all_to_all x1, blocking collectives, per_device(): lax.all_to_all(send.reshape(n_sp, -1, fw), SP, 0, 0, tiled=True)  27.9 us
    ppermute x5, starting transfers between devices, over_y(): return lax.ppermute(v, 'y', [(i, (i + step) % n_y) for i in range(n_y)])  20.8 us
    ppermute x5, waiting for transfers between devices, over_y(): return lax.ppermute(v, 'y', [(i, (i + step) % n_y) for i in range(n_y)])  17.9 us
    all_gather x1, blocking collectives, per_device(): mix_grad = lax.all_gather(own_grad, TP, axis=1, tiled=True)  17.6 us
    all_to_all x1, waiting for transfers between devices, per_device(): lax.all_to_all(part.reshape(2 * n_y, *part.shape[2:]), TP, 0, 0, tiled=True)  16.5 us
    pallas_call x9, Pallas kernels, call(): pl.pallas_call(body, out_shape=tuple(outs), in_specs=[SMEM] * scalars + [...  12.9 us
    ppermute x5, starting transfers between devices, over_cores(): return lax.ppermute(v, 'c', [(0, 1), (1, 0)])  10.6 us
    all_to_all x1, waiting for transfers between devices, per_device(): over_x = lax.all_to_all(last.reshape(n_x, -1, fw), 'x', 0, 0, tiled=True)  8.47 us
  transfers between devices with their start and end apart: 14, of which 7 were waited for; matrix products, arithmetic and copies ran while one was open for 3% of the time, Pallas kernels for 4%

profile of v6, /device:TPU:8, one launch (start us, length us, event | category | flops | bytes accessed | tf_op | source)
XLA Modules:
  0.0 171.0 jit_solution(3362605327904514271)
XLA Ops:
  1.4 6.8 %collective-permute-start = (bf16[2,128,128]{2,1,0:T(8,128)(2,1)S(1)}, bf16[2,128,128]{2,1,0:T(8,128)(2,1)S(1)}, u32[]{:S(2)}, u32[]{:S(2)}) collective-permute-start(bf16[2,128,128]{2,1,0:T(8,128)(2,1)S(1)} %get-tuple-element.69), channel_id=1, source_target_pairs={{0,8},{2,10},{4,12},{6,14},{8,0},{10,2},{12,4},{14,6},{1,9},{3,11}... | collective-permute-start | bytes 196616 | tf_op jit(solution)/shard_map/ppermute | solution.py:342
  8.3 3.2 %collective-permute-done = bf16[2,128,128]{2,1,0:T(8,128)(2,1)S(1)} collective-permute-done((bf16[2,128,128]{2,1,0:T(8,128)(2,1)S(1)}, bf16[2,128,128]{2,1,0:T(8,128)(2,1)S(1)}, u32[]{:S(2)}, u32[]{:S(2)}) %collective-permute-start) | collective-permute-done | bytes 65568 | tf_op jit(solution)/shard_map/ppermute | solution.py:342
  11.5 1.9 %collective-permute-start.1 = (bf16[2,2,128,128]{3,2,1,0:T(8,128)(2,1)S(1)}, bf16[2,2,128,128]{3,2,1,0:T(8,128)(2,1)S(1)}, u32[]{:S(2)}, u32[]{:S(2)}) collective-permute-start(bf16[2,2,128,128]{3,2,1,0:T(8,128)(2,1)S(1)} %pad_maximum_fusion.1.mine), channel_id=1, source_target_pairs={{0,1},{1,0},{2,3},{3,2},{4,5},{5,4},{6,7},{7,6},{8,9},{9,8},{10,11... | collective-permute-start | bytes 393224 | tf_op jit(solution)/shard_map/ppermute | solution.py:345
  14.1 0.9 shard_map.180
  15.3 27.9 %all_to_all.25 = bf16[32,40,128]{2,1,0:T(8,128)(2,1)S(1)} all-to-all(bf16[32,40,128]{2,1,0:T(8,128)(2,1)S(1)} %bitcast.30), channel_id=1, replica_groups=mesh['z'=8,'x'=4,'y'=8,'c'=2] {'z','x'}, dimensions={0} | all-to-all | bytes 655360 | tf_op jit(solution)/shard_map/all_to_all | solution.py:354
  43.4 1.1 pad_maximum_fusion
  44.5 1.9 %collective-permute-start.6 = (bf16[2,2048,128]{2,1,0:T(8,128)(2,1)}, bf16[2,2048,128]{2,1,0:T(8,128)(2,1)S(1)}, u32[]{:S(2)}, u32[]{:S(2)}) collective-permute-start(bf16[2,2048,128]{2,1,0:T(8,128)(2,1)} %pad_maximum_fusion), channel_id=1, source_target_pairs={{0,1},{1,0},{2,3},{3,2},{4,5},{5,4},{6,7},{7,6},{8,9},{9,8},{10,11... | collective-permute-start | bytes 3145736 | tf_op jit(solution)/shard_map/ppermute | solution.py:345
  46.4 2.4 %collective-permute-start.7 = (bf16[128,2048]{1,0:T(8,128)(2,1)}, bf16[128,2048]{1,0:T(8,128)(2,1)}, u32[]{:S(2)}, u32[]{:S(2)}) collective-permute-start(bf16[128,2048]{1,0:T(8,128)(2,1)} %bitcast.12.wd), channel_id=1, source_target_pairs={{0,1},{1,0},{2,3},{3,2},{4,5},{5,4},{6,7},{7,6},{8,9},{9,8},{10,11... | collective-permute-start | bytes 1572872 | tf_op jit(solution)/shard_map/ppermute | solution.py:345
  48.8 6.2 %collective-permute-start.5 = (bf16[4,160,128]{2,1,0:T(8,128)(2,1)S(1)}, bf16[4,160,128]{2,1,0:T(8,128)(2,1)S(1)}, u32[]{:S(2)}, u32[]{:S(2)}) collective-permute-start(bf16[4,160,128]{2,1,0:T(8,128)(2,1)S(1)} %get-tuple-element.39.near), channel_id=1, source_target_pairs={{0,12},{2,14},{4,0},{6,2},{8,4},{10,6},{12,8},{14,10},{1,13},{3,15... | collective-permute-start | bytes 491528 | tf_op jit(solution)/shard_map/ppermute | solution.py:342
  55.1 3.0 %collective-permute-start.3 = (bf16[2,4,160,128]{3,2,1,0:T(8,128)(2,1)S(1)}, bf16[2,4,160,128]{3,2,1,0:T(8,128)(2,1)S(1)}, u32[]{:S(2)}, u32[]{:S(2)}) collective-permute-start(bf16[2,4,160,128]{3,2,1,0:T(8,128)(2,1)S(1)} %get-tuple-element.37.both), channel_id=1, source_target_pairs={{0,14},{2,0},{4,2},{6,4},{8,6},{10,8},{12,10},{14,12},{1,15},{3,1}... | collective-permute-start | bytes 983048 | tf_op jit(solution)/shard_map/ppermute | solution.py:342
  58.1 2.9 %collective-permute-start.2 = (bf16[2,4,160,128]{3,2,1,0:T(8,128)(2,1)S(1)}, bf16[2,4,160,128]{3,2,1,0:T(8,128)(2,1)S(1)}, u32[]{:S(2)}, u32[]{:S(2)}) collective-permute-start(bf16[2,4,160,128]{3,2,1,0:T(8,128)(2,1)S(1)} %get-tuple-element.37.both), channel_id=1, source_target_pairs={{0,2},{2,4},{4,6},{6,8},{8,10},{10,12},{12,14},{14,0},{1,3},{3,5},... | collective-permute-start | bytes 983048 | tf_op jit(solution)/shard_map/ppermute | solution.py:342
  60.9 2.1 %collective-permute-done.5.b2 = bf16[4,160,128]{2,1,0:T(8,128)(2,1)S(1)} collective-permute-done((bf16[4,160,128]{2,1,0:T(8,128)(2,1)S(1)}, bf16[4,160,128]{2,1,0:T(8,128)(2,1)S(1)}, u32[]{:S(2)}, u32[]{:S(2)}) %collective-permute-start.5) | collective-permute-done | bytes 163872 | tf_op jit(solution)/shard_map/ppermute | solution.py:342
  63.1 1.9 %collective-permute-start.4 = (bf16[4,160,128]{2,1,0:T(8,128)(2,1)S(1)}, bf16[4,160,128]{2,1,0:T(8,128)(2,1)}, u32[]{:S(2)}, u32[]{:S(2)}) collective-permute-start(bf16[4,160,128]{2,1,0:T(8,128)(2,1)S(1)} %get-tuple-element.39.near), channel_id=1, source_target_pairs={{0,4},{2,6},{4,8},{6,10},{8,12},{10,14},{12,0},{14,2},{1,5},{3,7},... | collective-permute-start | bytes 491528 | tf_op jit(solution)/shard_map/ppermute | solution.py:342
  65.0 12.5 %collective-permute-done.4.f2 = bf16[4,160,128]{2,1,0:T(8,128)(2,1)} collective-permute-done((bf16[4,160,128]{2,1,0:T(8,128)(2,1)S(1)}, bf16[4,160,128]{2,1,0:T(8,128)(2,1)}, u32[]{:S(2)}, u32[]{:S(2)}) %collective-permute-start.4) | collective-permute-done | bytes 163872 | tf_op jit(solution)/shard_map/ppermute | solution.py:342
  77.5 4.1 %shard_map.183 = (bf16[160,512]{1,0:T(8,128)(2,1)}, bf16[160,256]{1,0:T(8,128)(2,1)}, bf16[8,2,160,128]{3,2,1,0:T(8,128)(2,1)}) custom-call(s32[1]{0:T(128)} %bitcast.chip, bf16[2,4,160,128]{3,2,1,0:T(8,128)(2,1)S(1)} %get-tuple-element.37.both, bf16[2,4,160,128]{3,2,1,0:T(8,128)(2,1)S(1)} %collective-permute-done.2.f1, ...), custom_call_target="tpu_custom_call" | custom-call | tf_op jit(solution)/shard_map/pallas_call | solution.py:31
  81.7 4.7 %all-to-all-start.1 = ((bf16[16,160,128]{2,1,0:T(8,128)(2,1)}), bf16[16,160,128]{2,1,0:T(8,128)(2,1)S(1)}, u32[]{:S(2)}, u32[]{:S(2)}) async-start(bf16[16,160,128]{2,1,0:T(8,128)(2,1)} %bitcast.34), calls=%async_computation.1 | async-start | bytes 1310720 | tf_op jit(solution)/shard_map/all_to_all | solution.py:383
  86.4 16.5 %all-to-all-done.1 = bf16[16,160,128]{2,1,0:T(8,128)(2,1)S(1)} async-done(((bf16[16,160,128]{2,1,0:T(8,128)(2,1)}), bf16[16,160,128]{2,1,0:T(8,128)(2,1)S(1)}, u32[]{:S(2)}, u32[]{:S(2)}) %all-to-all-start.1) | async-done | bytes 655392 | tf_op jit(solution)/shard_map/all_to_all | solution.py:383
  102.9 1.0 shard_map.185
  104.0 4.2 %all-to-all-start.2 = ((bf16[32,16,128]{2,1,0:T(8,128)(2,1)}), bf16[32,16,128]{2,1,0:T(8,128)(2,1)S(1)}, u32[]{:S(2)}, u32[]{:S(2)}) async-start(bf16[32,16,128]{2,1,0:T(8,128)(2,1)} %bitcast.18), calls=%async_computation.2 | async-start | bytes 262144 | tf_op jit(solution)/shard_map/all_to_all | solution.py:385
  109.2 3.6 %shard_map.184 = (bf16[2,2048,128]{2,1,0:T(8,128)(2,1)}, bf16[2,2048,128]{2,1,0:T(8,128)(2,1)}, bf16[128,2048]{1,0:T(8,128)(2,1)}, bf16[128,2048]{1,0:T(8,128)(2,1)}) custom-call(s32[1]{0:T(128)} %bitcast.chip, bf16[2,4,160,128]{3,2,1,0:T(8,128)(2,1)S(1)} %get-tuple-element.37.both, bf16[2,4,160,128]{3,2,1,0:T(8,128)(2,1)S(1)} %collective-permute-done.2.f1, ...), custom_call_target="tpu_custom_call" | custom-call | tf_op jit(solution)/shard_map/pallas_call | solution.py:31
  112.8 1.9 %collective-permute-start.9 = (bf16[128,2048]{1,0:T(8,128)(2,1)}, bf16[128,2048]{1,0:T(8,128)(2,1)}, u32[]{:S(2)}, u32[]{:S(2)}) collective-permute-start(bf16[128,2048]{1,0:T(8,128)(2,1)} %get-tuple-element.48), channel_id=1, source_target_pairs={{0,1},{1,0},{2,3},{3,2},{4,5},{5,4},{6,7},{7,6},{8,9},{9,8},{10,11... | collective-permute-start | bytes 1572872 | tf_op jit(solution)/shard_map/ppermute | solution.py:345
  114.7 2.4 %collective-permute-start.8 = (bf16[2,2048,128]{2,1,0:T(8,128)(2,1)}, bf16[2,2048,128]{2,1,0:T(8,128)(2,1)S(1)}, u32[]{:S(2)}, u32[]{:S(2)}) collective-permute-start(bf16[2,2048,128]{2,1,0:T(8,128)(2,1)} %get-tuple-element.46), channel_id=1, source_target_pairs={{0,1},{1,0},{2,3},{3,2},{4,5},{5,4},{6,7},{7,6},{8,9},{9,8},{10,11... | collective-permute-start | bytes 3145736 | tf_op jit(solution)/shard_map/ppermute | solution.py:345
  117.2 1.9 %all-to-all-done.2 = bf16[32,16,128]{2,1,0:T(8,128)(2,1)S(1)} async-done(((bf16[32,16,128]{2,1,0:T(8,128)(2,1)}), bf16[32,16,128]{2,1,0:T(8,128)(2,1)S(1)}, u32[]{:S(2)}, u32[]{:S(2)}) %all-to-all-start.2) | async-done | bytes 131104 | tf_op jit(solution)/shard_map/all_to_all | solution.py:385
  119.1 1.1 fusion
  120.2 17.6 %all_gather.3.mix = bf16[128,2048]{1,0:T(8,128)(2,1)S(1)} all-gather(bf16[128,128]{1,0:T(8,128)(2,1)S(1)} %fusion), channel_id=1, replica_groups=mesh['z'=8,'x'=4,'y'=8,'c'=2] {'y','c'}, dimensions={1}, use_global_device_ids=true | all-gather | bytes 557056 | tf_op jit(solution)/shard_map/all_gather | solution.py:392
  137.8 1.3 shard_map.186
  139.1 3.7 %all-to-all-start.3 = ((bf16[4,576,128]{2,1,0:T(8,128)(2,1)}), bf16[4,576,128]{2,1,0:T(8,128)(2,1)S(1)}, u32[]{:S(2)}, u32[]{:S(2)}) async-start(bf16[4,576,128]{2,1,0:T(8,128)(2,1)} %bitcast.20), calls=%async_computation.3 | async-start | bytes 1179648 | tf_op jit(solution)/shard_map/all_to_all | solution.py:396
  142.9 2.2 %fusion.1 = bf16[1,128,2048]{2,1,0:T(8,128)(2,1)} fusion(bf16[128,2048]{1,0:T(8,128)(2,1)} %collective-permute-done.9, bf16[128,2048]{1,0:T(8,128)(2,1)} %get-tuple-element.47), kind=kLoop, calls=%fused_computation.6 | loop fusion | flops 1048576 | bytes 1572864 | tf_op jit(solution)/shard_map/broadcast_in_dim | solution.py:390
  145.1 8.5 %all-to-all-done.3 = bf16[4,576,128]{2,1,0:T(8,128)(2,1)S(1)} async-done(((bf16[4,576,128]{2,1,0:T(8,128)(2,1)}), bf16[4,576,128]{2,1,0:T(8,128)(2,1)S(1)}, u32[]{:S(2)}, u32[]{:S(2)}) %all-to-all-start.3) | async-done | bytes 589856 | tf_op jit(solution)/shard_map/all_to_all | solution.py:396
  154.3 6.7 %all-to-all-start.4 = ((bf16[8,72,128]{2,1,0:T(8,128)(2,1)}), bf16[8,72,128]{2,1,0:T(8,128)(2,1)S(1)}, u32[]{:S(2)}, u32[]{:S(2)}) async-start(bf16[8,72,128]{2,1,0:T(8,128)(2,1)} %get-tuple-element.55), calls=%async_computation.4 | async-start | bytes 294912 | tf_op jit(solution)/shard_map/all_to_all | solution.py:398
  161.1 1.2 add_convert_fusion.1
  162.3 8.0 %all-to-all-done.4.last = bf16[8,72,128]{2,1,0:T(8,128)(2,1)S(1)} async-done(((bf16[8,72,128]{2,1,0:T(8,128)(2,1)}), bf16[8,72,128]{2,1,0:T(8,128)(2,1)S(1)}, u32[]{:S(2)}, u32[]{:S(2)}) %all-to-all-start.4) | async-done | bytes 147488 | tf_op jit(solution)/shard_map/all_to_all | solution.py:398
  (46 shorter events, 4.4 us)
Async XLA Ops:
  1.4 10.1 %collective-permute-start = (bf16[2,128,128]{2,1,0:T(8,128)(2,1)S(1)}, bf16[2,128,128]{2,1,0:T(8,128)(2,1)S(1)}, u32[]{:S(2)}, u32[]{:S(2)}) collective-permute-start(bf16[2,128,128]{2,1,0:T(8,128)(2,1)S(1)} %get-tuple-element.69), channel_id=1, source_target_pairs={{0,8},{2,10},{4,12},{6,14},{8,0},{10,2},{12,4},{14,6},{1,9},{3,11}... | collective-permute-start | bytes 196616 | tf_op jit(solution)/shard_map/ppermute | solution.py:342
  11.5 3.5 %collective-permute-start.1 = (bf16[2,2,128,128]{3,2,1,0:T(8,128)(2,1)S(1)}, bf16[2,2,128,128]{3,2,1,0:T(8,128)(2,1)S(1)}, u32[]{:S(2)}, u32[]{:S(2)}) collective-permute-start(bf16[2,2,128,128]{3,2,1,0:T(8,128)(2,1)S(1)} %pad_maximum_fusion.1.mine), channel_id=1, source_target_pairs={{0,1},{1,0},{2,3},{3,2},{4,5},{5,4},{6,7},{7,6},{8,9},{9,8},{10,11... | collective-permute-start | bytes 393224 | tf_op jit(solution)/shard_map/ppermute | solution.py:345
  13.4 0.7 copy-start.6
  13.5 0.7 copy-start.5
  15.0 28.4 %copy-start.1 = (bf16[1,2048,128]{2,1,0:T(8,128)(2,1)S(1)}, bf16[1,2048,128]{2,1,0:T(8,128)(2,1)}, u32[]{:S(2)}) copy-start(bf16[1,2048,128]{2,1,0:T(8,128)(2,1)} %param.17) | copy-start | bytes 1572868
  15.3 28.1 %copy-start = (bf16[1,2048,128]{2,1,0:T(8,128)(2,1)S(1)}, bf16[1,2048,128]{2,1,0:T(8,128)(2,1)}, u32[]{:S(2)}) copy-start(bf16[1,2048,128]{2,1,0:T(8,128)(2,1)} %param.18) | copy-start | bytes 1572868
  44.5 33.0 %collective-permute-start.6 = (bf16[2,2048,128]{2,1,0:T(8,128)(2,1)}, bf16[2,2048,128]{2,1,0:T(8,128)(2,1)S(1)}, u32[]{:S(2)}, u32[]{:S(2)}) collective-permute-start(bf16[2,2048,128]{2,1,0:T(8,128)(2,1)} %pad_maximum_fusion), channel_id=1, source_target_pairs={{0,1},{1,0},{2,3},{3,2},{4,5},{5,4},{6,7},{7,6},{8,9},{9,8},{10,11... | collective-permute-start | bytes 3145736 | tf_op jit(solution)/shard_map/ppermute | solution.py:345
  46.4 31.1 %collective-permute-start.7 = (bf16[128,2048]{1,0:T(8,128)(2,1)}, bf16[128,2048]{1,0:T(8,128)(2,1)}, u32[]{:S(2)}, u32[]{:S(2)}) collective-permute-start(bf16[128,2048]{1,0:T(8,128)(2,1)} %bitcast.12.wd), channel_id=1, source_target_pairs={{0,1},{1,0},{2,3},{3,2},{4,5},{5,4},{6,7},{7,6},{8,9},{9,8},{10,11... | collective-permute-start | bytes 1572872 | tf_op jit(solution)/shard_map/ppermute | solution.py:345
  48.8 14.2 %collective-permute-start.5 = (bf16[4,160,128]{2,1,0:T(8,128)(2,1)S(1)}, bf16[4,160,128]{2,1,0:T(8,128)(2,1)S(1)}, u32[]{:S(2)}, u32[]{:S(2)}) collective-permute-start(bf16[4,160,128]{2,1,0:T(8,128)(2,1)S(1)} %get-tuple-element.39.near), channel_id=1, source_target_pairs={{0,12},{2,14},{4,0},{6,2},{8,4},{10,6},{12,8},{14,10},{1,13},{3,15... | collective-permute-start | bytes 491528 | tf_op jit(solution)/shard_map/ppermute | solution.py:342
  55.1 22.4 %collective-permute-start.3 = (bf16[2,4,160,128]{3,2,1,0:T(8,128)(2,1)S(1)}, bf16[2,4,160,128]{3,2,1,0:T(8,128)(2,1)S(1)}, u32[]{:S(2)}, u32[]{:S(2)}) collective-permute-start(bf16[2,4,160,128]{3,2,1,0:T(8,128)(2,1)S(1)} %get-tuple-element.37.both), channel_id=1, source_target_pairs={{0,14},{2,0},{4,2},{6,4},{8,6},{10,8},{12,10},{14,12},{1,15},{3,1}... | collective-permute-start | bytes 983048 | tf_op jit(solution)/shard_map/ppermute | solution.py:342
  58.1 19.5 %collective-permute-start.2 = (bf16[2,4,160,128]{3,2,1,0:T(8,128)(2,1)S(1)}, bf16[2,4,160,128]{3,2,1,0:T(8,128)(2,1)S(1)}, u32[]{:S(2)}, u32[]{:S(2)}) collective-permute-start(bf16[2,4,160,128]{3,2,1,0:T(8,128)(2,1)S(1)} %get-tuple-element.37.both), channel_id=1, source_target_pairs={{0,2},{2,4},{4,6},{6,8},{8,10},{10,12},{12,14},{14,0},{1,3},{3,5},... | collective-permute-start | bytes 983048 | tf_op jit(solution)/shard_map/ppermute | solution.py:342
  63.1 14.5 %collective-permute-start.4 = (bf16[4,160,128]{2,1,0:T(8,128)(2,1)S(1)}, bf16[4,160,128]{2,1,0:T(8,128)(2,1)}, u32[]{:S(2)}, u32[]{:S(2)}) collective-permute-start(bf16[4,160,128]{2,1,0:T(8,128)(2,1)S(1)} %get-tuple-element.39.near), channel_id=1, source_target_pairs={{0,4},{2,6},{4,8},{6,10},{8,12},{10,14},{12,0},{14,2},{1,5},{3,7},... | collective-permute-start | bytes 491528 | tf_op jit(solution)/shard_map/ppermute | solution.py:342
  81.7 4.7 %copy-start.14 = (f32[128]{0:T(128)S(1)}, f32[128]{0:T(128)}, u32[]{:S(2)}) copy-start(f32[128]{0:T(128)} %param.25) | copy-start | bytes 1540
  81.7 21.3 %all-to-all-start.1 = ((bf16[16,160,128]{2,1,0:T(8,128)(2,1)}), bf16[16,160,128]{2,1,0:T(8,128)(2,1)S(1)}, u32[]{:S(2)}, u32[]{:S(2)}) async-start(bf16[16,160,128]{2,1,0:T(8,128)(2,1)} %bitcast.34), calls=%async_computation.1 | async-start | bytes 1310720 | tf_op jit(solution)/shard_map/all_to_all | solution.py:383
  104.0 4.2 %copy-start.8 = (bf16[128,128]{1,0:T(8,128)(2,1)S(1)}, bf16[128,128]{1,0:T(8,128)(2,1)}, u32[]{:S(2)}) copy-start(bf16[128,128]{1,0:T(8,128)(2,1)} %param.22) | copy-start | bytes 98308
  104.0 4.2 %copy-start.9 = (bf16[128,128]{1,0:T(8,128)(2,1)S(1)}, bf16[128,128]{1,0:T(8,128)(2,1)}, u32[]{:S(2)}) copy-start(bf16[128,128]{1,0:T(8,128)(2,1)} %param.21) | copy-start | bytes 98308
  104.0 4.2 %copy-start.11 = (bf16[128,128]{1,0:T(8,128)(2,1)S(1)}, bf16[128,128]{1,0:T(8,128)(2,1)}, u32[]{:S(2)}) copy-start(bf16[128,128]{1,0:T(8,128)(2,1)} %param.24) | copy-start | bytes 98308
  104.0 4.2 %copy-start.13 = (bf16[128,128]{1,0:T(8,128)(2,1)S(1)}, bf16[128,128]{1,0:T(8,128)(2,1)}, u32[]{:S(2)}) copy-start(bf16[128,128]{1,0:T(8,128)(2,1)} %param.23) | copy-start | bytes 98308
  104.0 15.1 %all-to-all-start.2 = ((bf16[32,16,128]{2,1,0:T(8,128)(2,1)}), bf16[32,16,128]{2,1,0:T(8,128)(2,1)S(1)}, u32[]{:S(2)}, u32[]{:S(2)}) async-start(bf16[32,16,128]{2,1,0:T(8,128)(2,1)} %bitcast.18), calls=%async_computation.2 | async-start | bytes 262144 | tf_op jit(solution)/shard_map/all_to_all | solution.py:385
  108.2 0.9 copy-start.3
  108.2 1.0 copy-start.4
  109.2 8.0 %copy-start.10 = (bf16[128,128]{1,0:T(8,128)(2,1)S(1)}, bf16[128,128]{1,0:T(8,128)(2,1)}, u32[]{:S(2)}) copy-start(bf16[128,128]{1,0:T(8,128)(2,1)} %param.21) | copy-start | bytes 98308
  109.2 8.0 %copy-start.12 = (bf16[128,128]{1,0:T(8,128)(2,1)S(1)}, bf16[128,128]{1,0:T(8,128)(2,1)}, u32[]{:S(2)}) copy-start(bf16[128,128]{1,0:T(8,128)(2,1)} %param.24) | copy-start | bytes 98308
  112.8 30.1 %collective-permute-start.9 = (bf16[128,2048]{1,0:T(8,128)(2,1)}, bf16[128,2048]{1,0:T(8,128)(2,1)}, u32[]{:S(2)}, u32[]{:S(2)}) collective-permute-start(bf16[128,2048]{1,0:T(8,128)(2,1)} %get-tuple-element.48), channel_id=1, source_target_pairs={{0,1},{1,0},{2,3},{3,2},{4,5},{5,4},{6,7},{7,6},{8,9},{9,8},{10,11... | collective-permute-start | bytes 1572872 | tf_op jit(solution)/shard_map/ppermute | solution.py:345
  114.7 46.3 %collective-permute-start.8 = (bf16[2,2048,128]{2,1,0:T(8,128)(2,1)}, bf16[2,2048,128]{2,1,0:T(8,128)(2,1)S(1)}, u32[]{:S(2)}, u32[]{:S(2)}) collective-permute-start(bf16[2,2048,128]{2,1,0:T(8,128)(2,1)} %get-tuple-element.46), channel_id=1, source_target_pairs={{0,1},{1,0},{2,3},{3,2},{4,5},{5,4},{6,7},{7,6},{8,9},{9,8},{10,11... | collective-permute-start | bytes 3145736 | tf_op jit(solution)/shard_map/ppermute | solution.py:345
  117.1 20.7 %copy-start.2 = (bf16[128,2048]{1,0:T(8,128)(2,1)S(1)}, bf16[128,2048]{1,0:T(8,128)(2,1)}, u32[]{:S(2)}) copy-start(bf16[128,2048]{1,0:T(8,128)(2,1)} %out_proj.1) | copy-start | bytes 1572868
  139.1 14.4 %all-to-all-start.3 = ((bf16[4,576,128]{2,1,0:T(8,128)(2,1)}), bf16[4,576,128]{2,1,0:T(8,128)(2,1)S(1)}, u32[]{:S(2)}, u32[]{:S(2)}) async-start(bf16[4,576,128]{2,1,0:T(8,128)(2,1)} %bitcast.20), calls=%async_computation.3 | async-start | bytes 1179648 | tf_op jit(solution)/shard_map/all_to_all | solution.py:396
  142.9 18.2 %copy-start.7 = (bf16[2,2048,128]{2,1,0:T(8,128)(2,1)S(1)}, bf16[2,2048,128]{2,1,0:T(8,128)(2,1)}, u32[]{:S(2)}) copy-start(bf16[2,2048,128]{2,1,0:T(8,128)(2,1)} %get-tuple-element.45) | copy-start | bytes 3145732
  154.3 16.0 %all-to-all-start.4 = ((bf16[8,72,128]{2,1,0:T(8,128)(2,1)}), bf16[8,72,128]{2,1,0:T(8,128)(2,1)S(1)}, u32[]{:S(2)}, u32[]{:S(2)}) async-start(bf16[8,72,128]{2,1,0:T(8,128)(2,1)} %get-tuple-element.55), calls=%async_computation.4 | async-start | bytes 294912 | tf_op jit(solution)/shard_map/all_to_all | solution.py:398

commit v7 on v5

--- a/solution.py
+++ b/solution.py
@@ -120,11 +120,11 @@
     return call(sort_body, out, recv, scratch=[pltpu.VMEM(recv.shape, F32)], kept=(0, 1))
 
 
-def shards(chip, both, f1, b1, f2, b2, n_y):
+def shards(chip, both, f1, b1, f2, b2, near, n_y):
     found = []
     for off, ref in ((0, both), (n_y - 1, f1), (1, b1)):
         for n in range(2):
-            found.append((off + 4 * n, [ref[n, i] for i in range(4)]))
+            found.append((off + 4 * n, [near[i] if off == n == 0 else ref[n, i] for i in range(4)]))
     for off, ref in ((n_y - 2, f2), (2, b2)):
         found.append((off, [ref[i] for i in range(4)]))
     for off, p in found:
@@ -132,7 +132,7 @@
         yield y, jnp.concatenate(p[:2], axis=1), jnp.concatenate(p[2:], axis=1)
 
 
-def expert_body(chip, both, f1, b1, f2, b2, wgu_peer, wg, wu, wd, wd_peer, gu_grad, hidden, part):
+def expert_body(chip, both, f1, b1, f2, b2, near, wgu_peer, wg, wu, wd, wd_peer, gu_grad, hidden, part):
     n_y = part.shape[0]
     fw = wd.shape[0]
     rows, hid = hidden.shape
@@ -143,7 +143,7 @@
         at = pl.ds(pl.multiple_of(y * 2 * fw, 2 * fw), 2 * fw)
         return jnp.concatenate([wg[at, :], wgu_peer[0, at, :], wu[at, :], wgu_peer[1, at, :]], axis=1), at
 
-    for y, x_in, x_cot in shards(chip[0], both, f1, b1, f2, b2, n_y):
+    for y, x_in, x_cot in shards(chip[0], both, f1, b1, f2, b2, near, n_y):
         w, at = weights(y)
         acc = acc + dot(x_in, w, ((1,), (0,)))
         back = back + dot(x_cot, jnp.concatenate([wd[:, at], wd_peer[:, at]], axis=0), ((1,), (1,)))
@@ -171,11 +171,11 @@
     return call(expert_body, out, chip, *blocks, *weights, scalars=1)
 
 
-def weight_body(chip, both, f1, b1, f2, b2, gu_grad, hidden, dgu, dgu_send, dd, dd_send):
+def weight_body(chip, both, f1, b1, f2, b2, near, gu_grad, hidden, dgu, dgu_send, dd, dd_send):
     fw = dd.shape[0]
     hid = hidden.shape[1]
     n_y = dd.shape[1] // (2 * fw)
-    for y, x_in, x_cot in shards(chip[0], both, f1, b1, f2, b2, n_y):
+    for y, x_in, x_cot in shards(chip[0], both, f1, b1, f2, b2, near, n_y):
         at = pl.ds(pl.multiple_of(y * 2 * fw, 2 * fw), 2 * fw)
         r = dot(x_in, gu_grad[...], ((0,), (0,))).astype(BF16)
         for i in range(2):
@@ -189,7 +189,7 @@
 def expert_weight_grads(chip, blocks, gu_grad, hidden, d):
     fw = blocks[0].shape[3]
     out = (whole((2, d, fw), BF16),) * 2 + (whole((fw, d), BF16),) * 2
-    return call(weight_body, out, chip, *blocks, gu_grad, hidden, scalars=1, loose=(6, 7))
+    return call(weight_body, out, chip, *blocks, gu_grad, hidden, scalars=1, loose=(7, 8))
 
 
 def add_body(parts, out, *, half):
@@ -319,12 +319,12 @@
     recv = lax.all_to_all(send.reshape(n_sp, -1, fw), SP, 0, 0, tiled=True).reshape(send.shape)
     both, near = sort_pieces(recv)
 
-    near, late_gate, late_up, late_down = lax.optimization_barrier((near, gate_w, up_w, down_w))
+    late_gate, late_up, late_down = gate_w, up_w, down_w
     wgu = jnp.concatenate([late_gate, late_up], axis=0)
     wgu_peer = over_cores(wgu)
     wd_peer = over_cores(late_down[0])
     first = (both, over_y(both, 1), over_y(both, -1))
-    blocks = (*first, over_y(near, 2), over_y(near, -2))
+    blocks = (*first, over_y(near, 2), over_y(near, -2), near)
 
     gu_grad, hidden, part = expert_rows_grad(
         chip, blocks, wgu_peer, late_gate[0], late_up[0], late_down[0], wd_peer, n_y

time: 168 us -> 166 us (0.988)
  blocking collectives: 45.5 us -> 17.6 us
  starting transfers between devices: 48.7 us -> 64.7 us
  waiting for transfers between devices: 53.9 us -> 59.7 us
    all_to_all x1 -> x0, blocking collectives: 27.9 us -> none  [per_device(): lax.all_to_all(send.reshape(n_sp, -1, fw), SP, 0, 0, tiled=True)]
    all_to_all x0 -> x1, starting transfers between devices: none -> 13.3 us  [per_device(): lax.all_to_all(send.reshape(n_sp, -1, fw), SP, 0, 0, tiled=True)]
    all_to_all x0 -> x1, waiting for transfers between devices: none -> 12.4 us  [per_device(): lax.all_to_all(send.reshape(n_sp, -1, fw), SP, 0, 0, tiled=True)]
    ppermute x5, waiting for transfers between devices: 17.9 us -> 12.4 us  [over_y(): return lax.ppermute(v, 'y', [(i, (i + step) % n_y) for i in range(n_y)])]
  transfers between devices with their start and end apart: 13 -> 14, of which waited for: 6 -> 7; matrix products, arithmetic and copies ran while one was open for 2% -> 3% of each run, Pallas kernels for 3% -> 4%
where the time goes in v7:
time: 166 us; the launch traced here: 165 us
  starting transfers between devices  64.7 us (39%)
  waiting for transfers between devices  59.7 us (36%)
  blocking collectives  17.6 us (11%)
  Pallas kernels  12.9 us (8%)
  other arithmetic  5.44 us (3%)
  local copies, waits for them, and re-layouts  3.11 us (2%)
    ppermute x5, starting transfers between devices, over_y(): return lax.ppermute(v, 'y', [(i, (i + step) % n_y) for i in range(n_y)])  22 us
    all_gather x1, blocking collectives, per_device(): mix_grad = lax.all_gather(own_grad, TP, axis=1, tiled=True)  17.6 us
    all_to_all x1, waiting for transfers between devices, per_device(): last = lax.all_to_all(last, SP, 0, 0, tiled=True)  16.8 us
    all_to_all x1, waiting for transfers between devices, per_device(): lax.all_to_all(part.reshape(2 * n_y, *part.shape[2:]), TP, 0, 0, tiled=True)  16.5 us
    all_to_all x1, starting transfers between devices, per_device(): lax.all_to_all(send.reshape(n_sp, -1, fw), SP, 0, 0, tiled=True)  13.3 us
    pallas_call x8, Pallas kernels, call(): pl.pallas_call(body, out_shape=tuple(outs), in_specs=[SMEM] * scalars + [...  12.9 us
    all_to_all x1, waiting for transfers between devices, per_device(): lax.all_to_all(send.reshape(n_sp, -1, fw), SP, 0, 0, tiled=True)  12.4 us
    ppermute x5, waiting for transfers between devices, over_y(): return lax.ppermute(v, 'y', [(i, (i + step) % n_y) for i in range(n_y)])  12.4 us
  transfers between devices with their start and end apart: 14, of which 7 were waited for; matrix products, arithmetic and copies ran while one was open for 3% of the time, Pallas kernels for 4%

profile of v7, /device:TPU:8, one launch (start us, length us, event | category | flops | bytes accessed | tf_op | source)
XLA Modules:
  0.0 164.6 jit_solution(11186698278313227972)
XLA Ops:
  1.4 6.8 %collective-permute-start = (bf16[2,128,128]{2,1,0:T(8,128)(2,1)S(1)}, bf16[2,128,128]{2,1,0:T(8,128)(2,1)S(1)}, u32[]{:S(2)}, u32[]{:S(2)}) collective-permute-start(bf16[2,128,128]{2,1,0:T(8,128)(2,1)S(1)} %get-tuple-element.55), channel_id=1, source_target_pairs={{0,8},{2,10},{4,12},{6,14},{8,0},{10,2},{12,4},{14,6},{1,9},{3,11}... | collective-permute-start | bytes 196616 | tf_op jit(solution)/shard_map/ppermute | solution.py:307
  8.3 3.2 %collective-permute-done = bf16[2,128,128]{2,1,0:T(8,128)(2,1)S(1)} collective-permute-done((bf16[2,128,128]{2,1,0:T(8,128)(2,1)S(1)}, bf16[2,128,128]{2,1,0:T(8,128)(2,1)S(1)}, u32[]{:S(2)}, u32[]{:S(2)}) %collective-permute-start) | collective-permute-done | bytes 65568 | tf_op jit(solution)/shard_map/ppermute | solution.py:307
  11.5 1.9 %collective-permute-start.1 = (bf16[2,2,128,128]{3,2,1,0:T(8,128)(2,1)S(1)}, bf16[2,2,128,128]{3,2,1,0:T(8,128)(2,1)S(1)}, u32[]{:S(2)}, u32[]{:S(2)}) collective-permute-start(bf16[2,2,128,128]{3,2,1,0:T(8,128)(2,1)S(1)} %pad_maximum_fusion.1.mine), channel_id=1, source_target_pairs={{0,1},{1,0},{2,3},{3,2},{4,5},{5,4},{6,7},{7,6},{8,9},{9,8},{10,11... | collective-permute-start | bytes 393224 | tf_op jit(solution)/shard_map/ppermute | solution.py:310
  13.4 2.3 %pad_maximum_fusion = bf16[2,2048,128]{2,1,0:T(8,128)(2,1)} fusion(bf16[1,2048,128]{2,1,0:T(8,128)(2,1)} %param.18, bf16[1,2048,128]{2,1,0:T(8,128)(2,1)} %param.17), kind=kLoop, calls=%fused_computation.2 | loop fusion | flops 524288 | bytes 2097152 | tf_op jit(solution)/shard_map/concatenate | solution.py:323
  15.7 2.4 %collective-permute-start.6 = (bf16[2,2048,128]{2,1,0:T(8,128)(2,1)}, bf16[2,2048,128]{2,1,0:T(8,128)(2,1)S(1)}, u32[]{:S(2)}, u32[]{:S(2)}) collective-permute-start(bf16[2,2048,128]{2,1,0:T(8,128)(2,1)} %pad_maximum_fusion), channel_id=1, source_target_pairs={{0,1},{1,0},{2,3},{3,2},{4,5},{5,4},{6,7},{7,6},{8,9},{9,8},{10,11... | collective-permute-start | bytes 3145736 | tf_op jit(solution)/shard_map/ppermute | solution.py:310
  18.8 0.9 shard_map.180
  19.7 1.0 shard_map.181
  20.7 13.3 %all-to-all-start = ((bf16[32,40,128]{2,1,0:T(8,128)(2,1)}), bf16[32,40,128]{2,1,0:T(8,128)(2,1)S(1)}, u32[]{:S(2)}, u32[]{:S(2)}) async-start(bf16[32,40,128]{2,1,0:T(8,128)(2,1)} %bitcast.8), calls=%async_computation | async-start | bytes 655360 | tf_op jit(solution)/shard_map/all_to_all | solution.py:319
  34.0 1.9 %collective-permute-start.7 = (bf16[128,2048]{1,0:T(8,128)(2,1)}, bf16[128,2048]{1,0:T(8,128)(2,1)}, u32[]{:S(2)}, u32[]{:S(2)}) collective-permute-start(bf16[128,2048]{1,0:T(8,128)(2,1)} %bitcast.27), channel_id=1, source_target_pairs={{0,1},{1,0},{2,3},{3,2},{4,5},{5,4},{6,7},{7,6},{8,9},{9,8},{10,11... | collective-permute-start | bytes 1572872 | tf_op jit(solution)/shard_map/ppermute | solution.py:310
  36.0 12.4 %all-to-all-done = bf16[32,40,128]{2,1,0:T(8,128)(2,1)S(1)} async-done(((bf16[32,40,128]{2,1,0:T(8,128)(2,1)}), bf16[32,40,128]{2,1,0:T(8,128)(2,1)S(1)}, u32[]{:S(2)}, u32[]{:S(2)}) %all-to-all-start) | async-done | bytes 327712 | tf_op jit(solution)/shard_map/all_to_all | solution.py:319
  48.6 3.0 %collective-permute-start.3 = (bf16[2,4,160,128]{3,2,1,0:T(8,128)(2,1)S(1)}, bf16[2,4,160,128]{3,2,1,0:T(8,128)(2,1)S(1)}, u32[]{:S(2)}, u32[]{:S(2)}) collective-permute-start(bf16[2,4,160,128]{3,2,1,0:T(8,128)(2,1)S(1)} %get-tuple-element.30.both), channel_id=1, source_target_pairs={{0,14},{2,0},{4,2},{6,4},{8,6},{10,8},{12,10},{14,12},{1,15},{3,1}... | collective-permute-start | bytes 983048 | tf_op jit(solution)/shard_map/ppermute | solution.py:307
  51.5 3.5 %collective-permute-start.2 = (bf16[2,4,160,128]{3,2,1,0:T(8,128)(2,1)S(1)}, bf16[2,4,160,128]{3,2,1,0:T(8,128)(2,1)S(1)}, u32[]{:S(2)}, u32[]{:S(2)}) collective-permute-start(bf16[2,4,160,128]{3,2,1,0:T(8,128)(2,1)S(1)} %get-tuple-element.30.both), channel_id=1, source_target_pairs={{0,2},{2,4},{4,6},{6,8},{8,10},{10,12},{12,14},{14,0},{1,3},{3,5},... | collective-permute-start | bytes 983048 | tf_op jit(solution)/shard_map/ppermute | solution.py:307
  55.0 6.9 %collective-permute-start.5 = (bf16[4,160,128]{2,1,0:T(8,128)(2,1)S(1)}, bf16[4,160,128]{2,1,0:T(8,128)(2,1)S(1)}, u32[]{:S(2)}, u32[]{:S(2)}) collective-permute-start(bf16[4,160,128]{2,1,0:T(8,128)(2,1)S(1)} %get-tuple-element.31.near), channel_id=1, source_target_pairs={{0,12},{2,14},{4,0},{6,2},{8,4},{10,6},{12,8},{14,10},{1,13},{3,15... | collective-permute-start | bytes 491528 | tf_op jit(solution)/shard_map/ppermute | solution.py:307
  61.9 1.9 %collective-permute-start.4 = (bf16[4,160,128]{2,1,0:T(8,128)(2,1)S(1)}, bf16[4,160,128]{2,1,0:T(8,128)(2,1)}, u32[]{:S(2)}, u32[]{:S(2)}) collective-permute-start(bf16[4,160,128]{2,1,0:T(8,128)(2,1)S(1)} %get-tuple-element.31.near), channel_id=1, source_target_pairs={{0,4},{2,6},{4,8},{6,10},{8,12},{10,14},{12,0},{14,2},{1,5},{3,7},... | collective-permute-start | bytes 491528 | tf_op jit(solution)/shard_map/ppermute | solution.py:307
  63.8 2.7 %collective-permute-done.5.b2 = bf16[4,160,128]{2,1,0:T(8,128)(2,1)S(1)} collective-permute-done((bf16[4,160,128]{2,1,0:T(8,128)(2,1)S(1)}, bf16[4,160,128]{2,1,0:T(8,128)(2,1)S(1)}, u32[]{:S(2)}, u32[]{:S(2)}) %collective-permute-start.5) | collective-permute-done | bytes 163872 | tf_op jit(solution)/shard_map/ppermute | solution.py:307
  66.5 6.5 %collective-permute-done.4.f2 = bf16[4,160,128]{2,1,0:T(8,128)(2,1)} collective-permute-done((bf16[4,160,128]{2,1,0:T(8,128)(2,1)S(1)}, bf16[4,160,128]{2,1,0:T(8,128)(2,1)}, u32[]{:S(2)}, u32[]{:S(2)}) %collective-permute-start.4) | collective-permute-done | bytes 163872 | tf_op jit(solution)/shard_map/ppermute | solution.py:307
  73.0 1.0 copy-done.2
  74.1 4.0 %shard_map.183 = (bf16[160,512]{1,0:T(8,128)(2,1)}, bf16[160,256]{1,0:T(8,128)(2,1)}, bf16[8,2,160,128]{3,2,1,0:T(8,128)(2,1)}) custom-call(s32[1]{0:T(128)} %bitcast.chip, bf16[2,4,160,128]{3,2,1,0:T(8,128)(2,1)S(1)} %get-tuple-element.30.both, bf16[2,4,160,128]{3,2,1,0:T(8,128)(2,1)S(1)} %collective-permute-done.2.f1, ...), custom_call_target="tpu_custom_call" | custom-call | tf_op jit(solution)/shard_map/pallas_call | solution.py:31
  78.1 4.3 %all-to-all-start.1 = ((bf16[16,160,128]{2,1,0:T(8,128)(2,1)}), bf16[16,160,128]{2,1,0:T(8,128)(2,1)S(1)}, u32[]{:S(2)}, u32[]{:S(2)}) async-start(bf16[16,160,128]{2,1,0:T(8,128)(2,1)} %bitcast.31), calls=%async_computation.1 | async-start | bytes 1310720 | tf_op jit(solution)/shard_map/all_to_all | solution.py:347
  82.3 16.5 %all-to-all-done.1 = bf16[16,160,128]{2,1,0:T(8,128)(2,1)S(1)} async-done(((bf16[16,160,128]{2,1,0:T(8,128)(2,1)}), bf16[16,160,128]{2,1,0:T(8,128)(2,1)S(1)}, u32[]{:S(2)}, u32[]{:S(2)}) %all-to-all-start.1) | async-done | bytes 655392 | tf_op jit(solution)/shard_map/all_to_all | solution.py:347
  98.8 1.0 shard_map.185
  99.9 5.2 %all-to-all-start.2 = ((bf16[32,16,128]{2,1,0:T(8,128)(2,1)}), bf16[32,16,128]{2,1,0:T(8,128)(2,1)S(1)}, u32[]{:S(2)}, u32[]{:S(2)}) async-start(bf16[32,16,128]{2,1,0:T(8,128)(2,1)} %bitcast.17), calls=%async_computation.2 | async-start | bytes 262144 | tf_op jit(solution)/shard_map/all_to_all | solution.py:349
  106.3 3.6 %shard_map.184 = (bf16[2,2048,128]{2,1,0:T(8,128)(2,1)}, bf16[2,2048,128]{2,1,0:T(8,128)(2,1)}, bf16[128,2048]{1,0:T(8,128)(2,1)}, bf16[128,2048]{1,0:T(8,128)(2,1)}) custom-call(s32[1]{0:T(128)} %bitcast.chip, bf16[2,4,160,128]{3,2,1,0:T(8,128)(2,1)S(1)} %get-tuple-element.30.both, bf16[2,4,160,128]{3,2,1,0:T(8,128)(2,1)S(1)} %collective-permute-done.2.f1, ...), custom_call_target="tpu_custom_call" | custom-call | tf_op jit(solution)/shard_map/pallas_call | solution.py:31
  109.9 2.0 %collective-permute-start.9 = (bf16[128,2048]{1,0:T(8,128)(2,1)}, bf16[128,2048]{1,0:T(8,128)(2,1)S(1)}, u32[]{:S(2)}, u32[]{:S(2)}) collective-permute-start(bf16[128,2048]{1,0:T(8,128)(2,1)} %get-tuple-element.37), channel_id=1, source_target_pairs={{0,1},{1,0},{2,3},{3,2},{4,5},{5,4},{6,7},{7,6},{8,9},{9,8},{10,11... | collective-permute-start | bytes 1572872 | tf_op jit(solution)/shard_map/ppermute | solution.py:310
  112.0 2.4 %collective-permute-start.8 = (bf16[2,2048,128]{2,1,0:T(8,128)(2,1)}, bf16[2,2048,128]{2,1,0:T(8,128)(2,1)S(1)}, u32[]{:S(2)}, u32[]{:S(2)}) collective-permute-start(bf16[2,2048,128]{2,1,0:T(8,128)(2,1)} %get-tuple-element.35), channel_id=1, source_target_pairs={{0,1},{1,0},{2,3},{3,2},{4,5},{5,4},{6,7},{7,6},{8,9},{9,8},{10,11... | collective-permute-start | bytes 3145736 | tf_op jit(solution)/shard_map/ppermute | solution.py:310
  114.4 1.5 all-to-all-done.2
  116.2 17.6 %all_gather.3.mix = bf16[128,2048]{1,0:T(8,128)(2,1)S(1)} all-gather(bf16[128,128]{1,0:T(8,128)(2,1)S(1)} %fusion), channel_id=1, replica_groups=mesh['z'=8,'x'=4,'y'=8,'c'=2] {'y','c'}, dimensions={1}, use_global_device_ids=true | all-gather | bytes 557056 | tf_op jit(solution)/shard_map/all_gather | solution.py:356
  133.8 1.3 shard_map.186
  135.1 9.2 %all-to-all-start.3 = ((bf16[32,72,128]{2,1,0:T(8,128)(2,1)}), bf16[32,72,128]{2,1,0:T(8,128)(2,1)S(1)}, u32[]{:S(2)}, u32[]{:S(2)}) async-start(bf16[32,72,128]{2,1,0:T(8,128)(2,1)} %get-tuple-element.42), calls=%async_computation.3 | async-start | bytes 1179648 | tf_op jit(solution)/shard_map/all_to_all | solution.py:359
  144.4 0.9 fusion.1
  145.8 1.2 add_convert_fusion.1
  147.0 16.8 %all-to-all-done.3.last = bf16[32,72,128]{2,1,0:T(8,128)(2,1)S(1)} async-done(((bf16[32,72,128]{2,1,0:T(8,128)(2,1)}), bf16[32,72,128]{2,1,0:T(8,128)(2,1)S(1)}, u32[]{:S(2)}, u32[]{:S(2)}) %all-to-all-start.3) | async-done | bytes 589856 | tf_op jit(solution)/shard_map/all_to_all | solution.py:359
  (48 shorter events, 4.3 us)
Async XLA Ops:
  1.4 10.1 %collective-permute-start = (bf16[2,128,128]{2,1,0:T(8,128)(2,1)S(1)}, bf16[2,128,128]{2,1,0:T(8,128)(2,1)S(1)}, u32[]{:S(2)}, u32[]{:S(2)}) collective-permute-start(bf16[2,128,128]{2,1,0:T(8,128)(2,1)S(1)} %get-tuple-element.55), channel_id=1, source_target_pairs={{0,8},{2,10},{4,12},{6,14},{8,0},{10,2},{12,4},{14,6},{1,9},{3,11}... | collective-permute-start | bytes 196616 | tf_op jit(solution)/shard_map/ppermute | solution.py:307
  11.5 8.2 %collective-permute-start.1 = (bf16[2,2,128,128]{3,2,1,0:T(8,128)(2,1)S(1)}, bf16[2,2,128,128]{3,2,1,0:T(8,128)(2,1)S(1)}, u32[]{:S(2)}, u32[]{:S(2)}) collective-permute-start(bf16[2,2,128,128]{3,2,1,0:T(8,128)(2,1)S(1)} %pad_maximum_fusion.1.mine), channel_id=1, source_target_pairs={{0,1},{1,0},{2,3},{3,2},{4,5},{5,4},{6,7},{7,6},{8,9},{9,8},{10,11... | collective-permute-start | bytes 393224 | tf_op jit(solution)/shard_map/ppermute | solution.py:310
  13.4 4.7 %copy-start.7 = (f32[128,2]{0,1:T(2,128)S(1)}, f32[128,2]{0,1:T(2,128)}, u32[]{:S(2)}) copy-start(f32[128,2]{0,1:T(2,128)} %param.16) | copy-start | bytes 3076
  15.7 57.3 %collective-permute-start.6 = (bf16[2,2048,128]{2,1,0:T(8,128)(2,1)}, bf16[2,2048,128]{2,1,0:T(8,128)(2,1)S(1)}, u32[]{:S(2)}, u32[]{:S(2)}) collective-permute-start(bf16[2,2048,128]{2,1,0:T(8,128)(2,1)} %pad_maximum_fusion), channel_id=1, source_target_pairs={{0,1},{1,0},{2,3},{3,2},{4,5},{5,4},{6,7},{7,6},{8,9},{9,8},{10,11... | collective-permute-start | bytes 3145736 | tf_op jit(solution)/shard_map/ppermute | solution.py:310
  18.1 0.7 copy-start.6
  19.7 53.3 %copy-start.1 = (bf16[1,2048,128]{2,1,0:T(8,128)(2,1)S(1)}, bf16[1,2048,128]{2,1,0:T(8,128)(2,1)}, u32[]{:S(2)}) copy-start(bf16[1,2048,128]{2,1,0:T(8,128)(2,1)} %param.17) | copy-start | bytes 1572868
  20.7 52.3 %copy-start = (bf16[1,2048,128]{2,1,0:T(8,128)(2,1)S(1)}, bf16[1,2048,128]{2,1,0:T(8,128)(2,1)}, u32[]{:S(2)}) copy-start(bf16[1,2048,128]{2,1,0:T(8,128)(2,1)} %param.18) | copy-start | bytes 1572868
  20.7 27.7 %all-to-all-start = ((bf16[32,40,128]{2,1,0:T(8,128)(2,1)}), bf16[32,40,128]{2,1,0:T(8,128)(2,1)S(1)}, u32[]{:S(2)}, u32[]{:S(2)}) async-start(bf16[32,40,128]{2,1,0:T(8,128)(2,1)} %bitcast.8), calls=%async_computation | async-start | bytes 655360 | tf_op jit(solution)/shard_map/all_to_all | solution.py:319
  34.0 27.8 %collective-permute-start.7 = (bf16[128,2048]{1,0:T(8,128)(2,1)}, bf16[128,2048]{1,0:T(8,128)(2,1)}, u32[]{:S(2)}, u32[]{:S(2)}) collective-permute-start(bf16[128,2048]{1,0:T(8,128)(2,1)} %bitcast.27), channel_id=1, source_target_pairs={{0,1},{1,0},{2,3},{3,2},{4,5},{5,4},{6,7},{7,6},{8,9},{9,8},{10,11... | collective-permute-start | bytes 1572872 | tf_op jit(solution)/shard_map/ppermute | solution.py:310
  48.6 24.4 %collective-permute-start.3 = (bf16[2,4,160,128]{3,2,1,0:T(8,128)(2,1)S(1)}, bf16[2,4,160,128]{3,2,1,0:T(8,128)(2,1)S(1)}, u32[]{:S(2)}, u32[]{:S(2)}) collective-permute-start(bf16[2,4,160,128]{3,2,1,0:T(8,128)(2,1)S(1)} %get-tuple-element.30.both), channel_id=1, source_target_pairs={{0,14},{2,0},{4,2},{6,4},{8,6},{10,8},{12,10},{14,12},{1,15},{3,1}... | collective-permute-start | bytes 983048 | tf_op jit(solution)/shard_map/ppermute | solution.py:307
  51.5 21.5 %collective-permute-start.2 = (bf16[2,4,160,128]{3,2,1,0:T(8,128)(2,1)S(1)}, bf16[2,4,160,128]{3,2,1,0:T(8,128)(2,1)S(1)}, u32[]{:S(2)}, u32[]{:S(2)}) collective-permute-start(bf16[2,4,160,128]{3,2,1,0:T(8,128)(2,1)S(1)} %get-tuple-element.30.both), channel_id=1, source_target_pairs={{0,2},{2,4},{4,6},{6,8},{8,10},{10,12},{12,14},{14,0},{1,3},{3,5},... | collective-permute-start | bytes 983048 | tf_op jit(solution)/shard_map/ppermute | solution.py:307
  55.0 11.5 %collective-permute-start.5 = (bf16[4,160,128]{2,1,0:T(8,128)(2,1)S(1)}, bf16[4,160,128]{2,1,0:T(8,128)(2,1)S(1)}, u32[]{:S(2)}, u32[]{:S(2)}) collective-permute-start(bf16[4,160,128]{2,1,0:T(8,128)(2,1)S(1)} %get-tuple-element.31.near), channel_id=1, source_target_pairs={{0,12},{2,14},{4,0},{6,2},{8,4},{10,6},{12,8},{14,10},{1,13},{3,15... | collective-permute-start | bytes 491528 | tf_op jit(solution)/shard_map/ppermute | solution.py:307
  61.9 11.1 %collective-permute-start.4 = (bf16[4,160,128]{2,1,0:T(8,128)(2,1)S(1)}, bf16[4,160,128]{2,1,0:T(8,128)(2,1)}, u32[]{:S(2)}, u32[]{:S(2)}) collective-permute-start(bf16[4,160,128]{2,1,0:T(8,128)(2,1)S(1)} %get-tuple-element.31.near), channel_id=1, source_target_pairs={{0,4},{2,6},{4,8},{6,10},{8,12},{10,14},{12,0},{14,2},{1,5},{3,7},... | collective-permute-start | bytes 491528 | tf_op jit(solution)/shard_map/ppermute | solution.py:307
  73.0 1.0 copy-start.2
  78.1 4.3 %copy-start.16 = (f32[128]{0:T(128)S(1)}, f32[128]{0:T(128)}, u32[]{:S(2)}) copy-start(f32[128]{0:T(128)} %param.25) | copy-start | bytes 1540
  78.1 20.8 %all-to-all-start.1 = ((bf16[16,160,128]{2,1,0:T(8,128)(2,1)}), bf16[16,160,128]{2,1,0:T(8,128)(2,1)S(1)}, u32[]{:S(2)}, u32[]{:S(2)}) async-start(bf16[16,160,128]{2,1,0:T(8,128)(2,1)} %bitcast.31), calls=%async_computation.1 | async-start | bytes 1310720 | tf_op jit(solution)/shard_map/all_to_all | solution.py:347
  99.9 5.3 %copy-start.12 = (bf16[128,128]{1,0:T(8,128)(2,1)S(1)}, bf16[128,128]{1,0:T(8,128)(2,1)}, u32[]{:S(2)}) copy-start(bf16[128,128]{1,0:T(8,128)(2,1)} %param.22) | copy-start | bytes 98308
  99.9 5.3 %copy-start.13 = (bf16[128,128]{1,0:T(8,128)(2,1)S(1)}, bf16[128,128]{1,0:T(8,128)(2,1)}, u32[]{:S(2)}) copy-start(bf16[128,128]{1,0:T(8,128)(2,1)} %param.21) | copy-start | bytes 98308
  99.9 5.3 %copy-start.14 = (bf16[128,128]{1,0:T(8,128)(2,1)S(1)}, bf16[128,128]{1,0:T(8,128)(2,1)}, u32[]{:S(2)}) copy-start(bf16[128,128]{1,0:T(8,128)(2,1)} %param.24) | copy-start | bytes 98308
  99.9 5.3 %copy-start.15 = (bf16[128,128]{1,0:T(8,128)(2,1)S(1)}, bf16[128,128]{1,0:T(8,128)(2,1)}, u32[]{:S(2)}) copy-start(bf16[128,128]{1,0:T(8,128)(2,1)} %param.23) | copy-start | bytes 98308
  99.9 16.0 %all-to-all-start.2 = ((bf16[32,16,128]{2,1,0:T(8,128)(2,1)}), bf16[32,16,128]{2,1,0:T(8,128)(2,1)S(1)}, u32[]{:S(2)}, u32[]{:S(2)}) async-start(bf16[32,16,128]{2,1,0:T(8,128)(2,1)} %bitcast.17), calls=%async_computation.2 | async-start | bytes 262144 | tf_op jit(solution)/shard_map/all_to_all | solution.py:349
  105.3 0.9 copy-start.4
  105.3 1.0 copy-start.5
  106.3 9.6 %copy-start.10 = (bf16[512,128]{1,0:T(8,128)(2,1)S(1)}, bf16[512,128]{1,0:T(8,128)(2,1)}, u32[]{:S(2)}) copy-start(bf16[512,128]{1,0:T(8,128)(2,1)} %get-tuple-element.40) | copy-start | bytes 393220
  106.3 9.6 %copy-start.11 = (bf16[128,128]{1,0:T(8,128)(2,1)S(1)}, bf16[128,128]{1,0:T(8,128)(2,1)}, u32[]{:S(2)}) copy-start(bf16[128,128]{1,0:T(8,128)(2,1)} %param.14) | copy-start | bytes 98308
  109.9 23.9 %copy-start.3 = (bf16[128,2048]{1,0:T(8,128)(2,1)S(1)}, bf16[128,2048]{1,0:T(8,128)(2,1)}, u32[]{:S(2)}) copy-start(bf16[128,2048]{1,0:T(8,128)(2,1)} %out_proj.1) | copy-start | bytes 1572868
  109.9 34.4 %collective-permute-start.9 = (bf16[128,2048]{1,0:T(8,128)(2,1)}, bf16[128,2048]{1,0:T(8,128)(2,1)S(1)}, u32[]{:S(2)}, u32[]{:S(2)}) collective-permute-start(bf16[128,2048]{1,0:T(8,128)(2,1)} %get-tuple-element.37), channel_id=1, source_target_pairs={{0,1},{1,0},{2,3},{3,2},{4,5},{5,4},{6,7},{7,6},{8,9},{9,8},{10,11... | collective-permute-start | bytes 1572872 | tf_op jit(solution)/shard_map/ppermute | solution.py:310
  112.0 33.3 %collective-permute-start.8 = (bf16[2,2048,128]{2,1,0:T(8,128)(2,1)}, bf16[2,2048,128]{2,1,0:T(8,128)(2,1)S(1)}, u32[]{:S(2)}, u32[]{:S(2)}) collective-permute-start(bf16[2,2048,128]{2,1,0:T(8,128)(2,1)} %get-tuple-element.35), channel_id=1, source_target_pairs={{0,1},{1,0},{2,3},{3,2},{4,5},{5,4},{6,7},{7,6},{8,9},{9,8},{10,11... | collective-permute-start | bytes 3145736 | tf_op jit(solution)/shard_map/ppermute | solution.py:310
  135.1 9.2 %copy-start.9 = (bf16[128,2048]{1,0:T(8,128)(2,1)S(1)}, bf16[128,2048]{1,0:T(8,128)(2,1)}, u32[]{:S(2)}) copy-start(bf16[128,2048]{1,0:T(8,128)(2,1)} %get-tuple-element.36) | copy-start | bytes 1572868
  135.1 28.7 %all-to-all-start.3 = ((bf16[32,72,128]{2,1,0:T(8,128)(2,1)}), bf16[32,72,128]{2,1,0:T(8,128)(2,1)S(1)}, u32[]{:S(2)}, u32[]{:S(2)}) async-start(bf16[32,72,128]{2,1,0:T(8,128)(2,1)} %get-tuple-element.42), calls=%async_computation.3 | async-start | bytes 1179648 | tf_op jit(solution)/shard_map/all_to_all | solution.py:359
  144.3 1.4 copy-start.8
